TPU v7x, 256 devices: a whole 4x4x8 slice. The times are simulated.
256 devices in a mesh: ep: 64 (over z, y, core), tp: 4 (over x).
Axes of the slice: x: 4, y: 4, z: 8, core: 2. Of those that a mesh axis runs over, the one named last changes fastest.
Arguments:
- tokens: bfloat16 [1024, 2048], P('ep'), may hold values from -6 to 6
- lengths: int32 [1024], P('ep'), may hold values from 256 to 1023
- cache: bfloat16 [1024, 1024, 512], P('ep', None, 'tp'), may hold values from -6 to 6
- attn_gain: float32 [2048], replicated, may hold values from 0.1 to 1.9
- query_weight: bfloat16 [2048, 1024], P(None, 'tp'), may hold values from -0.125 to 0.125
- key_weight: bfloat16 [2048, 256], P(None, 'tp'), may hold values from -0.125 to 0.125
- value_weight: bfloat16 [2048, 256], P(None, 'tp'), may hold values from -0.125 to 0.125
- stick_bias: float32 [16], P('tp'), may hold values from -7 to -1
- out_weight: bfloat16 [1024, 2048], P('tp'), may hold values from -0.1875 to 0.1875
- ffn_gain: float32 [2048], replicated, may hold values from 0.1 to 1.9
- routes: int32 [1024, 6], P('ep'), may hold values from 0 to 63, all different within a row; in each aligned block of 16 rows (0 to 15, 16 to 31, ...) at most 3 rows name the same one
- route_weights: float32 [1024, 6], P('ep'), may hold values from 0.1 to 0.6
- expert_gate: bfloat16 [64, 2048, 1024], P('ep', None, 'tp'), may hold values from -0.125 to 0.125
- expert_up: bfloat16 [64, 2048, 1024], P('ep', None, 'tp'), may hold values from -0.125 to 0.125
- expert_down: bfloat16 [64, 1024, 2048], P('ep', 'tp'), may hold values from -0.1875 to 0.1875
- shared_gate: bfloat16 [2048, 512], P('ep', 'tp'), may hold values from -0.125 to 0.125
- shared_up: bfloat16 [2048, 512], P('ep', 'tp'), may hold values from -0.125 to 0.125
- shared_down: bfloat16 [512, 2048], P('tp'), may hold values from -0.25 to 0.25
- gate_vector: bfloat16 [2048], replicated, may hold values from -0.125 to 0.125
Outputs:
- layer_out: bfloat16 [1024, 2048], P('ep', 'tp')
- new_kv: bfloat16 [1024, 512], P('ep', 'tp')
Inputs may be any that keep to these rules, and one draw needn't show every extreme that they name: Each sequence's new token comes after its lengths cached positions. `routes`: each row names 6 different experts; among the 16 rows of one index of ep no expert is named by more than 3 rows.
All inputs are finite; a program needn't handle non-finite values.
Results may differ from a plain program's by a relative error of at most 0.012.
Values may be sent and summed in bfloat16 or wider, within the bound.
No kernel may reach another device: no remote copies, remote signals or barrier semaphores. Data moves between devices by JAX's collectives and lax.ppermute only.
A program may use at most 64 MiB of HBM per device.

v0:
```python
import jax
import jax.numpy as jnp
from jax import lax
from jax.sharding import PartitionSpec as P

HEAD_DIM = 64


epsilon = 1e-06


def copy_for_each(array, axis):
    copies = jnp.broadcast_to(array, (lax.axis_size(axis), *array.shape))
    return lax.all_to_all(copies, axis, split_axis=0, concat_axis=0, tiled=True)


def of_everyone(array, axis):
    return copy_for_each(array, axis).astype(jnp.float32).sum(axis=0)


def split_up(array, dim, length):
    before, after = (array.shape[:dim], array.shape[dim + 1 :])
    return jnp.moveaxis(array.reshape(*before, length, -1, *after), dim, 0)


def sent_and_summed(array, axis, dim):
    parts = split_up(array, dim, lax.axis_size(axis))
    arrived = lax.all_to_all(parts, axis, split_axis=0, concat_axis=0, tiled=True)
    return arrived.astype(jnp.float32).sum(axis=0)


def side_by_side(arrays, axis, dim, along):
    ends, at = ([], 0)
    for a in arrays[:-1]:
        at += a.shape[along]
        ends.append(at)
    both = jnp.concatenate(arrays, axis=along)
    return tuple(jnp.split(sent_and_summed(both, axis, dim), ends, axis=along))


def rms_scale(rows_in, gain_row):
    values_f = rows_in.astype(jnp.float32)
    return (
        values_f
        * lax.rsqrt(jnp.mean(values_f * values_f, axis=-1, keepdims=True) + epsilon)
        * gain_row
    )


def later_sum(values):
    lead = values.shape[:-1]
    length = values.shape[-1]
    width = 128
    count = length // width
    blocked = values.reshape(lead + (count, width))
    inner_rows = lax.broadcasted_iota(jnp.int32, (width, width), 0)
    inner_cols = lax.broadcasted_iota(jnp.int32, (width, width), 1)
    inner_table = (inner_rows > inner_cols).astype(jnp.float32)
    within = jnp.einsum("...bj,js->...bs", blocked, inner_table, precision=lax.Precision.HIGHEST)
    totals = jnp.sum(blocked, axis=-1)
    outer_rows = lax.broadcasted_iota(jnp.int32, (count, count), 0)
    outer_cols = lax.broadcasted_iota(jnp.int32, (count, count), 1)
    outer_table = (outer_rows > outer_cols).astype(jnp.float32)
    beyond = jnp.einsum("...j,ji->...i", totals, outer_table, precision=lax.Precision.HIGHEST)
    return (within + beyond[..., None]).reshape(lead + (length,))


def shards(
    tokens,
    lengths,
    cache,
    attn_gain,
    query_weight,
    key_weight,
    value_weight,
    stick_bias,
    out_weight,
    ffn_gain,
    routes,
    route_weights,
    expert_gate,
    expert_up,
    expert_down,
    shared_gate,
    shared_up,
    shared_down,
    gate_vector,
):
    ranks_tp = lax.axis_size("tp")
    ranks_ep = lax.axis_size("ep")
    row_count = tokens.shape[0]
    model_width = tokens.shape[1]
    quarter = model_width // ranks_tp
    part_index = lax.axis_index("tp")
    normed = rms_scale(tokens, attn_gain).astype(jnp.bfloat16)
    queries = jnp.dot(normed, query_weight, preferred_element_type=jnp.float32).astype(jnp.bfloat16)
    key_rows = jnp.dot(normed, key_weight, preferred_element_type=jnp.float32).astype(jnp.bfloat16)
    value_rows = jnp.dot(normed, value_weight, preferred_element_type=jnp.float32).astype(
        jnp.bfloat16
    )
    local_heads = key_weight.shape[1] // HEAD_DIM
    new_kv = jnp.stack(
        [
            key_rows.reshape(row_count, local_heads, HEAD_DIM),
            value_rows.reshape(row_count, local_heads, HEAD_DIM),
        ],
        axis=2,
    )
    new_kv = new_kv.reshape(row_count, local_heads * 2 * HEAD_DIM)
    group_size = queries.shape[1] // HEAD_DIM // local_heads
    grouped = queries.reshape(row_count, local_heads, group_size, HEAD_DIM)
    cache_len = cache.shape[1]
    cache_view = cache.reshape(row_count, cache_len, local_heads, 2, HEAD_DIM)
    scores = jnp.einsum(
        "nkgd,nckd->nkgc", grouped, cache_view[:, :, :, 0, :], preferred_element_type=jnp.float32
    ) * HEAD_DIM ** (-0.5)
    scores = scores + stick_bias.reshape(1, local_heads, group_size, 1)
    positions = lax.broadcasted_iota(jnp.int32, (1, 1, 1, cache_len), 3)
    usable = positions < lengths.reshape(row_count, 1, 1, 1)
    log_keep = jnp.where(usable, jax.nn.log_sigmoid(-scores), 0.0)
    behind = later_sum(log_keep)
    stick_weights = jnp.where(usable, jnp.exp(jax.nn.log_sigmoid(scores) + behind), 0.0).astype(
        jnp.bfloat16
    )
    heads_out = jnp.einsum(
        "nkgc,nckd->nkgd",
        stick_weights,
        cache_view[:, :, :, 1, :],
        preferred_element_type=jnp.float32,
    ).astype(jnp.bfloat16)
    attn_term = jnp.dot(
        heads_out.reshape(row_count, -1), out_weight, preferred_element_type=jnp.float32
    )
    attn_total = of_everyone(attn_term.astype(jnp.bfloat16), "tp").astype(jnp.float32)
    residual_full = tokens.astype(jnp.float32) + attn_total
    normed_mix = rms_scale(residual_full, ffn_gain).astype(jnp.bfloat16)
    residual = lax.dynamic_slice_in_dim(residual_full, part_index * quarter, quarter, 1)
    route_count = routes.shape[1]
    local_experts = expert_gate.shape[0]
    experts_all = ranks_ep * local_experts
    capacity = min(row_count, max(2, 2 * row_count * route_count // experts_all))
    slot_total = experts_all * capacity
    flat_routes = routes.reshape(-1)
    flat_count = flat_routes.shape[0]
    expert_hits = (
        flat_routes[:, None] == lax.broadcasted_iota(jnp.int32, (1, experts_all), 1)
    ).astype(jnp.float32)
    lower_table = (
        lax.broadcasted_iota(jnp.int32, (flat_count, flat_count), 0)
        > lax.broadcasted_iota(jnp.int32, (flat_count, flat_count), 1)
    ).astype(jnp.float32)
    earlier = jnp.dot(lower_table, expert_hits, precision=lax.Precision.HIGHEST)
    slot_rank = jnp.sum(earlier * expert_hits, axis=1).astype(jnp.int32)
    slot_index = flat_routes * capacity + slot_rank
    owned_slots = slot_index[:, None] == lax.broadcasted_iota(jnp.int32, (1, slot_total), 1)
    owned_slots = owned_slots.reshape(row_count, route_count, slot_total)
    take_matrix = jnp.any(owned_slots, axis=1).astype(jnp.bfloat16)
    mix_weights = jnp.sum(owned_slots.astype(jnp.float32) * route_weights[:, :, None], axis=1)
    pick_dims = (((0,), (0,)), ((), ()))
    sent_rows = lax.dot_general(
        take_matrix, normed_mix, pick_dims, preferred_element_type=jnp.float32
    ).astype(jnp.bfloat16)
    arrived = lax.all_to_all(sent_rows, "ep", split_axis=0, concat_axis=0, tiled=True)
    expert_grid = arrived.reshape(ranks_ep, local_experts, capacity, model_width)
    gate_val = jnp.einsum(
        "sjcd,jdf->sjcf", expert_grid, expert_gate, preferred_element_type=jnp.float32
    )
    up_val = jnp.einsum(
        "sjcd,jdf->sjcf", expert_grid, expert_up, preferred_element_type=jnp.float32
    )
    expert_hidden = (jax.nn.silu(gate_val) * up_val).astype(jnp.bfloat16)
    expert_term = jnp.einsum(
        "sjcf,jfd->sjcd", expert_hidden, expert_down, preferred_element_type=jnp.float32
    )
    expert_term = expert_term.reshape(-1, model_width)
    shared_width = shared_gate.shape[1]
    column_rows = lax.all_to_all(normed_mix, "ep", split_axis=1, concat_axis=0, tiled=True)
    joined_weights = jnp.concatenate([shared_gate, shared_up], axis=1)
    dense_total = sent_and_summed(
        jnp.dot(column_rows, joined_weights, preferred_element_type=jnp.float32).astype(
            jnp.bfloat16
        ),
        "ep",
        0,
    )
    gate_sum = dense_total[:, :shared_width]
    up_sum = dense_total[:, shared_width:]
    shared_hidden = (jax.nn.silu(gate_sum) * up_sum).astype(jnp.bfloat16)
    shared_term = jnp.dot(shared_hidden, shared_down, preferred_element_type=jnp.float32)
    expert_share, shared_share = side_by_side(
        (expert_term.astype(jnp.bfloat16), shared_term.astype(jnp.bfloat16)), "tp", 1, 0
    )
    expert_out = expert_share.astype(jnp.bfloat16).reshape(
        ranks_ep, local_experts * capacity, quarter
    )
    returned = lax.all_to_all(expert_out, "ep", split_axis=0, concat_axis=0, tiled=True).reshape(
        slot_total, quarter
    )
    routed = jnp.dot(mix_weights, returned.astype(jnp.float32), precision=lax.Precision.HIGHEST)
    mix_gate = jax.nn.sigmoid(jnp.dot(normed_mix, gate_vector, preferred_element_type=jnp.float32))
    layer_out = (residual + routed + mix_gate[:, None] * shared_share).astype(jnp.bfloat16)
    return (layer_out, new_kv)


def solution(mesh):
    placed = (
        P("ep", None),
        P("ep"),
        P("ep", None, "tp"),
        P(),
        P(None, "tp"),
        P(None, "tp"),
        P(None, "tp"),
        P("tp"),
        P("tp", None),
        P(),
        P("ep", None),
        P("ep", None),
        P("ep", None, "tp"),
        P("ep", None, "tp"),
        P("ep", "tp", None),
        P("ep", "tp"),
        P("ep", "tp"),
        P("tp", None),
        P(),
    )
    return jax.shard_map(
        shards,
        mesh=mesh,
        in_specs=placed,
        out_specs=(P("ep", "tp"), P("ep", "tp")),
        check_vma=False,
    )
```

profile of v0, /device:TPU:1, one launch (start us, length us, event | category | flops | bytes accessed | tf_op | source)
XLA Modules:
  0.0 153.7 jit_solution(14038592422454993125)
XLA Ops:
  0.6 1.1 fusion.39
  1.7 1.6 %convolution_convert_fusion.5 = bf16[16,256]{1,0:T(8,128)(2,1)S(1)} fusion(bf16[2048,256]{1,0:T(8,128)(2,1)} %param.23, bf16[16,2048]{1,0:T(8,128)(2,1)} %param.19, f32[2048]{0:T(1024)} %param.22, f32[16]{0:T(128)S(1)} %add_rsqrt_fusion.1), kind=kOutput, calls=%fused_computation.25 | convolution fusion | flops 16912384 | bytes 1130560 | tf_op jit(solution)/shard_map/dot_general | solution.py:96
  3.4 6.4 %copy.65 = bf16[16,1024,128]{1,2,0:T(8,128)(2,1)} copy(bf16[16,1024,128]{2,1,0:T(8,128)(2,1)} %param.21) | data formatting | bytes 8388608 | tf_op args[2]
  9.9 2.2 %fusion.32 = (f32[16,4,1024]{2,1,0:T(4,128)S(1)}, f32[16,4,1024]{2,1,0:T(4,128)S(1)}) fusion(pred[16,1024]{1,0:T(8,128)(4,1)S(1)} %iota_compare_fusion.2, f32[4]{0:T(128)S(1)} %copy-done.17, bf16[16,4,64]{2,1,0:T(4,128)(2,1)S(1)} %reshape.190, bf16[16,1024,1,2,64]{1,4,3,0,2:T(8,128)(2,1)} %bitcast.121), kind=kOutput, calls=%fused_computation.53 | convolution fusion | flops 9043968 | bytes 2646032 | tf_op jit(solution)/shard_map/nkgd,nckd->nkgc/dot_general | solution.py:114
  13.1 2.4 %fusion.10 = bf16[16,4,64]{2,1,0:T(4,128)(2,1)S(1)} fusion(bf16[16,1024,1,2,64]{1,4,3,0,2:T(8,128)(2,1)} %bitcast.122, f32[16,4,1024]{2,1,0:T(4,128)S(1)} %reshape.194, f32[16,4,1024]{2,1,0:T(4,128)S(1)} %get-tuple-element.5, pred[16,1024]{1,0:T(8,128)(4,1)S(1)} %iota_compare_fusion.2), kind=kOutput, calls=%fused_computation.23 | convolution fusion | flops 9113600 | bytes 2646016 | tf_op jit(solution)/shard_map/nkgc,nckd->nkgd/dot_general | solution.py:125
  15.8 10.2 %all_to_all.48 = bf16[4,16,2048]{2,1,0:T(8,128)(2,1)S(1)} all-to-all(bf16[4,16,2048]{2,1,0:T(8,128)(2,1)S(1)} %broadcast_in_dim.26), channel_id=1, replica_groups=mesh['ep'=64,'tp'=4] {'tp'}, dimensions={0} | all-to-all | bytes 524288 | tf_op jit(solution)/shard_map/all_to_all | solution.py:14
  26.9 23.6 %all_to_all.49 = bf16[64,2,256]{2,1,0:T(2,128)(2,1)S(1)} all-to-all(bf16[64,2,256]{2,1,0:T(2,128)(2,1)S(1)} %reshape.213), channel_id=1, replica_groups=mesh['ep'=64,'tp'=4] {'ep'}, dimensions={0} | all-to-all | bytes 131072 | tf_op jit(solution)/shard_map/all_to_all | solution.py:177
  50.7 1.1 convolution_convert_fusion.4
  51.8 4.5 %all-to-all-start.3 = ((bf16[64,16,256]{2,1,0:T(8,128)(2,1)}), bf16[64,16,256]{2,1,0:T(8,128)(2,1)S(1)}, u32[]{:S(2)}, u32[]{:S(2)}) async-start(bf16[64,16,256]{2,1,0:T(8,128)(2,1)} %bitcast.26), calls=%async_computation.3 | async-start | bytes 1048576 | tf_op jit(solution)/shard_map/all_to_all | solution.py:28
  57.3 1.3 all_to_all.33
  58.6 15.4 %all-to-all-done.3 = bf16[64,16,256]{2,1,0:T(8,128)(2,1)S(1)} async-done(((bf16[64,16,256]{2,1,0:T(8,128)(2,1)}), bf16[64,16,256]{2,1,0:T(8,128)(2,1)S(1)}, u32[]{:S(2)}, u32[]{:S(2)}) %all-to-all-start.3) | async-done | bytes 524320 | tf_op jit(solution)/shard_map/all_to_all | solution.py:28
  74.1 5.7 %all-to-all-start.1 = ((bf16[64,3,2048]{2,1,0:T(4,128)(2,1)}), bf16[64,3,2048]{2,1,0:T(4,128)(2,1)S(1)}, u32[]{:S(2)}, u32[]{:S(2)}) async-start(bf16[64,3,2048]{2,1,0:T(4,128)(2,1)} %all_to_all.33), calls=%async_computation.1 | async-start | bytes 2097152 | tf_op jit(solution)/shard_map/all_to_all | solution.py:163
  79.9 0.8 convolution_convert_fusion.2
  80.7 27.2 %all-to-all-done.1 = bf16[64,3,2048]{2,1,0:T(4,128)(2,1)S(1)} async-done(((bf16[64,3,2048]{2,1,0:T(4,128)(2,1)}), bf16[64,3,2048]{2,1,0:T(4,128)(2,1)S(1)}, u32[]{:S(2)}, u32[]{:S(2)}) %all-to-all-start.1) | async-done | bytes 786464 | tf_op jit(solution)/shard_map/all_to_all | solution.py:163
  107.9 2.2 %convolution_bitcast_fusion.1 = f32[64,1,3,256]{3,0,2,1:T(8,128)S(1)} fusion(bf16[1,2048,256]{2,1,0:T(8,128)(2,1)} %param.31, bf16[64,3,2048]{2,1,0:T(4,128)(2,1)S(1)} %all-to-all-done.1), kind=kOutput, calls=%fused_computation.16 | convolution fusion | flops 201326592 | bytes 2031616 | tf_op jit(solution)/shard_map/sjcd,jdf->sjcf/dot_general | solution.py:165
  110.2 2.4 %fusion = bf16[64,1,3,2048]{3,0,2,1:T(8,128)(2,1)S(1)} fusion(bf16[1,256,2048]{2,1,0:T(8,128)(2,1)S(1)} %copy-done, bf16[1,2048,256]{2,1,0:T(8,128)(2,1)} %param.32, bf16[64,3,2048]{2,1,0:T(4,128)(2,1)S(1)} %all-to-all-done.1, f32[64,1,3,256]{3,0,2,1:T(8,128)S(1)} %convolution_bitcast_fusion.1), kind=kOutput, calls=%fused_computation.2 | convolution fusion | flops 403341312 | bytes 3866624 | tf_op jit(solution)/shard_map/sjcf,jfd->sjcd/dot_general | solution.py:172
  114.0 0.9 pad_maximum_fusion
  114.9 1.0 copy.91
  115.9 3.5 %all-to-all-start.4 = ((bf16[4,208,512]{2,1,0:T(8,128)(2,1)}), bf16[4,208,512]{2,1,0:T(8,128)(2,1)S(1)}, u32[]{:S(2)}, u32[]{:S(2)}) async-start(bf16[4,208,512]{2,1,0:T(8,128)(2,1)} %bitcast.119), calls=%async_computation.4 | async-start | bytes 1703936 | tf_op jit(solution)/shard_map/all_to_all | solution.py:28
  119.9 11.4 %all-to-all-done.4 = bf16[4,208,512]{2,1,0:T(8,128)(2,1)S(1)} async-done(((bf16[4,208,512]{2,1,0:T(8,128)(2,1)}), bf16[4,208,512]{2,1,0:T(8,128)(2,1)S(1)}, u32[]{:S(2)}, u32[]{:S(2)}) %all-to-all-start.4) | async-done | bytes 852000 | tf_op jit(solution)/shard_map/all_to_all | solution.py:28
  131.5 0.8 reshape.203
  132.3 7.4 %all-to-all-start.5 = ((bf16[64,3,512]{2,1,0:T(4,128)(2,1)}), bf16[64,3,512]{2,1,0:T(4,128)(2,1)S(1)}, u32[]{:S(2)}, u32[]{:S(2)}) async-start(bf16[64,3,512]{2,1,0:T(4,128)(2,1)} %reshape.203), calls=%async_computation.5 | async-start | bytes 524288 | tf_op jit(solution)/shard_map/all_to_all | solution.py:196
  140.6 12.1 %all-to-all-done.5 = bf16[64,3,512]{2,1,0:T(4,128)(2,1)S(1)} async-done(((bf16[64,3,512]{2,1,0:T(4,128)(2,1)}), bf16[64,3,512]{2,1,0:T(4,128)(2,1)S(1)}, u32[]{:S(2)}, u32[]{:S(2)}) %all-to-all-start.5) | async-done | bytes 196640 | tf_op jit(solution)/shard_map/all_to_all | solution.py:196
  152.9 0.8 fusion.9
  (79 shorter events, 6.8 us)
Async XLA Ops:
  0.6 109.5 %copy-start = (bf16[1,256,2048]{2,1,0:T(8,128)(2,1)S(1)}, bf16[1,256,2048]{2,1,0:T(8,128)(2,1)}, u32[]{:S(2)}) copy-start(bf16[1,256,2048]{2,1,0:T(8,128)(2,1)} %param.33) | copy-start | bytes 3145732
  3.4 6.4 %copy-start.14 = (s32[16]{0:T(128)S(1)}, s32[16]{0:T(128)}, u32[]{:S(2)}) copy-start(s32[16]{0:T(128)} %param.20) | copy-start | bytes 196
  3.4 6.5 %copy-start.17 = (f32[4]{0:T(128)S(1)}, f32[4]{0:T(128)}, u32[]{:S(2)}) copy-start(f32[4]{0:T(128)} %param.26) | copy-start | bytes 52
  13.1 2.5 %copy-start.1 = (bf16[256,2048]{1,0:T(8,128)(2,1)S(1)}, bf16[256,2048]{1,0:T(8,128)(2,1)}, u32[]{:S(2)}) copy-start(bf16[256,2048]{1,0:T(8,128)(2,1)} %param.27) | copy-start | bytes 3145732
  15.4 10.6 %copy-start.2 = (bf16[16,2048]{1,0:T(8,128)(2,1)S(1)}, bf16[16,2048]{1,0:T(8,128)(2,1)}, u32[]{:S(2)}) copy-start(bf16[16,2048]{1,0:T(8,128)(2,1)} %param.19) | copy-start | bytes 196612
  15.4 10.8 %copy-start.11 = (f32[2048]{0:T(1024)S(1)}, f32[2048]{0:T(1024)}, u32[]{:S(2)}) copy-start(f32[2048]{0:T(1024)} %param.28) | copy-start | bytes 24580
  15.5 35.2 %copy-start.8 = (bf16[32,128]{1,0:T(8,128)(2,1)S(1)}, bf16[32,128]{1,0:T(8,128)(2,1)}, u32[]{:S(2)}) copy-start(bf16[32,128]{1,0:T(8,128)(2,1)} %param.35) | copy-start | bytes 24580
  15.5 35.2 %copy-start.9 = (bf16[32,128]{1,0:T(8,128)(2,1)S(1)}, bf16[32,128]{1,0:T(8,128)(2,1)}, u32[]{:S(2)}) copy-start(bf16[32,128]{1,0:T(8,128)(2,1)} %param.34) | copy-start | bytes 24580
  26.1 30.2 %copy-start.7 = (s32[16,6]{0,1:T(8,128)S(1)}, s32[16,6]{0,1:T(8,128)}, u32[]{:S(2)}) copy-start(s32[16,6]{0,1:T(8,128)} %param.29) | copy-start | bytes 1156
  26.3 31.0 %copy-start.4 = (bf16[16,2048]{1,0:T(8,128)(2,1)}, bf16[16,2048]{1,0:T(8,128)(2,1)S(1)}, u32[]{:S(2)}) copy-start(bf16[16,2048]{1,0:T(8,128)(2,1)S(1)} %multiply_convert_fusion) | copy-start | bytes 196612
  51.8 22.3 %all-to-all-start.3 = ((bf16[64,16,256]{2,1,0:T(8,128)(2,1)}), bf16[64,16,256]{2,1,0:T(8,128)(2,1)S(1)}, u32[]{:S(2)}, u32[]{:S(2)}) async-start(bf16[64,16,256]{2,1,0:T(8,128)(2,1)} %bitcast.26), calls=%async_computation.3 | async-start | bytes 1048576 | tf_op jit(solution)/shard_map/all_to_all | solution.py:28
  57.3 22.5 %copy-start.6 = (bf16[128,2048]{1,0:T(8,128)(2,1)S(1)}, bf16[128,2048]{1,0:T(8,128)(2,1)}, u32[]{:S(2)}) copy-start(bf16[128,2048]{1,0:T(8,128)(2,1)} %param.36) | copy-start | bytes 1572868
  74.1 33.9 %all-to-all-start.1 = ((bf16[64,3,2048]{2,1,0:T(4,128)(2,1)}), bf16[64,3,2048]{2,1,0:T(4,128)(2,1)S(1)}, u32[]{:S(2)}, u32[]{:S(2)}) async-start(bf16[64,3,2048]{2,1,0:T(4,128)(2,1)} %all_to_all.33), calls=%async_computation.1 | async-start | bytes 2097152 | tf_op jit(solution)/shard_map/all_to_all | solution.py:163
  114.9 4.5 %copy-start.3 = (bf16[16,2048]{1,0:T(8,128)(2,1)S(1)}, bf16[16,2048]{1,0:T(8,128)(2,1)}, u32[]{:S(2)}) copy-start(bf16[16,2048]{1,0:T(8,128)(2,1)} %param.19) | copy-start | bytes 196612
  114.9 4.5 %copy-start.10 = (f32[2048]{0:T(1024)S(1)}, f32[2048]{0:T(1024)}, u32[]{:S(2)}) copy-start(f32[2048]{0:T(1024)} %param.22) | copy-start | bytes 24580
  114.9 4.5 %copy-start.15 = (bf16[2048,64]{0,1:T(8,128)(2,1)S(1)}, bf16[2048,64]{0,1:T(8,128)(2,1)}, u32[]{:S(2)}) copy-start(bf16[2048,64]{0,1:T(8,128)(2,1)} %param.24) | copy-start | bytes 786436
  114.9 4.8 %copy-start.16 = (bf16[2048,64]{0,1:T(8,128)(2,1)S(1)}, bf16[2048,64]{0,1:T(8,128)(2,1)}, u32[]{:S(2)}) copy-start(bf16[2048,64]{0,1:T(8,128)(2,1)} %param.25) | copy-start | bytes 786436
  115.9 15.4 %all-to-all-start.4 = ((bf16[4,208,512]{2,1,0:T(8,128)(2,1)}), bf16[4,208,512]{2,1,0:T(8,128)(2,1)S(1)}, u32[]{:S(2)}, u32[]{:S(2)}) async-start(bf16[4,208,512]{2,1,0:T(8,128)(2,1)} %bitcast.119), calls=%async_computation.4 | async-start | bytes 1703936 | tf_op jit(solution)/shard_map/all_to_all | solution.py:28
  119.4 20.2 %copy-start.12 = (bf16[2048]{0:T(1024)(128)(2,1)S(1)}, bf16[2048]{0:T(1024)(128)(2,1)}, u32[]{:S(2)}) copy-start(bf16[2048]{0:T(1024)(128)(2,1)} %param.37) | copy-start | bytes 12292
  119.4 20.9 %copy-start.13 = (f32[16,6]{0,1:T(8,128)S(1)}, f32[16,6]{0,1:T(8,128)}, u32[]{:S(2)}) copy-start(f32[16,6]{0,1:T(8,128)} %param.30) | copy-start | bytes 1156
  119.5 21.0 %copy-start.5 = (bf16[16,2048]{1,0:T(8,128)(2,1)S(1)}, bf16[16,2048]{1,0:T(8,128)(2,1)}, u32[]{:S(2)}) copy-start(bf16[16,2048]{1,0:T(8,128)(2,1)} %copy-done.4) | copy-start | bytes 196612
  132.3 20.5 %all-to-all-start.5 = ((bf16[64,3,512]{2,1,0:T(4,128)(2,1)}), bf16[64,3,512]{2,1,0:T(4,128)(2,1)S(1)}, u32[]{:S(2)}, u32[]{:S(2)}) async-start(bf16[64,3,512]{2,1,0:T(4,128)(2,1)} %reshape.203), calls=%async_computation.5 | async-start | bytes 524288 | tf_op jit(solution)/shard_map/all_to_all | solution.py:196
where the time goes:
time: 155 us; the launch traced here: 154 us
  waiting for transfers between devices  66.1 us (43%)
  blocking collectives  33.8 us (22%)
  starting transfers between devices  21 us (14%)
  matrix products  15.4 us (10%)
  local copies, waits for them, and re-layouts  13.4 us (9%)
  other arithmetic  2.89 us (2%)
    all_to_all x1, waiting for transfers between devices, shards(): lax.all_to_all(sent_rows, 'ep', split_axis=0, concat_axis=0, tiled=True)  27.2 us
    all_to_all x2, waiting for transfers between devices, sent_and_summed(): lax.all_to_all(parts, axis, split_axis=0, concat_axis=0, tiled=True)  26.8 us
    all_to_all x1, blocking collectives, shards(): lax.all_to_all(normed_mix, 'ep', split_axis=1, concat_axis=0, tiled=True)  23.6 us
    all_to_all x1, waiting for transfers between devices, shards(): lax.all_to_all(expert_out, 'ep', split_axis=0, concat_axis=0, tiled=True)  12.1 us
    all_to_all x1, blocking collectives, copy_for_each(): return lax.all_to_all(copies, axis, split_axis=0, concat_axis=0, tiled=True)  10.2 us
    all_to_all x2, starting transfers between devices, sent_and_summed(): lax.all_to_all(parts, axis, split_axis=0, concat_axis=0, tiled=True)  7.96 us
    all_to_all x1, starting transfers between devices, shards(): lax.all_to_all(expert_out, 'ep', split_axis=0, concat_axis=0, tiled=True)  7.39 us
    unnamed x41, local copies, waits for them, and re-layouts  6.95 us
  transfers between devices with their start and end apart: 4, of which 4 were waited for; matrix products, arithmetic and copies ran while one was open for 2% of the time, Pallas kernels for 0%

commit v1 on v0

v1 whole, which is shorter than its diff:
```python
import jax
import jax.numpy as jnp
from jax import lax
from jax.experimental import pallas as pl
from jax.experimental.pallas import tpu as pltpu
from jax.sharding import PartitionSpec as P

HEAD_DIM = 64
EPS = 1e-06
CAP = 3
bf16 = jnp.bfloat16
f32 = jnp.float32

VM = pl.BlockSpec(memory_space=pltpu.VMEM)
SM = pl.BlockSpec(memory_space=pltpu.SMEM)
HBM = pl.BlockSpec(memory_space=pltpu.HBM)


def iota(shape, dim):
    return lax.broadcasted_iota(jnp.int32, shape, dim)


def dot(a, b, dims=((1,), (0,))):
    return lax.dot_general(a, b, (dims, ((), ())), preferred_element_type=f32)


def three_pieces(values):
    high = values.astype(bf16)
    rest = values - high.astype(f32)
    middle = rest.astype(bf16)
    low = (rest - middle.astype(f32)).astype(bf16)
    return high, middle, low


def call(kernel, outs, ins, in_specs=None, scratch=(), limit_mib=8):
    return pl.pallas_call(
        kernel,
        out_shape=tuple(jax.ShapeDtypeStruct(s, t) for s, t in outs),
        in_specs=in_specs or [VM] * len(ins),
        out_specs=tuple([VM] * len(outs)),
        scratch_shapes=list(scratch),
        compiler_params=pltpu.CompilerParams(vmem_limit_bytes=limit_mib * 1024 * 1024),
    )(*ins)


def attend_kernel(len_hbm, bias_hbm, tok_hbm, gain_hbm, cache_hbm, wq_hbm, wo_hbm,
                  part_ref, normed_ref,
                  len_ref, bias_ref, tok_ref, gain_ref, cache_v, wq_v, wo_v, s_v, sem_c, sem_w):
    rows = tok_ref.shape[0]
    span = cache_v.shape[1]
    heads = 4
    hr = rows * heads
    small = []
    for i, (src, dst) in enumerate(
        [(tok_hbm, tok_ref), (gain_hbm, gain_ref), (wq_hbm, wq_v), (wo_hbm, wo_v),
         (len_hbm, len_ref), (bias_hbm, bias_ref)]
    ):
        small.append(pltpu.make_async_copy(src, dst, sem_w.at[i]))
    tok_c, gain_c, wq_c, wo_c, len_c, bias_c = small
    tok_c.start()
    gain_c.start()
    wq_c.start()
    cache_c = []
    for n in range(rows):
        c = pltpu.make_async_copy(cache_hbm.at[n], cache_v.at[n], sem_c.at[n])
        c.start()
        cache_c.append(c)
    len_c.start()
    bias_c.start()
    wo_c.start()
    tok_c.wait()
    gain_c.wait()
    x = tok_ref[...].astype(f32)
    ms = jnp.mean(x * x, axis=-1, keepdims=True)
    normed = (x * lax.rsqrt(ms + EPS) * gain_ref[...]).astype(bf16)
    normed_ref[...] = normed
    expand = (iota((hr, rows), 0) // heads == iota((hr, rows), 1)).astype(bf16)
    lane = iota((hr, heads * HEAD_DIM), 1)
    row = iota((hr, heads * HEAD_DIM), 0)
    fold = ((iota((256, 128), 0) % HEAD_DIM) == iota((256, 128), 1)).astype(bf16)
    wq_c.wait()
    q = dot(normed, wq_v[...]).astype(bf16)
    qx = jnp.where(lane // HEAD_DIM == row % heads, dot(expand, q), 0.0).astype(bf16)
    qk = (dot(qx, fold) * (HEAD_DIM**-0.5)).astype(bf16)
    r16 = iota((16, span), 0) // heads
    for g in range(rows // 4):
        qg = qk[16 * g : 16 * g + 16, :]
        acc = None
        for i in range(4):
            n = 4 * g + i
            cache_c[n].wait()
            s = dot(qg, cache_v[n], ((1,), (1,)))
            acc = s if acc is None else jnp.where(r16 == i, s, acc)
        s_v[16 * g : 16 * g + 16, :] = acc
    rid = iota((hr, 128), 0)
    lens = jnp.zeros((hr, 128), jnp.int32)
    bias = jnp.zeros((hr, 128), f32)
    len_c.wait()
    bias_c.wait()
    for n in range(rows):
        lens = jnp.where(rid // heads == n, len_ref[n], lens)
    for h in range(heads):
        bias = jnp.where(rid % heads == h, bias_ref[h], bias)
    later = ((iota((128, 256), 0) > iota((128, 256), 1)) | (iota((128, 256), 1) >= 128)).astype(bf16)
    blocks = span // 128
    beyond = jnp.zeros((hr, 128), f32)
    weights = [None] * blocks
    for b in range(blocks - 1, -1, -1):
        z = s_v[:, b * 128 : (b + 1) * 128] + bias
        usable = (iota((hr, 128), 1) + b * 128) < lens
        soft = jnp.log1p(jnp.exp(-jnp.abs(z)))
        log_keep = jnp.where(usable, -(jnp.maximum(z, 0.0) + soft), 0.0)
        high, middle, low = three_pieces(log_keep)
        both = (dot(low, later) + dot(middle, later)) + dot(high, later)
        behind = both[:, :128] + beyond
        beyond = beyond + both[:, 128:]
        weights[b] = jnp.where(usable, jnp.exp(jnp.minimum(z, 0.0) - soft + behind), 0.0).astype(bf16)
    outs = []
    r16o = iota((16, 128), 0) // heads
    for g in range(rows // 4):
        pg = jnp.concatenate([w[16 * g : 16 * g + 16, :] for w in weights], axis=1)
        acc = None
        for i in range(4):
            o = dot(pg, cache_v[4 * g + i])
            acc = o if acc is None else jnp.where(r16o == i, o, acc)
        outs.append(acc)
    o = jnp.concatenate(outs, axis=0).astype(bf16)
    unfold = ((iota((128, 256), 0) - HEAD_DIM) == (iota((128, 256), 1) % HEAD_DIM)).astype(bf16)
    ox = jnp.where(lane // HEAD_DIM == row % heads, dot(o, unfold), 0.0).astype(bf16)
    collect = (iota((rows, hr), 1) // heads == iota((rows, hr), 0)).astype(bf16)
    heads_out = dot(collect, ox).astype(bf16)
    wo_c.wait()
    part_ref[...] = dot(heads_out, wo_v[...]).astype(bf16)


def attend(tokens, lengths, cache, gain, wq, bias, wo):
    rows, d = tokens.shape
    return call(
        attend_kernel, [((rows, d), bf16), ((rows, d), bf16)],
        (lengths, bias, tokens, gain.reshape(1, -1), cache, wq, wo),
        in_specs=[HBM] * 7,
        scratch=[
            pltpu.SMEM(lengths.shape, jnp.int32), pltpu.SMEM(bias.shape, f32),
            pltpu.VMEM(tokens.shape, bf16), pltpu.VMEM((1, d), f32),
            pltpu.VMEM(cache.shape, bf16), pltpu.VMEM(wq.shape, bf16), pltpu.VMEM(wo.shape, bf16),
            pltpu.VMEM((4 * rows, cache.shape[1]), f32),
            pltpu.SemaphoreType.DMA((rows,)), pltpu.SemaphoreType.DMA((6,)),
        ],
        limit_mib=16,
    )


def route_kernel(routes_ref, rw_ref, pick_ref, mix_ref):
    top, rows = routes_ref.shape
    experts = mix_ref.shape[1] // 8
    hits = jnp.zeros((experts, rows), f32)
    weight = jnp.zeros((experts, rows), f32)
    which = iota((experts, rows), 0)
    for j in range(top):
        same = which == routes_ref[j : j + 1, :]
        hits = jnp.where(same, 1.0, hits)
        weight = jnp.where(same, rw_ref[j : j + 1, :], weight)
    before = (iota((rows, rows), 0) < iota((rows, rows), 1)).astype(bf16)
    rank = dot(hits.astype(bf16), before)
    tile = (iota((rows, 8 * rows), 0) == iota((rows, 8 * rows), 1) % rows).astype(bf16)
    spread = (iota((8 * experts, experts), 0) // 8 == iota((8 * experts, experts), 1)).astype(bf16)
    here = (iota((8 * experts, 8 * rows), 0) % 8) == (iota((8 * experts, 8 * rows), 1) // rows)
    lane = iota((rows, 8 * experts), 1) % 8
    mixed = [jnp.zeros((rows, 8 * experts), f32) for _ in range(3)]
    for k in range(CAP):
        mine = jnp.where((hits > 0.5) & (rank == k), 1.0, 0.0)
        wide = dot(mine.astype(bf16), tile).astype(bf16)
        full = jnp.where(here, dot(spread, wide), 0.0)
        pick_ref[:, k * 8 * rows : (k + 1) * 8 * rows] = full.astype(bf16)
        for i, piece in enumerate(three_pieces(mine * weight)):
            part = dot(piece, spread, ((0,), (1,)))
            mixed[i] = jnp.where(lane // 2 == k, part, mixed[i])
    for h in range(2):
        for i in range(3):
            at = (h * 3 + i) * rows
            mix_ref[at : at + rows, :] = jnp.where(lane % 2 == h, mixed[i], 0.0).astype(bf16)


def mix_kernel(tok_ref, p0, p1, p2, p3, gain_ref, pick_ref, normed_ref, residual_ref, sent_ref):
    rows, d = tok_ref.shape
    wide = d // 8
    total = (p0[...].astype(f32) + p1[...].astype(f32)) + (p2[...].astype(f32) + p3[...].astype(f32))
    residual = tok_ref[...].astype(f32) + total
    residual_ref[...] = residual
    ms = jnp.mean(residual * residual, axis=-1, keepdims=True)
    normed = (residual * lax.rsqrt(ms + EPS) * gain_ref[...]).astype(bf16)
    normed_ref[...] = normed
    stacked = jnp.concatenate([normed[:, r * wide : (r + 1) * wide] for r in range(8)], axis=0)
    for k in range(CAP):
        pick = pick_ref[:, k * 8 * rows : (k + 1) * 8 * rows]
        sent_ref[:, k * wide : (k + 1) * wide] = dot(pick, stacked).astype(bf16)


def silu(v):
    return v / (1.0 + jnp.exp(-v))


def shared_kernel(ep_ref, normed_ref, gv_ref, b0, b1, b2, b3, b4, b5, b6, b7, hidden_ref, gate_ref):
    blocks = (b0, b1, b2, b3, b4, b5, b6, b7)
    rows, d = normed_ref.shape
    wide = d // 8
    ep = ep_ref[0]
    z = ep // 8
    y = (ep // 2) % 4
    c = ep % 2
    lane = iota((wide, wide), 1)
    there = ((y + 4 - lane // 64) % 4) * 64 + ((c + lane // 32) % 2) * 32 + lane % 32
    order = (iota((wide, wide), 0) == there).astype(bf16)
    cols = [normed_ref[:, pl.ds(pl.multiple_of(((z + 8 - j) % 8) * wide, wide), wide)] for j in range(8)]
    mine = dot(jnp.concatenate(cols, axis=0), order).astype(bf16)
    n = b0.shape[2]
    acc = jnp.zeros((rows, n), f32)
    for j in range(8):
        w = jnp.concatenate([b[j] for b in blocks], axis=0)
        acc = acc + dot(mine[j * rows : (j + 1) * rows, :], w)
    half = n // 2
    hidden = silu(acc[:, :half]) * acc[:, half:]
    hidden_ref[...] = hidden.astype(bf16)
    logit = jnp.sum(normed_ref[...].astype(f32) * gv_ref[...].astype(f32), axis=-1, keepdims=True)
    gate_ref[...] = jnp.broadcast_to(1.0 / (1.0 + jnp.exp(-logit)), gate_ref.shape)


def expert_kernel(arrived_ref, wg_ref, wu_ref, sh_ref, hidden_ref, x_v):
    n = arrived_ref.shape[0]
    peers = n // 8
    wide = arrived_ref.shape[1] // CAP
    a = iota((n, n), 0)
    b = iota((n, n), 1)
    order = ((b // 8 == a % peers) & (b % 8 == a // peers)).astype(bf16)
    sorted_rows = dot(order, arrived_ref[...]).astype(bf16)
    for r in range(8):
        for k in range(CAP):
            x_v[k * peers : (k + 1) * peers, r * wide : (r + 1) * wide] = sorted_rows[
                r * peers : (r + 1) * peers, k * wide : (k + 1) * wide
            ]
    x = x_v[...]
    gate = dot(x, wg_ref[0])
    up = dot(x, wu_ref[0])
    m = CAP * peers
    hidden_ref[:m, :] = (silu(gate) * up).astype(bf16)
    tail = hidden_ref.shape[0] - m
    sw = sh_ref.shape[1]
    hidden_ref[m:, :sw] = sh_ref[...]
    hidden_ref[m:, sw:] = jnp.zeros((tail, hidden_ref.shape[1] - sw), bf16)


def down_kernel(h0, h1, h2, h3, w0, w1, w2, w3, back_ref, shared_ref):
    hs = (h0, h1, h2, h3)
    ws = (w0, w1, w2, w3)
    n = back_ref.shape[0]
    peers = n // 8
    m = CAP * peers
    f = h0.shape[1]
    sw = w0.shape[0] - f
    acc = None
    sacc = None
    for h, w in zip(hs, ws):
        part = dot(h[:m, :], w[:f, :])
        acc = part if acc is None else acc + part
        part = dot(h[m:, :sw], w[f:, :])
        sacc = part if sacc is None else sacc + part
    shared_ref[...] = sacc
    out = acc.astype(bf16)
    half = out.shape[1] // 2
    pieces = [
        out[k * peers : (k + 1) * peers, h * half : (h + 1) * half] for k in range(CAP) for h in range(2)
    ]
    rhs = jnp.concatenate(pieces, axis=0)
    a = iota((n, 2 * m), 0)
    b = iota((n, 2 * m), 1)
    order = ((a % 8 == b // peers) & (a // 8 == b % peers)).astype(bf16)
    back_ref[...] = dot(order, rhs).astype(bf16)


def final_kernel(back_ref, mix_ref, residual_ref, shared_ref, gate_ref, out_ref):
    rows = out_ref.shape[0]
    half = out_ref.shape[1] // 2
    for h in range(2):
        r = dot(mix_ref[h * 3 * rows : (h + 1) * 3 * rows, :], back_ref[...])
        routed = (r[2 * rows :] + r[rows : 2 * rows]) + r[:rows]
        cols = slice(h * half, (h + 1) * half)
        total = residual_ref[:, cols] + routed + gate_ref[:, :1] * shared_ref[:, cols]
        out_ref[:, cols] = total.astype(bf16)


def around(k, size):
    return [(i, (i + k) % size) for i in range(size)]


def after(value, *deps):
    return lax.optimization_barrier((value, *deps))[0]


def shards(
    tokens, lengths, cache, attn_gain, query_weight, key_weight, value_weight, stick_bias, out_weight,
    ffn_gain, routes, route_weights, expert_gate, expert_up, expert_down, shared_gate, shared_up,
    shared_down, gate_vector,
):
    ntp = lax.axis_size("tp")
    nep = lax.axis_size("ep")
    rows, d = tokens.shape
    quarter = d // ntp
    part = lax.axis_index("tp")
    partial, normed = attend(tokens, lengths, cache, attn_gain, query_weight, stick_bias, out_weight)
    others = [lax.ppermute(partial, "tp", around(k, ntp)) for k in (2, 1, 3)]

    n_pick = 8 * nep
    pick, mix = call(
        route_kernel, [((n_pick, CAP * 8 * rows), bf16), ((6 * rows, n_pick), bf16)],
        (after(routes.T, partial), route_weights.T),
    )
    normed_mix, residual_full, sent = call(
        mix_kernel, [((rows, d), bf16), ((rows, d), f32), ((n_pick, CAP * d // 8), bf16)],
        (tokens, partial, *others, ffn_gain.reshape(1, -1), pick),
    )
    arrived = lax.all_to_all(sent.reshape(nep, 8, -1), "ep", 0, 0, tiled=True)
    arrived = arrived.reshape(n_pick, -1)

    joined = after(jnp.concatenate([shared_gate, shared_up], axis=1), sent)

    def shift(value, dz, dy, dc):
        perm = []
        for i in range(nep):
            z, y, c = i // 8, i // 2 % 4, i % 2
            perm.append((i, (z + dz) % (nep // 8) * 8 + (y + dy) % 4 * 2 + (c + dc) % 2))
        return lax.ppermute(value, "ep", perm)

    column = jnp.stack([joined] + [shift(joined, k, 0, 0) for k in range(1, nep // 8)])
    planes = [column] + [shift(column, 0, k, 0) for k in range(1, 4)]
    blocks = []
    for block in planes:
        blocks += [block, shift(block, 0, 0, 1)]
    down_all = after(jnp.concatenate([expert_down[0], shared_down], axis=0), sent)
    downs = []
    for k in range(ntp):
        cut = lax.dynamic_slice_in_dim(down_all, ((part + k) % ntp) * quarter, quarter, 1)
        downs.append(cut if k == 0 else lax.ppermute(cut, "tp", around(k, ntp)))
    shared_hidden, mix_gate = call(
        shared_kernel, [((rows, shared_gate.shape[1]), bf16), ((rows, 128), f32)],
        (lax.axis_index("ep").reshape(1), normed_mix, gate_vector.reshape(1, -1), *blocks),
        in_specs=[SM] + [VM] * 10,
    )
    m = CAP * nep
    (hidden,) = call(
        expert_kernel, [((m + rows, expert_gate.shape[2]), bf16)],
        (arrived, expert_gate, expert_up, shared_hidden), scratch=[pltpu.VMEM((m, d), bf16)],
    )
    hiddens = [hidden] + [lax.ppermute(hidden, "tp", around(k, ntp)) for k in range(1, ntp)]
    back, shared_out = call(down_kernel, [((n_pick, quarter // 2), bf16), ((rows, quarter), f32)], (*hiddens, *downs))
    returned = lax.all_to_all(back.reshape(nep, 8, -1), "ep", 0, 0, tiled=True).reshape(n_pick, -1)
    late = after(normed, back)
    residual = lax.dynamic_slice_in_dim(residual_full, part * quarter, quarter, 1)
    local_heads = key_weight.shape[1] // HEAD_DIM
    key_rows = jnp.dot(late, key_weight, preferred_element_type=f32).astype(bf16)
    value_rows = jnp.dot(late, value_weight, preferred_element_type=f32).astype(bf16)
    new_kv = jnp.stack(
        [key_rows.reshape(rows, local_heads, HEAD_DIM), value_rows.reshape(rows, local_heads, HEAD_DIM)], axis=2
    ).reshape(rows, -1)
    (layer_out,) = call(final_kernel, [((rows, quarter), bf16)], (returned, mix, residual, shared_out, mix_gate))
    return (layer_out, new_kv)


def solution(mesh):
    placed = (
        P("ep", None), P("ep"), P("ep", None, "tp"), P(), P(None, "tp"), P(None, "tp"), P(None, "tp"),
        P("tp"), P("tp", None), P(), P("ep", None), P("ep", None), P("ep", None, "tp"),
        P("ep", None, "tp"), P("ep", "tp", None), P("ep", "tp"), P("ep", "tp"), P("tp", None), P(),
    )

    return jax.shard_map(shards, mesh=mesh, in_specs=placed, out_specs=(P("ep", "tp"), P("ep", "tp")), check_vma=False)
```

time: 155 us -> 138 us (0.89)
  blocking collectives: 33.8 us -> 0 us
  starting transfers between devices: 21 us -> 53.2 us
  waiting for transfers between devices: 66.1 us -> 42.7 us
  matrix products: 15.4 us -> 0.36 us
  Pallas kernels: 0 us -> 14.7 us
  local copies, waits for them, and re-layouts: 13.4 us -> 24.3 us
  other arithmetic: 2.89 us -> 1.31 us
    all_to_all x4 -> x2, waiting for transfers between devices: 66.1 us -> 11.2 us  [the longest x1 11.2 us: shards(): lax.all_to_all(back.reshape(nep, 8, -1), 'ep', 0, 0, tiled=True)]
    ppermute x0 -> x23, starting transfers between devices: none -> 35.8 us  [the longest x14 23.5 us: shift(): return lax.ppermute(value, 'ep', perm)]
    all_to_all x2 -> x0, blocking collectives: 33.8 us -> none  [the longest x1 23.6 us: shards(): lax.all_to_all(normed_mix, 'ep', split_axis=1, concat_axis=0, tiled=True)]
    ppermute x0 -> x23, waiting for transfers between devices: none -> 31.5 us  [the longest x14 24.6 us: shift(): return lax.ppermute(value, 'ep', perm)]
    dot_general x16 -> x2, matrix products: 15.4 us -> 0.36 us  [the longest x1 0.19 us: shards(): jnp.dot(late, key_weight, preferred_element_type=f32).astype(bf16)]
    pallas_call x0 -> x7, Pallas kernels: none -> 14.7 us  [call(): pl.pallas_call(kernel, out_shape=tuple((jax.ShapeDtypeStruct(s, t) for s,...]
    unnamed x41 -> x73, local copies, waits for them, and re-layouts: 6.95 us -> 19.8 us
    all_to_all x4 -> x2, starting transfers between devices: 21 us -> 17.4 us  [the longest x1 10.1 us: shards(): arrived = lax.all_to_all(sent.reshape(nep, 8, -1), 'ep', 0, 0, tiled=True)]
  transfers between devices with their start and end apart: 4 -> 25, of which waited for: 4 -> 12; matrix products, arithmetic and copies ran while one was open for 2% -> 8% of each run, Pallas kernels for 0% -> 3%
where the time goes in v1:
time: 138 us; the launch traced here: 137 us
  starting transfers between devices  53.2 us (39%)
  waiting for transfers between devices  42.7 us (31%)
  local copies, waits for them, and re-layouts  24.3 us (18%)
  Pallas kernels  14.7 us (11%)
    ppermute x14, waiting for transfers between devices, shift(): return lax.ppermute(value, 'ep', perm)  24.6 us
    ppermute x14, starting transfers between devices, shift(): return lax.ppermute(value, 'ep', perm)  23.5 us
    unnamed x73, local copies, waits for them, and re-layouts  19.8 us
    pallas_call x7, Pallas kernels, call(): pl.pallas_call(kernel, out_shape=tuple((jax.ShapeDtypeStruct(s, t) for s,...  14.7 us
    all_to_all x1, waiting for transfers between devices, shards(): lax.all_to_all(back.reshape(nep, 8, -1), 'ep', 0, 0, tiled=True)  11.2 us
    all_to_all x1, starting transfers between devices, shards(): arrived = lax.all_to_all(sent.reshape(nep, 8, -1), 'ep', 0, 0, tiled=True)  10.1 us
    all_to_all x1, starting transfers between devices, shards(): lax.all_to_all(back.reshape(nep, 8, -1), 'ep', 0, 0, tiled=True)  7.27 us
    ppermute x3, waiting for transfers between devices, shards(): lax.ppermute(hidden, 'tp', around(k, ntp))  5.62 us
  transfers between devices with their start and end apart: 25, of which 12 were waited for; matrix products, arithmetic and copies ran while one was open for 8% of the time, Pallas kernels for 3%

profile of v1, /device:TPU:1, one launch (start us, length us, event | category | flops | bytes accessed | tf_op | source)
XLA Modules:
  0.0 137.4 jit_solution(2370066315054854043)
XLA Ops:
  0.7 2.2 %copy-done.1 = bf16[16,1024,128]{2,1,0:T(8,128)(2,1)S(1)} copy-done((bf16[16,1024,128]{2,1,0:T(8,128)(2,1)S(1)}, bf16[16,1024,128]{2,1,0:T(8,128)(2,1)}, u32[]{:S(2)}) %copy-start.1) | copy-done | bytes 4194328
  8.2 6.2 %shard_map.194 = (bf16[16,2048]{1,0:T(8,128)(2,1)S(1)}, bf16[16,2048]{1,0:T(8,128)(2,1)S(1)}) custom-call(s32[16]{0:T(128)S(1)} %copy-done.25, f32[4]{0:T(128)S(1)} %copy-done.26, bf16[16,2048]{1,0:T(8,128)(2,1)S(1)} %copy-done.6, f32[1,2048]{1,0:T(1,128)S(1)} %bitcast.38, bf16[16,1024,128]{2,1,0:T(8,128)(2,1)S(1)} %copy-done.1, ...), custom_call_target="tpu_custom_call" | custom-call | tf_op jit(solution)/shard_map/pallas_call | solution.py:36
  15.0 3.3 %collective-permute-start.2 = (bf16[16,2048]{1,0:T(8,128)(2,1)S(1)}, bf16[16,2048]{1,0:T(8,128)(2,1)S(1)}, u32[]{:S(2)}, u32[]{:S(2)}) collective-permute-start(bf16[16,2048]{1,0:T(8,128)(2,1)S(1)} %get-tuple-element.17.p0), channel_id=1, source_target_pairs={{0,3},{1,0},{2,1},{3,2},{4,7},{5,4},{6,5},{7,6},{8,11},{9,8},{10,9... | collective-permute-start | bytes 196616 | tf_op jit(solution)/shard_map/ppermute | solution.py:310
  18.3 1.7 %collective-permute-start = (bf16[16,2048]{1,0:T(8,128)(2,1)S(1)}, bf16[16,2048]{1,0:T(8,128)(2,1)S(1)}, u32[]{:S(2)}, u32[]{:S(2)}) collective-permute-start(bf16[16,2048]{1,0:T(8,128)(2,1)S(1)} %get-tuple-element.17.p0), channel_id=1, source_target_pairs={{0,2},{1,3},{2,0},{3,1},{4,6},{5,7},{6,4},{7,5},{8,10},{9,11},{10,... | collective-permute-start | bytes 196616 | tf_op jit(solution)/shard_map/ppermute | solution.py:310
  21.7 1.3 pad_maximum_fusion
  23.5 1.4 %shard_map.196 = (bf16[16,2048]{1,0:T(8,128)(2,1)S(1)}, f32[16,2048]{1,0:T(8,128)S(1)}, bf16[512,768]{1,0:T(8,128)(2,1)}) custom-call(bf16[16,2048]{1,0:T(8,128)(2,1)S(1)} %copy-done.7, bf16[16,2048]{1,0:T(8,128)(2,1)S(1)} %get-tuple-element.17.p0, bf16[16,2048]{1,0:T(8,128)(2,1)S(1)} %collective-permute-done.p1, ...), custom_call_target="tpu_custom_call" | custom-call | tf_op jit(solution)/shard_map/pallas_call | solution.py:36
  26.1 5.6 %collective-permute-start.9 = (bf16[32,256]{1,0:T(8,128)(2,1)S(1)}, bf16[32,256]{1,0:T(8,128)(2,1)S(1)}, u32[]{:S(2)}, u32[]{:S(2)}) collective-permute-start(bf16[32,256]{1,0:T(8,128)(2,1)S(1)} %pad_maximum_fusion.1), channel_id=1, source_target_pairs={{0,224},{4,228},{8,232},{12,236},{16,240},{20,244},{24,248},{28,25... | collective-permute-start | bytes 49160 | tf_op jit(solution)/shard_map/ppermute | solution.py:331
  33.3 4.5 %collective-permute-start.6 = (bf16[32,256]{1,0:T(8,128)(2,1)S(1)}, bf16[32,256]{1,0:T(8,128)(2,1)S(1)}, u32[]{:S(2)}, u32[]{:S(2)}) collective-permute-start(bf16[32,256]{1,0:T(8,128)(2,1)S(1)} %pad_maximum_fusion.1), channel_id=1, source_target_pairs={{0,128},{4,132},{8,136},{12,140},{16,144},{20,148},{24,152},{28,15... | collective-permute-start | bytes 49160 | tf_op jit(solution)/shard_map/ppermute | solution.py:331
  39.2 10.1 %all-to-all-start = ((bf16[64,8,768]{2,1,0:T(8,128)(2,1)}), bf16[64,8,768]{2,1,0:T(8,128)(2,1)S(1)}, u32[]{:S(2)}, u32[]{:S(2)}) async-start(bf16[64,8,768]{2,1,0:T(8,128)(2,1)} %bitcast.4), calls=%async_computation | async-start | bytes 1572864 | tf_op jit(solution)/shard_map/all_to_all | solution.py:321
  49.3 2.3 %collective-permute-start.4 = (bf16[32,256]{1,0:T(8,128)(2,1)S(1)}, bf16[32,256]{1,0:T(8,128)(2,1)S(1)}, u32[]{:S(2)}, u32[]{:S(2)}) collective-permute-start(bf16[32,256]{1,0:T(8,128)(2,1)S(1)} %pad_maximum_fusion.1), channel_id=1, source_target_pairs={{0,64},{4,68},{8,72},{12,76},{16,80},{20,84},{24,88},{28,92},{32,9... | collective-permute-start | bytes 49160 | tf_op jit(solution)/shard_map/ppermute | solution.py:331
  52.3 18.0 %collective-permute-done.4 = bf16[32,256]{1,0:T(8,128)(2,1)S(1)} collective-permute-done((bf16[32,256]{1,0:T(8,128)(2,1)S(1)}, bf16[32,256]{1,0:T(8,128)(2,1)S(1)}, u32[]{:S(2)}, u32[]{:S(2)}) %collective-permute-start.4) | collective-permute-done | bytes 16416 | tf_op jit(solution)/shard_map/ppermute | solution.py:331
  71.2 4.7 %collective-permute-done.5 = bf16[32,256]{1,0:T(8,128)(2,1)S(1)} collective-permute-done((bf16[32,256]{1,0:T(8,128)(2,1)S(1)}, bf16[32,256]{1,0:T(8,128)(2,1)S(1)}, u32[]{:S(2)}, u32[]{:S(2)}) %collective-permute-start.5) | collective-permute-done | bytes 16416 | tf_op jit(solution)/shard_map/ppermute | solution.py:331
  78.9 2.1 %collective-permute-start.15 = (bf16[8,32,256]{2,1,0:T(8,128)(2,1)}, bf16[8,32,256]{2,1,0:T(8,128)(2,1)S(1)}, u32[]{:S(2)}, u32[]{:S(2)}) collective-permute-start(bf16[8,32,256]{2,1,0:T(8,128)(2,1)} %constant_dynamic-update-slice_fusion.b0), channel_id=1, source_target_pairs={{0,24},{4,28},{8,0},{12,4},{16,8},{20,12},{24,16},{28,20},{32,56},... | collective-permute-start | bytes 393224 | tf_op jit(solution)/shard_map/ppermute | solution.py:331
  82.3 2.4 %constant_dynamic-slice_fusion.1 = (bf16[384,512]{1,0:T(8,128)(2,1)}, bf16[384,512]{1,0:T(8,128)(2,1)}, bf16[384,512]{1,0:T(8,128)(2,1)}, bf16[384,512]{1,0:T(8,128)(2,1)S(1)}) fusion(bf16[384,2048]{1,0:T(8,128)(2,1)} %pad_maximum_fusion, s32[]{:T(128)S(6)} %select_n.41, s32[]{:T(128)S(6)} %select_n.39, s32[]{:T(128)S(6)} %select_n.37, s32[]{:T(128)S(6)} %select_n.35), kind=kLoop, calls=%fused_computation.16 | loop fusion | bytes 3145744 | tf_op jit(solution)/shard_map/dynamic_slice | solution.py:341
  84.8 2.5 %collective-permute-start.22 = (bf16[384,512]{1,0:T(8,128)(2,1)}, bf16[384,512]{1,0:T(8,128)(2,1)}, u32[]{:S(2)}, u32[]{:S(2)}) collective-permute-start(bf16[384,512]{1,0:T(8,128)(2,1)} %get-tuple-element.32), channel_id=1, source_target_pairs={{0,3},{1,0},{2,1},{3,2},{4,7},{5,4},{6,5},{7,6},{8,11},{9,8},{10,9... | collective-permute-start | bytes 1179656 | tf_op jit(solution)/shard_map/ppermute | solution.py:342
  87.8 4.3 %collective-permute-start.10 = (bf16[8,32,256]{2,1,0:T(8,128)(2,1)}, bf16[8,32,256]{2,1,0:T(8,128)(2,1)S(1)}, u32[]{:S(2)}, u32[]{:S(2)}) collective-permute-start(bf16[8,32,256]{2,1,0:T(8,128)(2,1)} %constant_dynamic-update-slice_fusion.b0), channel_id=1, source_target_pairs={{0,4},{4,0},{8,12},{12,8},{16,20},{20,16},{24,28},{28,24},{32,36},... | collective-permute-start | bytes 393224 | tf_op jit(solution)/shard_map/ppermute | solution.py:331
  100.2 1.6 %shard_map.197 = (bf16[16,128]{1,0:T(8,128)(2,1)S(1)}, f32[16,128]{1,0:T(8,128)S(1)}) custom-call(s32[1]{0:T(128)} %bitcast.6.ep_ref, bf16[16,2048]{1,0:T(8,128)(2,1)S(1)} %copy-done.19, bf16[1,2048]{1,0:T(2,128)(2,1)S(1)} %reshape.36.gv_ref, bf16[8,32,256]{2,1,0:T(8,128)(2,1)} %constant_dynamic-update-slice_fusion.b0, bf16[8,32,256]{2,1,0:T(8,128)(2,1)S(1)} %copy-done.13, ...), custom_call_target="tpu_custom_call" | custom-call | tf_op jit(solution)/shard_map/pallas_call | solution.py:36
  102.9 2.4 %collective-permute-start.19 = (bf16[208,256]{1,0:T(8,128)(2,1)S(1)}, bf16[208,256]{1,0:T(8,128)(2,1)S(1)}, u32[]{:S(2)}, u32[]{:S(2)}) collective-permute-start(bf16[208,256]{1,0:T(8,128)(2,1)S(1)} %shard_map.198.h0), channel_id=1, source_target_pairs={{0,3},{1,0},{2,1},{3,2},{4,7},{5,4},{6,5},{7,6},{8,11},{9,8},{10,9... | collective-permute-start | bytes 319496 | tf_op jit(solution)/shard_map/ppermute | solution.py:353
  105.3 1.8 %collective-permute-start.18 = (bf16[208,256]{1,0:T(8,128)(2,1)S(1)}, bf16[208,256]{1,0:T(8,128)(2,1)S(1)}, u32[]{:S(2)}, u32[]{:S(2)}) collective-permute-start(bf16[208,256]{1,0:T(8,128)(2,1)S(1)} %shard_map.198.h0), channel_id=1, source_target_pairs={{0,2},{1,3},{2,0},{3,1},{4,6},{5,7},{6,4},{7,5},{8,10},{9,11},{10,... | collective-permute-start | bytes 319496 | tf_op jit(solution)/shard_map/ppermute | solution.py:353
  108.5 2.3 %collective-permute-done.18.h2 = bf16[208,256]{1,0:T(8,128)(2,1)S(1)} collective-permute-done((bf16[208,256]{1,0:T(8,128)(2,1)S(1)}, bf16[208,256]{1,0:T(8,128)(2,1)S(1)}, u32[]{:S(2)}, u32[]{:S(2)}) %collective-permute-start.18) | collective-permute-done | bytes 106528 | tf_op jit(solution)/shard_map/ppermute | solution.py:353
  110.9 2.7 %collective-permute-done.17.h1 = bf16[208,256]{1,0:T(8,128)(2,1)S(1)} collective-permute-done((bf16[208,256]{1,0:T(8,128)(2,1)S(1)}, bf16[208,256]{1,0:T(8,128)(2,1)S(1)}, u32[]{:S(2)}, u32[]{:S(2)}) %collective-permute-start.17) | collective-permute-done | bytes 106528 | tf_op jit(solution)/shard_map/ppermute | solution.py:353
  113.5 2.7 %shard_map.199 = (bf16[512,256]{1,0:T(8,128)(2,1)}, f32[16,512]{1,0:T(8,128)S(1)}) custom-call(bf16[208,256]{1,0:T(8,128)(2,1)S(1)} %shard_map.198.h0, bf16[208,256]{1,0:T(8,128)(2,1)S(1)} %collective-permute-done.17.h1, bf16[208,256]{1,0:T(8,128)(2,1)S(1)} %collective-permute-done.18.h2, bf16[208,256]{1,0:T(8,128)(2,1)S(1)} %collective-permute-done.19.h3, ...), custom_call_target="tpu_custom_call" | custom-call | tf_op jit(solution)/shard_map/pallas_call | solution.py:36
  116.3 7.3 %all-to-all-start.1 = ((bf16[64,8,256]{2,1,0:T(8,128)(2,1)}), bf16[64,8,256]{2,1,0:T(8,128)(2,1)S(1)}, u32[]{:S(2)}, u32[]{:S(2)}) async-start(bf16[64,8,256]{2,1,0:T(8,128)(2,1)} %bitcast.16), calls=%async_computation.1 | async-start | bytes 524288 | tf_op jit(solution)/shard_map/all_to_all | solution.py:355
  125.4 11.2 %all-to-all-done.1 = bf16[64,8,256]{2,1,0:T(8,128)(2,1)S(1)} async-done(((bf16[64,8,256]{2,1,0:T(8,128)(2,1)}), bf16[64,8,256]{2,1,0:T(8,128)(2,1)S(1)}, u32[]{:S(2)}, u32[]{:S(2)}) %all-to-all-start.1) | async-done | bytes 262176 | tf_op jit(solution)/shard_map/all_to_all | solution.py:355
  (117 shorter events, 31.9 us)
Async XLA Ops:
  15.0 8.0 %collective-permute-start.2 = (bf16[16,2048]{1,0:T(8,128)(2,1)S(1)}, bf16[16,2048]{1,0:T(8,128)(2,1)S(1)}, u32[]{:S(2)}, u32[]{:S(2)}) collective-permute-start(bf16[16,2048]{1,0:T(8,128)(2,1)S(1)} %get-tuple-element.17.p0), channel_id=1, source_target_pairs={{0,3},{1,0},{2,1},{3,2},{4,7},{5,4},{6,5},{7,6},{8,11},{9,8},{10,9... | collective-permute-start | bytes 196616 | tf_op jit(solution)/shard_map/ppermute | solution.py:310
  18.3 4.9 %collective-permute-start.1 = (bf16[16,2048]{1,0:T(8,128)(2,1)S(1)}, bf16[16,2048]{1,0:T(8,128)(2,1)S(1)}, u32[]{:S(2)}, u32[]{:S(2)}) collective-permute-start(bf16[16,2048]{1,0:T(8,128)(2,1)S(1)} %get-tuple-element.17.p0), channel_id=1, source_target_pairs={{0,1},{1,2},{2,3},{3,0},{4,5},{5,6},{6,7},{7,4},{8,9},{9,10},{10,1... | collective-permute-start | bytes 196616 | tf_op jit(solution)/shard_map/ppermute | solution.py:310
  18.3 5.1 %collective-permute-start = (bf16[16,2048]{1,0:T(8,128)(2,1)S(1)}, bf16[16,2048]{1,0:T(8,128)(2,1)S(1)}, u32[]{:S(2)}, u32[]{:S(2)}) collective-permute-start(bf16[16,2048]{1,0:T(8,128)(2,1)S(1)} %get-tuple-element.17.p0), channel_id=1, source_target_pairs={{0,2},{1,3},{2,0},{3,1},{4,6},{5,7},{6,4},{7,5},{8,10},{9,11},{10,... | collective-permute-start | bytes 196616 | tf_op jit(solution)/shard_map/ppermute | solution.py:310
  26.1 52.2 %collective-permute-start.9 = (bf16[32,256]{1,0:T(8,128)(2,1)S(1)}, bf16[32,256]{1,0:T(8,128)(2,1)S(1)}, u32[]{:S(2)}, u32[]{:S(2)}) collective-permute-start(bf16[32,256]{1,0:T(8,128)(2,1)S(1)} %pad_maximum_fusion.1), channel_id=1, source_target_pairs={{0,224},{4,228},{8,232},{12,236},{16,240},{20,244},{24,248},{28,25... | collective-permute-start | bytes 49160 | tf_op jit(solution)/shard_map/ppermute | solution.py:331
  31.7 46.0 %collective-permute-start.8 = (bf16[32,256]{1,0:T(8,128)(2,1)S(1)}, bf16[32,256]{1,0:T(8,128)(2,1)S(1)}, u32[]{:S(2)}, u32[]{:S(2)}) collective-permute-start(bf16[32,256]{1,0:T(8,128)(2,1)S(1)} %pad_maximum_fusion.1), channel_id=1, source_target_pairs={{0,192},{4,196},{8,200},{12,204},{16,208},{20,212},{24,216},{28,22... | collective-permute-start | bytes 49160 | tf_op jit(solution)/shard_map/ppermute | solution.py:331
  32.9 44.2 %collective-permute-start.7 = (bf16[32,256]{1,0:T(8,128)(2,1)S(1)}, bf16[32,256]{1,0:T(8,128)(2,1)S(1)}, u32[]{:S(2)}, u32[]{:S(2)}) collective-permute-start(bf16[32,256]{1,0:T(8,128)(2,1)S(1)} %pad_maximum_fusion.1), channel_id=1, source_target_pairs={{0,160},{4,164},{8,168},{12,172},{16,176},{20,180},{24,184},{28,18... | collective-permute-start | bytes 49160 | tf_op jit(solution)/shard_map/ppermute | solution.py:331
  33.3 43.1 %collective-permute-start.6 = (bf16[32,256]{1,0:T(8,128)(2,1)S(1)}, bf16[32,256]{1,0:T(8,128)(2,1)S(1)}, u32[]{:S(2)}, u32[]{:S(2)}) collective-permute-start(bf16[32,256]{1,0:T(8,128)(2,1)S(1)} %pad_maximum_fusion.1), channel_id=1, source_target_pairs={{0,128},{4,132},{8,136},{12,140},{16,144},{20,148},{24,152},{28,15... | collective-permute-start | bytes 49160 | tf_op jit(solution)/shard_map/ppermute | solution.py:331
  37.8 11.5 %collective-permute-start.3 = (bf16[32,256]{1,0:T(8,128)(2,1)S(1)}, bf16[32,256]{1,0:T(8,128)(2,1)S(1)}, u32[]{:S(2)}, u32[]{:S(2)}) collective-permute-start(bf16[32,256]{1,0:T(8,128)(2,1)S(1)} %pad_maximum_fusion.1), channel_id=1, source_target_pairs={{0,32},{4,36},{8,40},{12,44},{16,48},{20,52},{24,56},{28,60},{32,6... | collective-permute-start | bytes 49160 | tf_op jit(solution)/shard_map/ppermute | solution.py:331
  39.2 62.7 %all-to-all-start = ((bf16[64,8,768]{2,1,0:T(8,128)(2,1)}), bf16[64,8,768]{2,1,0:T(8,128)(2,1)S(1)}, u32[]{:S(2)}, u32[]{:S(2)}) async-start(bf16[64,8,768]{2,1,0:T(8,128)(2,1)} %bitcast.4), calls=%async_computation | async-start | bytes 1572864 | tf_op jit(solution)/shard_map/all_to_all | solution.py:321
  49.3 21.0 %collective-permute-start.4 = (bf16[32,256]{1,0:T(8,128)(2,1)S(1)}, bf16[32,256]{1,0:T(8,128)(2,1)S(1)}, u32[]{:S(2)}, u32[]{:S(2)}) collective-permute-start(bf16[32,256]{1,0:T(8,128)(2,1)S(1)} %pad_maximum_fusion.1), channel_id=1, source_target_pairs={{0,64},{4,68},{8,72},{12,76},{16,80},{20,84},{24,88},{28,92},{32,9... | collective-permute-start | bytes 49160 | tf_op jit(solution)/shard_map/ppermute | solution.py:331
  70.3 5.6 %collective-permute-start.5 = (bf16[32,256]{1,0:T(8,128)(2,1)S(1)}, bf16[32,256]{1,0:T(8,128)(2,1)S(1)}, u32[]{:S(2)}, u32[]{:S(2)}) collective-permute-start(bf16[32,256]{1,0:T(8,128)(2,1)S(1)} %pad_maximum_fusion.1), channel_id=1, source_target_pairs={{0,96},{4,100},{8,104},{12,108},{16,112},{20,116},{24,120},{28,124... | collective-permute-start | bytes 49160 | tf_op jit(solution)/shard_map/ppermute | solution.py:331
  78.9 8.4 %collective-permute-start.15 = (bf16[8,32,256]{2,1,0:T(8,128)(2,1)}, bf16[8,32,256]{2,1,0:T(8,128)(2,1)S(1)}, u32[]{:S(2)}, u32[]{:S(2)}) collective-permute-start(bf16[8,32,256]{2,1,0:T(8,128)(2,1)} %constant_dynamic-update-slice_fusion.b0), channel_id=1, source_target_pairs={{0,24},{4,28},{8,0},{12,4},{16,8},{20,12},{24,16},{28,20},{32,56},... | collective-permute-start | bytes 393224 | tf_op jit(solution)/shard_map/ppermute | solution.py:331
  81.0 6.8 %collective-permute-start.13 = (bf16[8,32,256]{2,1,0:T(8,128)(2,1)}, bf16[8,32,256]{2,1,0:T(8,128)(2,1)}, u32[]{:S(2)}, u32[]{:S(2)}) collective-permute-start(bf16[8,32,256]{2,1,0:T(8,128)(2,1)} %constant_dynamic-update-slice_fusion.b0), channel_id=1, source_target_pairs={{0,16},{4,20},{8,24},{12,28},{16,0},{20,4},{24,8},{28,12},{32,48},... | collective-permute-start | bytes 393224 | tf_op jit(solution)/shard_map/ppermute | solution.py:331
  82.0 10.1 %collective-permute-start.11 = (bf16[8,32,256]{2,1,0:T(8,128)(2,1)}, bf16[8,32,256]{2,1,0:T(8,128)(2,1)}, u32[]{:S(2)}, u32[]{:S(2)}) collective-permute-start(bf16[8,32,256]{2,1,0:T(8,128)(2,1)} %constant_dynamic-update-slice_fusion.b0), channel_id=1, source_target_pairs={{0,8},{4,12},{8,16},{12,20},{16,24},{20,28},{24,0},{28,4},{32,40},... | collective-permute-start | bytes 393224 | tf_op jit(solution)/shard_map/ppermute | solution.py:331
  84.8 22.3 %collective-permute-start.22 = (bf16[384,512]{1,0:T(8,128)(2,1)}, bf16[384,512]{1,0:T(8,128)(2,1)}, u32[]{:S(2)}, u32[]{:S(2)}) collective-permute-start(bf16[384,512]{1,0:T(8,128)(2,1)} %get-tuple-element.32), channel_id=1, source_target_pairs={{0,3},{1,0},{2,1},{3,2},{4,7},{5,4},{6,5},{7,6},{8,11},{9,8},{10,9... | collective-permute-start | bytes 1179656 | tf_op jit(solution)/shard_map/ppermute | solution.py:342
  87.3 19.9 %collective-permute-start.21 = (bf16[384,512]{1,0:T(8,128)(2,1)}, bf16[384,512]{1,0:T(8,128)(2,1)}, u32[]{:S(2)}, u32[]{:S(2)}) collective-permute-start(bf16[384,512]{1,0:T(8,128)(2,1)} %get-tuple-element.33), channel_id=1, source_target_pairs={{0,2},{1,3},{2,0},{3,1},{4,6},{5,7},{6,4},{7,5},{8,10},{9,11},{10,... | collective-permute-start | bytes 1179656 | tf_op jit(solution)/shard_map/ppermute | solution.py:342
  87.3 20.7 %collective-permute-start.20 = (bf16[384,512]{1,0:T(8,128)(2,1)}, bf16[384,512]{1,0:T(8,128)(2,1)}, u32[]{:S(2)}, u32[]{:S(2)}) collective-permute-start(bf16[384,512]{1,0:T(8,128)(2,1)} %get-tuple-element.34), channel_id=1, source_target_pairs={{0,1},{1,2},{2,3},{3,0},{4,5},{5,6},{6,7},{7,4},{8,9},{9,10},{10,1... | collective-permute-start | bytes 1179656 | tf_op jit(solution)/shard_map/ppermute | solution.py:342
  87.8 5.5 %collective-permute-start.10 = (bf16[8,32,256]{2,1,0:T(8,128)(2,1)}, bf16[8,32,256]{2,1,0:T(8,128)(2,1)S(1)}, u32[]{:S(2)}, u32[]{:S(2)}) collective-permute-start(bf16[8,32,256]{2,1,0:T(8,128)(2,1)} %constant_dynamic-update-slice_fusion.b0), channel_id=1, source_target_pairs={{0,4},{4,0},{8,12},{12,8},{16,20},{20,16},{24,28},{28,24},{32,36},... | collective-permute-start | bytes 393224 | tf_op jit(solution)/shard_map/ppermute | solution.py:331
  92.1 2.2 %collective-permute-start.16 = (bf16[8,32,256]{2,1,0:T(8,128)(2,1)S(1)}, bf16[8,32,256]{2,1,0:T(8,128)(2,1)S(1)}, u32[]{:S(2)}, u32[]{:S(2)}) collective-permute-start(bf16[8,32,256]{2,1,0:T(8,128)(2,1)S(1)} %collective-permute-done.15.b6), channel_id=1, source_target_pairs={{0,4},{4,0},{8,12},{12,8},{16,20},{20,16},{24,28},{28,24},{32,36},... | collective-permute-start | bytes 393224 | tf_op jit(solution)/shard_map/ppermute | solution.py:331
  94.0 1.7 %collective-permute-start.14 = (bf16[8,32,256]{2,1,0:T(8,128)(2,1)}, bf16[8,32,256]{2,1,0:T(8,128)(2,1)}, u32[]{:S(2)}, u32[]{:S(2)}) collective-permute-start(bf16[8,32,256]{2,1,0:T(8,128)(2,1)} %collective-permute-done.13.b4), channel_id=1, source_target_pairs={{0,4},{4,0},{8,12},{12,8},{16,20},{20,16},{24,28},{28,24},{32,36},... | collective-permute-start | bytes 393224 | tf_op jit(solution)/shard_map/ppermute | solution.py:331
  102.9 5.6 %collective-permute-start.19 = (bf16[208,256]{1,0:T(8,128)(2,1)S(1)}, bf16[208,256]{1,0:T(8,128)(2,1)S(1)}, u32[]{:S(2)}, u32[]{:S(2)}) collective-permute-start(bf16[208,256]{1,0:T(8,128)(2,1)S(1)} %shard_map.198.h0), channel_id=1, source_target_pairs={{0,3},{1,0},{2,1},{3,2},{4,7},{5,4},{6,5},{7,6},{8,11},{9,8},{10,9... | collective-permute-start | bytes 319496 | tf_op jit(solution)/shard_map/ppermute | solution.py:353
  105.3 5.6 %collective-permute-start.18 = (bf16[208,256]{1,0:T(8,128)(2,1)S(1)}, bf16[208,256]{1,0:T(8,128)(2,1)S(1)}, u32[]{:S(2)}, u32[]{:S(2)}) collective-permute-start(bf16[208,256]{1,0:T(8,128)(2,1)S(1)} %shard_map.198.h0), channel_id=1, source_target_pairs={{0,2},{1,3},{2,0},{3,1},{4,6},{5,7},{6,4},{7,5},{8,10},{9,11},{10,... | collective-permute-start | bytes 319496 | tf_op jit(solution)/shard_map/ppermute | solution.py:353
  107.1 6.4 %collective-permute-start.17 = (bf16[208,256]{1,0:T(8,128)(2,1)S(1)}, bf16[208,256]{1,0:T(8,128)(2,1)S(1)}, u32[]{:S(2)}, u32[]{:S(2)}) collective-permute-start(bf16[208,256]{1,0:T(8,128)(2,1)S(1)} %shard_map.198.h0), channel_id=1, source_target_pairs={{0,1},{1,2},{2,3},{3,0},{4,5},{5,6},{6,7},{7,4},{8,9},{9,10},{10,1... | collective-permute-start | bytes 319496 | tf_op jit(solution)/shard_map/ppermute | solution.py:353
  116.3 20.4 %all-to-all-start.1 = ((bf16[64,8,256]{2,1,0:T(8,128)(2,1)}), bf16[64,8,256]{2,1,0:T(8,128)(2,1)S(1)}, u32[]{:S(2)}, u32[]{:S(2)}) async-start(bf16[64,8,256]{2,1,0:T(8,128)(2,1)} %bitcast.16), calls=%async_computation.1 | async-start | bytes 524288 | tf_op jit(solution)/shard_map/all_to_all | solution.py:355
  (34 other events, 326.2 us)

commit v2 on v1

v2 whole, which is shorter than its diff:
```python
import jax
import jax.numpy as jnp
from jax import lax
from jax.experimental import pallas as pl
from jax.experimental.pallas import tpu as pltpu
from jax.sharding import PartitionSpec as P

HEAD_DIM = 64
EPS = 1e-06
CAP = 3
bf16 = jnp.bfloat16
f32 = jnp.float32

VM = pl.BlockSpec(memory_space=pltpu.VMEM)
SM = pl.BlockSpec(memory_space=pltpu.SMEM)
HBM = pl.BlockSpec(memory_space=pltpu.HBM)


def iota(shape, dim):
    return lax.broadcasted_iota(jnp.int32, shape, dim)


def dot(a, b, dims=((1,), (0,))):
    return lax.dot_general(a, b, (dims, ((), ())), preferred_element_type=f32)


def three_pieces(values):
    high = values.astype(bf16)
    rest = values - high.astype(f32)
    middle = rest.astype(bf16)
    low = (rest - middle.astype(f32)).astype(bf16)
    return high, middle, low


def hbm(value):
    return pltpu.with_memory_space_constraint(value, pltpu.HBM)


def call(kernel, outs, ins, in_specs=None, out_specs=None, scratch=(), limit_mib=8):
    in_specs = in_specs or [VM] * len(ins)
    out_specs = out_specs or [VM] * len(outs)
    ins = [hbm(x) if spec is HBM else x for x, spec in zip(ins, in_specs)]
    shapes = [
        pltpu.HBM(s, t) if spec is HBM else jax.ShapeDtypeStruct(s, t) for (s, t), spec in zip(outs, out_specs)
    ]
    return pl.pallas_call(
        kernel,
        out_shape=tuple(shapes),
        in_specs=in_specs,
        out_specs=tuple(out_specs),
        scratch_shapes=list(scratch),
        compiler_params=pltpu.CompilerParams(vmem_limit_bytes=limit_mib * 1024 * 1024),
    )(*ins)


def copy_all(pairs, sems, first=0):
    copies = [pltpu.make_async_copy(src, dst, sems.at[first + i]) for i, (src, dst) in enumerate(pairs)]
    for c in copies:
        c.start()
    return copies


def attend_kernel(len_hbm, bias_hbm, tok_hbm, gain_hbm, cache_hbm, wq_hbm, wo_hbm, sg_hbm, su_hbm,
                  part_ref, joined_hbm,
                  len_ref, bias_ref, tok_ref, gain_ref, cache_v, wq_v, wo_v, s_v, joined_v, sem_c, sem_w, sem_j):
    rows = tok_ref.shape[0]
    span = cache_v.shape[1]
    heads = 4
    hr = rows * heads
    small = []
    for i, (src, dst) in enumerate(
        [(tok_hbm, tok_ref), (gain_hbm, gain_ref), (wq_hbm, wq_v), (wo_hbm, wo_v),
         (len_hbm, len_ref), (bias_hbm, bias_ref)]
    ):
        small.append(pltpu.make_async_copy(src, dst, sem_w.at[i]))
    tok_c, gain_c, wq_c, wo_c, len_c, bias_c = small
    tok_c.start()
    gain_c.start()
    wq_c.start()
    cache_c = []
    for n in range(rows):
        c = pltpu.make_async_copy(cache_hbm.at[n], cache_v.at[n], sem_c.at[n])
        c.start()
        cache_c.append(c)
    len_c.start()
    bias_c.start()
    wo_c.start()
    width = sg_hbm.shape[1]
    for c in copy_all([(sg_hbm, joined_v.at[:, :width]), (su_hbm, joined_v.at[:, width:])], sem_j, 8):
        small.append(c)
    tok_c.wait()
    gain_c.wait()
    x = tok_ref[...].astype(f32)
    ms = jnp.mean(x * x, axis=-1, keepdims=True)
    normed = (x * lax.rsqrt(ms + EPS) * gain_ref[...]).astype(bf16)
    expand = (iota((hr, rows), 0) // heads == iota((hr, rows), 1)).astype(bf16)
    lane = iota((hr, heads * HEAD_DIM), 1)
    row = iota((hr, heads * HEAD_DIM), 0)
    fold = ((iota((256, 128), 0) % HEAD_DIM) == iota((256, 128), 1)).astype(bf16)
    wq_c.wait()
    q = dot(normed, wq_v[...]).astype(bf16)
    qx = jnp.where(lane // HEAD_DIM == row % heads, dot(expand, q), 0.0).astype(bf16)
    qk = (dot(qx, fold) * (HEAD_DIM**-0.5)).astype(bf16)
    wide_q = jnp.concatenate([qk] * 4, axis=1)
    own_seq = iota(wide_q.shape, 1) // 128 == (iota(wide_q.shape, 0) // heads) % 4
    wide_q = jnp.where(own_seq, wide_q.astype(f32), 0.0).astype(bf16)
    for g in range(rows // 4):
        for n in range(4 * g, 4 * g + 4):
            cache_c[n].wait()
        keys = jnp.concatenate([cache_v[n] for n in range(4 * g, 4 * g + 4)], axis=1)
        s_v[16 * g : 16 * g + 16, :] = dot(wide_q[16 * g : 16 * g + 16, :], keys, ((1,), (1,)))
    for c in small[6:]:
        c.wait()
    sends = copy_all([(joined_v, joined_hbm.at[j]) for j in range(joined_hbm.shape[0])], sem_j)
    rid = iota((hr, 128), 0)
    lens = jnp.zeros((hr, 128), jnp.int32)
    bias = jnp.zeros((hr, 128), f32)
    len_c.wait()
    bias_c.wait()
    for n in range(rows):
        lens = jnp.where(rid // heads == n, len_ref[n], lens)
    for h in range(heads):
        bias = jnp.where(rid % heads == h, bias_ref[h], bias)
    later = ((iota((128, 256), 0) > iota((128, 256), 1)) | (iota((128, 256), 1) >= 128)).astype(bf16)
    blocks = span // 128
    usable, own, pieces = [], [], []
    for b in range(blocks):
        z = s_v[:, b * 128 : (b + 1) * 128] + bias
        ok = (iota((hr, 128), 1) + b * 128) < lens
        soft = jnp.log1p(jnp.exp(-jnp.abs(z)))
        usable.append(ok)
        own.append(jnp.minimum(z, 0.0) - soft)
        pieces.append(three_pieces(jnp.where(ok, -(jnp.maximum(z, 0.0) + soft), 0.0)))
    high, middle, low = [jnp.concatenate([p[i] for p in pieces], axis=0) for i in range(3)]
    both = (dot(low, later) + dot(middle, later)) + dot(high, later)
    beyond = jnp.zeros((hr, 128), f32)
    weights = [None] * blocks
    for b in range(blocks - 1, -1, -1):
        mine = both[b * hr : (b + 1) * hr, :]
        behind = mine[:, :128] + beyond
        beyond = beyond + mine[:, 128:]
        weights[b] = jnp.where(usable[b], jnp.exp(own[b] + behind), 0.0).astype(bf16)
    outs = []
    r16o = iota((16, 128), 0) // heads
    for g in range(rows // 4):
        pg = jnp.concatenate([w[16 * g : 16 * g + 16, :] for w in weights], axis=1)
        acc = None
        for i in range(4):
            o = dot(pg, cache_v[4 * g + i])
            acc = o if acc is None else jnp.where(r16o == i, o, acc)
        outs.append(acc)
    o = jnp.concatenate(outs, axis=0).astype(bf16)
    unfold = ((iota((128, 256), 0) - HEAD_DIM) == (iota((128, 256), 1) % HEAD_DIM)).astype(bf16)
    ox = jnp.where(lane // HEAD_DIM == row % heads, dot(o, unfold), 0.0).astype(bf16)
    collect = (iota((rows, hr), 1) // heads == iota((rows, hr), 0)).astype(bf16)
    heads_out = dot(collect, ox).astype(bf16)
    wo_c.wait()
    part_ref[...] = dot(heads_out, wo_v[...]).astype(bf16)
    for c in sends:
        c.wait()


def attend(tokens, lengths, cache, gain, wq, bias, wo, shared_gate, shared_up):
    rows, d = tokens.shape
    joined = (shared_gate.shape[0], 2 * shared_gate.shape[1])
    return call(
        attend_kernel, [((rows, d), bf16), ((8, *joined), bf16)],
        (lengths, bias, tokens, gain.reshape(1, -1), cache, wq, wo, shared_gate, shared_up),
        in_specs=[HBM] * 9, out_specs=[VM, HBM],
        scratch=[
            pltpu.SMEM(lengths.shape, jnp.int32), pltpu.SMEM(bias.shape, f32),
            pltpu.VMEM(tokens.shape, bf16), pltpu.VMEM((1, d), f32),
            pltpu.VMEM(cache.shape, bf16), pltpu.VMEM(wq.shape, bf16), pltpu.VMEM(wo.shape, bf16),
            pltpu.VMEM((4 * rows, cache.shape[1]), f32),
            pltpu.VMEM(joined, bf16),
            pltpu.SemaphoreType.DMA((rows,)), pltpu.SemaphoreType.DMA((6,)), pltpu.SemaphoreType.DMA((10,)),
        ],
        limit_mib=16,
    )


def slots_of(routes_ref, rw_ref):
    top, rows = routes_ref.shape
    experts = 64
    hits = jnp.zeros((experts, rows), f32)
    weight = jnp.zeros((experts, rows), f32)
    which = iota((experts, rows), 0)
    for j in range(top):
        same = which == routes_ref[j : j + 1, :]
        hits = jnp.where(same, 1.0, hits)
        if rw_ref is not None:
            weight = jnp.where(same, rw_ref[j : j + 1, :], weight)
    before = (iota((rows, rows), 0) < iota((rows, rows), 1)).astype(bf16)
    rank = dot(hits.astype(bf16), before)
    slots = [jnp.where((hits > 0.5) & (rank == k), 1.0, 0.0) for k in range(CAP)]
    spread = (iota((8 * experts, experts), 0) // 8 == iota((8 * experts, experts), 1)).astype(bf16)
    return slots, weight, spread


def pick_kernel(routes_ref, pick_ref):
    rows = routes_ref.shape[1]
    slots, _, spread = slots_of(routes_ref, None)
    n = spread.shape[0]
    tile = (iota((rows, 8 * rows), 0) == iota((rows, 8 * rows), 1) % rows).astype(bf16)
    here = (iota((n, 8 * rows), 0) % 8) == (iota((n, 8 * rows), 1) // rows)
    for k in range(CAP):
        wide = dot(slots[k].astype(bf16), tile).astype(bf16)
        full = jnp.where(here, dot(spread, wide), 0.0)
        pick_ref[:, k * 8 * rows : (k + 1) * 8 * rows] = full.astype(bf16)


def mix_kernel(part_ref, tok_ref, p0, p1, p2, p3, gain_ref, pick_ref, normed_hbm, residual_hbm, sent_hbm,
               normed_v, residual_v, sent_v, sems):
    rows, d = tok_ref.shape
    wide = d // 8
    quarter = residual_hbm.shape[1]
    total = (p0[...].astype(f32) + p1[...].astype(f32)) + (p2[...].astype(f32) + p3[...].astype(f32))
    residual = tok_ref[...].astype(f32) + total
    residual_v[...] = residual
    ms = jnp.mean(residual * residual, axis=-1, keepdims=True)
    normed = (residual * lax.rsqrt(ms + EPS) * gain_ref[...]).astype(bf16)
    normed_v[...] = normed
    mine = pl.ds(pl.multiple_of(part_ref[0] * quarter, quarter), quarter)
    copies = copy_all([(normed_v, normed_hbm), (residual_v.at[:, mine], residual_hbm)], sems)
    stacked = jnp.concatenate([normed[:, r * wide : (r + 1) * wide] for r in range(8)], axis=0)
    for k in range(CAP):
        pick = pick_ref[:, k * 8 * rows : (k + 1) * 8 * rows]
        cols = slice(k * wide, (k + 1) * wide)
        sent_v[:, cols] = dot(pick, stacked).astype(bf16)
        copies += copy_all([(sent_v.at[:, cols], sent_hbm.at[:, cols])], sems, 2 + k)
    for c in copies:
        c.wait()


def cut_kernel(part_ref, down_hbm, shared_hbm, o0, o1, o2, o3, all_v, sems):
    outs = (o0, o1, o2, o3)
    quarter = o0.shape[1]
    f = down_hbm.shape[1]
    first = copy_all([(down_hbm.at[0], all_v.at[:f, :]), (shared_hbm, all_v.at[f:, :])], sems, 4)
    for c in first:
        c.wait()
    pairs = []
    for k in (1, 3, 2, 0):
        cols = pl.ds(pl.multiple_of(((part_ref[0] + k) % 4) * quarter, quarter), quarter)
        pairs.append((all_v.at[:, cols], outs[k]))
    for c in copy_all(pairs, sems):
        c.wait()


def silu(v):
    return v / (1.0 + jnp.exp(-v))


def shared_kernel(ep_ref, normed_ref, b0, b1, b2, b3, b4, b5, b6, b7, hidden_ref):
    blocks = (b0, b1, b2, b3, b4, b5, b6, b7)
    rows, d = normed_ref.shape
    wide = d // 8
    ep = ep_ref[0]
    y = (ep // 2) % 4
    c = ep % 2
    lane = iota((wide, wide), 1)
    there = ((y + 4 - lane // 64) % 4) * 64 + ((c + lane // 32) % 2) * 32 + lane % 32
    order = (iota((wide, wide), 0) == there).astype(bf16)
    cols = [normed_ref[:, j * wide : (j + 1) * wide] for j in range(8)]
    mine = dot(jnp.concatenate(cols, axis=0), order).astype(bf16)
    n = b0.shape[2]
    acc = jnp.zeros((rows, n), f32)
    for j in range(8):
        w = jnp.concatenate([b[j] for b in blocks], axis=0)
        acc = acc + dot(mine[j * rows : (j + 1) * rows, :], w)
    half = n // 2
    hidden = silu(acc[:, :half]) * acc[:, half:]
    hidden_ref[...] = hidden.astype(bf16)


def expert_kernel(arrived_ref, wg_ref, wu_ref, sh_ref, hidden_ref, x_v):
    n = arrived_ref.shape[0]
    peers = n // 8
    wide = arrived_ref.shape[1] // CAP
    a = iota((n, n), 0)
    b = iota((n, n), 1)
    order = ((b // 8 == a % peers) & (b % 8 == a // peers)).astype(bf16)
    sorted_rows = dot(order, arrived_ref[...]).astype(bf16)
    for r in range(8):
        for k in range(CAP):
            x_v[k * peers : (k + 1) * peers, r * wide : (r + 1) * wide] = sorted_rows[
                r * peers : (r + 1) * peers, k * wide : (k + 1) * wide
            ]
    x = x_v[...]
    gate = dot(x, wg_ref[0])
    up = dot(x, wu_ref[0])
    m = CAP * peers
    hidden_ref[:m, :] = (silu(gate) * up).astype(bf16)
    hidden_ref[m:, : sh_ref.shape[1]] = sh_ref[...]
    hidden_ref[m:, sh_ref.shape[1] :] = jnp.zeros((sh_ref.shape[0], hidden_ref.shape[1] - sh_ref.shape[1]), bf16)


def down_kernel(h0, h1, h2, h3, w0, w1, w2, w3, back_ref, w_v, sems):
    n = back_ref.shape[0]
    peers = n // 8
    f = h0.shape[1]
    m = CAP * peers
    copies = copy_all([(w.at[:f, :], w_v.at[k]) for k, w in enumerate((w0, w1, w2, w3))], sems)
    a = iota((n, 2 * m), 0)
    b = iota((n, 2 * m), 1)
    order = ((a % 8 == b // peers) & (a // 8 == b % peers)).astype(bf16)
    acc = None
    for k, h in enumerate((h0, h1, h2, h3)):
        copies[k].wait()
        part = dot(h[:m, :], w_v[k])
        acc = part if acc is None else acc + part
    out = acc.astype(bf16)
    half = out.shape[1] // 2
    pieces = [
        out[k * peers : (k + 1) * peers, h * half : (h + 1) * half] for k in range(CAP) for h in range(2)
    ]
    rhs = jnp.concatenate(pieces, axis=0)
    back_ref[...] = dot(order, rhs).astype(bf16)


def side_kernel(routes_ref, rw_ref, tok_hbm, gain_ref, kw_hbm, vw_hbm, mixed_hbm, gv_ref,
                mix_ref, kv_ref, gate_ref, tok_ref, both_ref, mixed_ref, sems):
    rows = tok_ref.shape[0]
    n = kw_hbm.shape[0]
    copies = copy_all([(tok_hbm, tok_ref), (kw_hbm, both_ref.at[:n, :]), (vw_hbm, both_ref.at[n:, :]),
                       (mixed_hbm, mixed_ref)], sems)
    for c in copies:
        c.wait()
    x = tok_ref[...].astype(f32)
    ms = jnp.mean(x * x, axis=-1, keepdims=True)
    normed = (x * lax.rsqrt(ms + EPS) * gain_ref[...]).astype(bf16)
    kv_ref[...] = dot(normed, both_ref[...], ((1,), (1,))).astype(bf16)
    slots, weight, spread = slots_of(routes_ref, rw_ref)
    lane = iota((rows, spread.shape[0]), 1) % 8
    mixed = [jnp.zeros(lane.shape, f32) for _ in range(3)]
    for k in range(CAP):
        for i, piece in enumerate(three_pieces(slots[k] * weight)):
            mixed[i] = jnp.where(lane // 2 == k, dot(piece, spread, ((0,), (1,))), mixed[i])
    for h in range(2):
        for i in range(3):
            row = (h * 3 + i) * rows
            mix_ref[row : row + rows, :] = jnp.where(lane % 2 == h, mixed[i], 0.0).astype(bf16)
    total = jnp.zeros((rows, 128), f32)
    for j in range(gv_ref.shape[0]):
        total = total + mixed_ref[:, j * 128 : (j + 1) * 128].astype(f32) * gv_ref[j : j + 1, :].astype(f32)
    logit = jnp.sum(total, axis=-1, keepdims=True)
    gate_ref[...] = jnp.broadcast_to(1.0 / (1.0 + jnp.exp(-logit)), gate_ref.shape)


def base_kernel(residual_hbm, gate_ref, s0, s1, s2, s3, w0, w1, w2, w3, base_ref, residual_v, w_v, sems):
    at = w0.shape[0] - w_v.shape[1]
    copies = copy_all([(w.at[at:, :], w_v.at[k]) for k, w in enumerate((w0, w1, w2, w3))], sems)
    copies += copy_all([(residual_hbm, residual_v)], sems, 4)
    acc = None
    for k, h in enumerate((s0, s1, s2, s3)):
        copies[k].wait()
        part = dot(h[h.shape[0] - base_ref.shape[0] :, : w_v.shape[1]], w_v[k])
        acc = part if acc is None else acc + part
    copies[4].wait()
    base_ref[...] = residual_v[...] + gate_ref[:, :1] * acc


def final_kernel(back_ref, mix_ref, base_ref, out_ref):
    rows = out_ref.shape[0]
    half = out_ref.shape[1] // 2
    for h in range(2):
        r = dot(mix_ref[h * 3 * rows : (h + 1) * 3 * rows, :], back_ref[...])
        routed = (r[2 * rows :] + r[rows : 2 * rows]) + r[:rows]
        cols = slice(h * half, (h + 1) * half)
        out_ref[:, cols] = (base_ref[:, cols] + routed).astype(bf16)


def around(k, size):
    return [(i, (i + k) % size) for i in range(size)]


def after(value, *deps):
    return lax.optimization_barrier((value, *deps))[0]


def shards(
    tokens, lengths, cache, attn_gain, query_weight, key_weight, value_weight, stick_bias, out_weight,
    ffn_gain, routes, route_weights, expert_gate, expert_up, expert_down, shared_gate, shared_up,
    shared_down, gate_vector,
):
    ntp = lax.axis_size("tp")
    nep = lax.axis_size("ep")
    rows, d = tokens.shape
    quarter = d // ntp
    part = lax.axis_index("tp").reshape(1)
    n_pick = 8 * nep

    def shift(value, dz, dy, dc):
        perm = []
        for i in range(nep):
            z, y, c = i // 8, i // 2 % 4, i % 2
            perm.append((i, (z + dz) % (nep // 8) * 8 + (y + dy) % 4 * 2 + (c + dc) % 2))
        return lax.ppermute(value, "ep", perm)

    partial, copies = attend(
        tokens, lengths, cache, attn_gain, query_weight, stick_bias, out_weight, shared_gate, shared_up
    )
    groups = [[z * 8 + r for z in range(nep // 8)] for r in range(8)]
    others = [lax.ppermute(partial, "tp", around(k, ntp)) for k in (2, 1, 3)]
    column = lax.all_to_all(copies, "ep", 0, 0, axis_index_groups=groups, tiled=True)
    (pick,) = call(pick_kernel, [((n_pick, CAP * 8 * rows), bf16)], (after(routes.T, partial),))
    normed_mix, residual, sent = call(
        mix_kernel, [((rows, d), bf16), ((rows, quarter), f32), ((n_pick, CAP * d // 8), bf16)],
        (part, tokens, partial, *others, ffn_gain.reshape(1, -1), pick),
        in_specs=[SM] + [VM] * 7, out_specs=[HBM] * 3,
        scratch=[pltpu.VMEM((rows, d), bf16), pltpu.VMEM((rows, d), f32),
                 pltpu.VMEM((n_pick, CAP * d // 8), bf16), pltpu.SemaphoreType.DMA((5,))],
    )
    arrived = lax.all_to_all(sent.reshape(nep, 8, -1), "ep", 0, 0, tiled=True)
    arrived = arrived.reshape(n_pick, -1)
    column = after(column, sent)
    planes = [column] + [shift(column, 0, k, 0) for k in range(1, 4)]
    blocks = []
    for block in planes:
        blocks += [block, shift(block, 0, 0, 1)]
    f = expert_down.shape[1] + shared_down.shape[0]
    cuts = call(
        cut_kernel, [((f, quarter), bf16)] * 4, (part, after(expert_down, sent), shared_down),
        in_specs=[SM, HBM, HBM], out_specs=[HBM] * 4,
        scratch=[pltpu.VMEM((f, d), bf16), pltpu.SemaphoreType.DMA((6,))],
    )
    downs = [cuts[0]] + [lax.ppermute(cuts[k], "tp", around(k, ntp)) for k in range(1, ntp)]
    mix, new_kv, mix_gate = call(
        side_kernel,
        [((6 * rows, n_pick), bf16), ((rows, 2 * HEAD_DIM), bf16), ((rows, 128), f32)],
        (routes.T, route_weights.T, after(tokens, sent), attn_gain.reshape(1, -1), key_weight.T, value_weight.T,
         normed_mix, gate_vector.reshape(-1, 128)),
        in_specs=[VM, VM, HBM, VM, HBM, HBM, HBM, VM],
        scratch=[pltpu.VMEM((rows, d), bf16), pltpu.VMEM((2 * HEAD_DIM, d), bf16), pltpu.VMEM((rows, d), bf16),
                 pltpu.SemaphoreType.DMA((4,))],
    )
    (shared_hidden,) = call(
        shared_kernel, [((rows, shared_gate.shape[1]), bf16)],
        (lax.axis_index("ep").reshape(1), normed_mix, *blocks), in_specs=[SM] + [VM] * 9,
    )
    m = CAP * nep
    (hidden,) = call(
        expert_kernel, [((m + rows, expert_gate.shape[2]), bf16)],
        (arrived, expert_gate, expert_up, shared_hidden), scratch=[pltpu.VMEM((m, d), bf16)],
    )
    hiddens = [hidden] + [lax.ppermute(hidden, "tp", around(k, ntp)) for k in range(1, ntp)]
    (back,) = call(
        down_kernel, [((n_pick, quarter // 2), bf16)], (*hiddens, *downs), in_specs=[VM] * 4 + [HBM] * 4,
        scratch=[pltpu.VMEM((ntp, expert_down.shape[1], quarter), bf16), pltpu.SemaphoreType.DMA((4,))],
    )
    returned = lax.all_to_all(back.reshape(nep, 8, -1), "ep", 0, 0, tiled=True)
    returned = returned.reshape(n_pick, -1)
    (base,) = call(
        base_kernel, [((rows, quarter), f32)], (after(residual, back), mix_gate, *hiddens, *downs),
        in_specs=[HBM] + [VM] * 5 + [HBM] * 4,
        scratch=[pltpu.VMEM((rows, quarter), f32), pltpu.VMEM((ntp, shared_down.shape[0], quarter), bf16),
                 pltpu.SemaphoreType.DMA((5,))],
    )
    (layer_out,) = call(final_kernel, [((rows, quarter), bf16)], (returned, mix, base))
    return (layer_out, new_kv)


def solution(mesh):
    placed = (
        P("ep", None), P("ep"), P("ep", None, "tp"), P(), P(None, "tp"), P(None, "tp"), P(None, "tp"),
        P("tp"), P("tp", None), P(), P("ep", None), P("ep", None), P("ep", None, "tp"),
        P("ep", None, "tp"), P("ep", "tp", None), P("ep", "tp"), P("ep", "tp"), P("tp", None), P(),
    )

    return jax.shard_map(shards, mesh=mesh, in_specs=placed, out_specs=(P("ep", "tp"), P("ep", "tp")), check_vma=False)
```

time: 138 us -> 102 us (0.74)
  waiting for transfers between devices: 42.7 us -> 21.9 us
  local copies, waits for them, and re-layouts: 24.3 us -> 4 us
  Pallas kernels: 14.7 us -> 20.8 us
    ppermute x14 -> x7, waiting for transfers between devices: 24.6 us -> 2.16 us  [shift(): return lax.ppermute(value, 'ep', perm)]
    unnamed x73 -> x26, local copies, waits for them, and re-layouts: 19.8 us -> 4 us
    ppermute x14 -> x7, starting transfers between devices: 23.5 us -> 11.1 us  [shift(): return lax.ppermute(value, 'ep', perm)]
    all_to_all x1 -> x2, starting transfers between devices: 7.27 us -> 18.4 us  [the longest x1 9.23 us: shards(): returned = lax.all_to_all(back.reshape(nep, 8, -1), 'ep', 0, 0, tiled=True)]
    pallas_call x7 -> x10, Pallas kernels: 14.7 us -> 20.8 us  [call(): pl.pallas_call(kernel, out_shape=tuple(shapes), in_specs=in_specs, out_sp...]
    dynamic_slice x2 -> x0, local copies, waits for them, and re-layouts: 3.2 us -> none  [the longest x1 2.43 us: shards(): lax.dynamic_slice_in_dim(down_all, (part + k) % ntp * quarter, quarter, 1)]
    all_to_all x1, starting transfers between devices: 10.1 us -> 12.6 us  [shards(): arrived = lax.all_to_all(sent.reshape(nep, 8, -1), 'ep', 0, 0, tiled=True)]
    ppermute x3, waiting for transfers between devices: 0.43 us -> 2.84 us  [shards(): others = [lax.ppermute(partial, 'tp', around(k, ntp)) for k in (2, 1, 3)]]
  transfers between devices with their start and end apart: 25 -> 19, of which waited for: 12 -> 10; matrix products, arithmetic and copies ran while one was open for 8% -> 0% of each run, Pallas kernels for 3% -> 10%
where the time goes in v2:
time: 102 us; the launch traced here: 101 us
  starting transfers between devices  53.5 us (52%)
  waiting for transfers between devices  21.9 us (21%)
  Pallas kernels  20.8 us (20%)
  local copies, waits for them, and re-layouts  4 us (4%)
    pallas_call x10, Pallas kernels, call(): pl.pallas_call(kernel, out_shape=tuple(shapes), in_specs=in_specs, out_sp...  20.8 us
    all_to_all x1, starting transfers between devices, shards(): arrived = lax.all_to_all(sent.reshape(nep, 8, -1), 'ep', 0, 0, tiled=True)  12.6 us
    ppermute x7, starting transfers between devices, shift(): return lax.ppermute(value, 'ep', perm)  11.1 us
    all_to_all x1, waiting for transfers between devices, shards(): returned = lax.all_to_all(back.reshape(nep, 8, -1), 'ep', 0, 0, tiled=True)  9.5 us
    all_to_all x1, starting transfers between devices, shards(): returned = lax.all_to_all(back.reshape(nep, 8, -1), 'ep', 0, 0, tiled=True)  9.23 us
    all_to_all x1, starting transfers between devices, shards(): lax.all_to_all(copies, 'ep', 0, 0, axis_index_groups=groups, tiled=True)  9.15 us
    ppermute x3, waiting for transfers between devices, shards(): lax.ppermute(hidden, 'tp', around(k, ntp))  7.41 us
    ppermute x3, starting transfers between devices, shards(): others = [lax.ppermute(partial, 'tp', around(k, ntp)) for k in (2, 1, 3)]  4.21 us
  transfers between devices with their start and end apart: 19, of which 10 were waited for; matrix products, arithmetic and copies ran while one was open for 0% of the time, Pallas kernels for 10%

profile of v2, /device:TPU:1, one launch (start us, length us, event | category | flops | bytes accessed | tf_op | source)
XLA Modules:
  0.0 101.1 jit_solution(3415401552629293578)
XLA Ops:
  0.7 6.9 %shard_map.194 = (bf16[16,2048]{1,0:T(8,128)(2,1)S(1)}, bf16[8,32,256]{2,1,0:T(8,128)(2,1)}) custom-call(s32[16]{0:T(128)} %len_hbm.1, f32[4]{0:T(128)} %bias_hbm.1, bf16[16,2048]{1,0:T(8,128)(2,1)} %tok_hbm.2, f32[1,2048]{1,0:T(1,128)} %bitcast.15, bf16[16,1024,128]{2,1,0:T(8,128)(2,1)} %cache_hbm.1, bf16[2048,256]{1,0:T(8,128)(2,1)} %wq_hbm.1, ...), custom_call_target="tpu_custom_call" | custom-call | tf_op jit(solution)/shard_map/pallas_call | solution.py:46
  7.6 9.1 %all-to-all-start.1 = ((bf16[8,32,256]{2,1,0:T(8,128)(2,1)}), bf16[8,32,256]{2,1,0:T(8,128)(2,1)S(1)}, u32[]{:S(2)}, u32[]{:S(2)}) async-start(bf16[8,32,256]{2,1,0:T(8,128)(2,1)} %get-tuple-element.23), calls=%async_computation.1 | async-start | bytes 262144 | tf_op jit(solution)/shard_map/all_to_all | solution.py:405
  16.8 2.5 %collective-permute-start.2 = (bf16[16,2048]{1,0:T(8,128)(2,1)S(1)}, bf16[16,2048]{1,0:T(8,128)(2,1)S(1)}, u32[]{:S(2)}, u32[]{:S(2)}) collective-permute-start(bf16[16,2048]{1,0:T(8,128)(2,1)S(1)} %get-tuple-element.19.p0), channel_id=1, source_target_pairs={{0,3},{1,0},{2,1},{3,2},{4,7},{5,4},{6,5},{7,6},{8,11},{9,8},{10,9... | collective-permute-start | bytes 196616 | tf_op jit(solution)/shard_map/ppermute | solution.py:404
  19.3 1.7 %collective-permute-start = (bf16[16,2048]{1,0:T(8,128)(2,1)S(1)}, bf16[16,2048]{1,0:T(8,128)(2,1)S(1)}, u32[]{:S(2)}, u32[]{:S(2)}) collective-permute-start(bf16[16,2048]{1,0:T(8,128)(2,1)S(1)} %get-tuple-element.19.p0), channel_id=1, source_target_pairs={{0,2},{1,3},{2,0},{3,1},{4,6},{5,7},{6,4},{7,5},{8,10},{9,11},{10,... | collective-permute-start | bytes 196616 | tf_op jit(solution)/shard_map/ppermute | solution.py:404
  21.6 2.8 %collective-permute-done.1.p2 = bf16[16,2048]{1,0:T(8,128)(2,1)S(1)} collective-permute-done((bf16[16,2048]{1,0:T(8,128)(2,1)S(1)}, bf16[16,2048]{1,0:T(8,128)(2,1)S(1)}, u32[]{:S(2)}, u32[]{:S(2)}) %collective-permute-start.1) | collective-permute-done | bytes 65568 | tf_op jit(solution)/shard_map/ppermute | solution.py:404
  24.5 1.4 %shard_map.196 = (bf16[16,2048]{1,0:T(8,128)(2,1)}, f32[16,512]{1,0:T(8,128)}, bf16[512,768]{1,0:T(8,128)(2,1)}) custom-call(s32[1]{0:T(128)} %bitcast.part_ref, bf16[16,2048]{1,0:T(8,128)(2,1)S(1)} %copy-done.2, bf16[16,2048]{1,0:T(8,128)(2,1)S(1)} %get-tuple-element.19.p0, bf16[16,2048]{1,0:T(8,128)(2,1)S(1)} %collective-permute-done.p1, ...), custom_call_target="tpu_custom_call" | custom-call | tf_op jit(solution)/shard_map/pallas_call | solution.py:46
  25.9 12.6 %all-to-all-start = ((bf16[64,8,768]{2,1,0:T(8,128)(2,1)}), bf16[64,8,768]{2,1,0:T(8,128)(2,1)S(1)}, u32[]{:S(2)}, u32[]{:S(2)}) async-start(bf16[64,8,768]{2,1,0:T(8,128)(2,1)} %bitcast.22), calls=%async_computation | async-start | bytes 1572864 | tf_op jit(solution)/shard_map/all_to_all | solution.py:414
  38.6 2.6 %collective-permute-start.8 = (bf16[8,32,256]{2,1,0:T(8,128)(2,1)S(1)}, bf16[8,32,256]{2,1,0:T(8,128)(2,1)S(1)}, u32[]{:S(2)}, u32[]{:S(2)}) collective-permute-start(bf16[8,32,256]{2,1,0:T(8,128)(2,1)S(1)} %all-to-all-done.1.b0), channel_id=1, source_target_pairs={{0,24},{4,28},{8,0},{12,4},{16,8},{20,12},{24,16},{28,20},{32,56},... | collective-permute-start | bytes 393224 | tf_op jit(solution)/shard_map/ppermute | solution.py:398
  42.4 2.6 %shard_map.199 = (bf16[384,512]{1,0:T(8,128)(2,1)}, bf16[384,512]{1,0:T(8,128)(2,1)}, bf16[384,512]{1,0:T(8,128)(2,1)}, bf16[384,512]{1,0:T(8,128)(2,1)}) custom-call(s32[1]{0:T(128)} %bitcast.part_ref, bf16[1,256,2048]{2,1,0:T(8,128)(2,1)} %down_hbm, bf16[128,2048]{1,0:T(8,128)(2,1)} %shared_hbm.1), custom_call_target="tpu_custom_call" | custom-call | tf_op jit(solution)/shard_map/pallas_call | solution.py:46
  45.1 3.7 %collective-permute-start.14 = (bf16[384,512]{1,0:T(8,128)(2,1)}, bf16[384,512]{1,0:T(8,128)(2,1)}, u32[]{:S(2)}, u32[]{:S(2)}) collective-permute-start(bf16[384,512]{1,0:T(8,128)(2,1)} %get-tuple-element.28), channel_id=1, source_target_pairs={{0,2},{1,3},{2,0},{3,1},{4,6},{5,7},{6,4},{7,5},{8,10},{9,11},{10,... | collective-permute-start | bytes 1179656 | tf_op jit(solution)/shard_map/ppermute | solution.py:427
  49.1 6.3 %collective-permute-start.3 = (bf16[8,32,256]{2,1,0:T(8,128)(2,1)S(1)}, bf16[8,32,256]{2,1,0:T(8,128)(2,1)S(1)}, u32[]{:S(2)}, u32[]{:S(2)}) collective-permute-start(bf16[8,32,256]{2,1,0:T(8,128)(2,1)S(1)} %all-to-all-done.1.b0), channel_id=1, source_target_pairs={{0,4},{4,0},{8,12},{12,8},{16,20},{20,16},{24,28},{28,24},{32,36},... | collective-permute-start | bytes 393224 | tf_op jit(solution)/shard_map/ppermute | solution.py:398
  58.7 1.0 collective-permute-done.5.b3
  60.5 0.9 copy-done.5
  62.3 1.4 %shard_map.197.sh_ref = bf16[16,128]{1,0:T(8,128)(2,1)S(1)} custom-call(s32[1]{0:T(128)} %bitcast.6.ep_ref, bf16[16,2048]{1,0:T(8,128)(2,1)S(1)} %copy-done.3, bf16[8,32,256]{2,1,0:T(8,128)(2,1)S(1)} %all-to-all-done.1.b0, bf16[8,32,256]{2,1,0:T(8,128)(2,1)S(1)} %copy-done.5, bf16[8,32,256]{2,1,0:T(8,128)(2,1)S(1)} %collective-permute-done.4.b2, ...), custom_call_target="tpu_custom_call" | custom-call | tf_op jit(solution)/shard_map/pallas_call | solution.py:46
  63.8 1.0 shard_map.198.h0.s0
  64.8 2.6 %collective-permute-start.12 = (bf16[208,256]{1,0:T(8,128)(2,1)S(1)}, bf16[208,256]{1,0:T(8,128)(2,1)S(1)}, u32[]{:S(2)}, u32[]{:S(2)}) collective-permute-start(bf16[208,256]{1,0:T(8,128)(2,1)S(1)} %shard_map.198.h0.s0), channel_id=1, source_target_pairs={{0,3},{1,0},{2,1},{3,2},{4,7},{5,4},{6,5},{7,6},{8,11},{9,8},{10,9... | collective-permute-start | bytes 319496 | tf_op jit(solution)/shard_map/ppermute | solution.py:446
  68.1 3.6 %collective-permute-done.12.h3.s3 = bf16[208,256]{1,0:T(8,128)(2,1)S(1)} collective-permute-done((bf16[208,256]{1,0:T(8,128)(2,1)S(1)}, bf16[208,256]{1,0:T(8,128)(2,1)S(1)}, u32[]{:S(2)}, u32[]{:S(2)}) %collective-permute-start.12) | collective-permute-done | bytes 106528 | tf_op jit(solution)/shard_map/ppermute | solution.py:446
  71.7 1.2 %collective-permute-done.11.h2.s2 = bf16[208,256]{1,0:T(8,128)(2,1)S(1)} collective-permute-done((bf16[208,256]{1,0:T(8,128)(2,1)S(1)}, bf16[208,256]{1,0:T(8,128)(2,1)S(1)}, u32[]{:S(2)}, u32[]{:S(2)}) %collective-permute-start.11) | collective-permute-done | bytes 106528 | tf_op jit(solution)/shard_map/ppermute | solution.py:446
  72.9 2.6 %collective-permute-done.10.h1.s1 = bf16[208,256]{1,0:T(8,128)(2,1)S(1)} collective-permute-done((bf16[208,256]{1,0:T(8,128)(2,1)S(1)}, bf16[208,256]{1,0:T(8,128)(2,1)S(1)}, u32[]{:S(2)}, u32[]{:S(2)}) %collective-permute-start.10) | collective-permute-done | bytes 106528 | tf_op jit(solution)/shard_map/ppermute | solution.py:446
  75.5 2.5 %shard_map.200 = bf16[512,256]{1,0:T(8,128)(2,1)} custom-call(bf16[208,256]{1,0:T(8,128)(2,1)S(1)} %shard_map.198.h0.s0, bf16[208,256]{1,0:T(8,128)(2,1)S(1)} %collective-permute-done.10.h1.s1, bf16[208,256]{1,0:T(8,128)(2,1)S(1)} %collective-permute-done.11.h2.s2, bf16[208,256]{1,0:T(8,128)(2,1)S(1)} %collective-permute-done.12.h3.s3, ...), custom_call_target="tpu_custom_call" | custom-call | tf_op jit(solution)/shard_map/pallas_call | solution.py:46
  78.0 9.2 %all-to-all-start.2 = ((bf16[64,8,256]{2,1,0:T(8,128)(2,1)}), bf16[64,8,256]{2,1,0:T(8,128)(2,1)S(1)}, u32[]{:S(2)}, u32[]{:S(2)}) async-start(bf16[64,8,256]{2,1,0:T(8,128)(2,1)} %bitcast.7), calls=%async_computation.2 | async-start | bytes 524288 | tf_op jit(solution)/shard_map/all_to_all | solution.py:451
  87.3 2.2 %shard_map.201 = (bf16[96,512]{1,0:T(8,128)(2,1)S(1)}, bf16[16,128]{1,0:T(8,128)(2,1)}, f32[16,128]{1,0:T(8,128)S(1)}) custom-call(s32[6,16]{1,0:T(8,128)S(1)} %bitcast.18, f32[6,16]{1,0:T(8,128)S(1)} %bitcast.20, bf16[16,2048]{1,0:T(8,128)(2,1)} %tok_hbm.2, f32[1,2048]{1,0:T(1,128)S(1)} %bitcast.16, bf16[64,2048]{1,0:T(8,128)(2,1)} %bitcast.23, ...), custom_call_target="tpu_custom_call" | custom-call | tf_op jit(solution)/shard_map/pallas_call | solution.py:46
  89.5 1.3 %shard_map.202.base_ref = f32[16,512]{1,0:T(8,128)S(1)} custom-call(f32[16,512]{1,0:T(8,128)} %get-tuple-element.33.residual_hbm, f32[16,128]{1,0:T(8,128)S(1)} %get-tuple-element.34.gate_ref, bf16[208,256]{1,0:T(8,128)(2,1)S(1)} %shard_map.198.h0.s0, bf16[208,256]{1,0:T(8,128)(2,1)S(1)} %collective-permute-done.10.h1.s1, ...), custom_call_target="tpu_custom_call" | custom-call | tf_op jit(solution)/shard_map/pallas_call | solution.py:46
  90.8 9.5 %all-to-all-done.2 = bf16[64,8,256]{2,1,0:T(8,128)(2,1)S(1)} async-done(((bf16[64,8,256]{2,1,0:T(8,128)(2,1)}), bf16[64,8,256]{2,1,0:T(8,128)(2,1)S(1)}, u32[]{:S(2)}, u32[]{:S(2)}) %all-to-all-start.2) | async-done | bytes 262176 | tf_op jit(solution)/shard_map/all_to_all | solution.py:451
  (50 shorter events, 8.9 us)
Async XLA Ops:
  7.6 56.1 %copy-start = (bf16[1,2048,256]{2,1,0:T(8,128)(2,1)S(1)}, bf16[1,2048,256]{2,1,0:T(8,128)(2,1)}, u32[]{:S(2)}) copy-start(bf16[1,2048,256]{2,1,0:T(8,128)(2,1)} %wg_ref.1) | copy-start | bytes 3145732
  7.6 56.1 %copy-start.1 = (bf16[1,2048,256]{2,1,0:T(8,128)(2,1)S(1)}, bf16[1,2048,256]{2,1,0:T(8,128)(2,1)}, u32[]{:S(2)}) copy-start(bf16[1,2048,256]{2,1,0:T(8,128)(2,1)} %wu_ref.1) | copy-start | bytes 3145732
  7.6 18.3 %all-to-all-start.1 = ((bf16[8,32,256]{2,1,0:T(8,128)(2,1)}), bf16[8,32,256]{2,1,0:T(8,128)(2,1)S(1)}, u32[]{:S(2)}, u32[]{:S(2)}) async-start(bf16[8,32,256]{2,1,0:T(8,128)(2,1)} %get-tuple-element.23), calls=%async_computation.1 | async-start | bytes 262144 | tf_op jit(solution)/shard_map/all_to_all | solution.py:405
  16.8 4.9 %collective-permute-start.2 = (bf16[16,2048]{1,0:T(8,128)(2,1)S(1)}, bf16[16,2048]{1,0:T(8,128)(2,1)S(1)}, u32[]{:S(2)}, u32[]{:S(2)}) collective-permute-start(bf16[16,2048]{1,0:T(8,128)(2,1)S(1)} %get-tuple-element.19.p0), channel_id=1, source_target_pairs={{0,3},{1,0},{2,1},{3,2},{4,7},{5,4},{6,5},{7,6},{8,11},{9,8},{10,9... | collective-permute-start | bytes 196616 | tf_op jit(solution)/shard_map/ppermute | solution.py:404
  19.3 5.2 %collective-permute-start.1 = (bf16[16,2048]{1,0:T(8,128)(2,1)S(1)}, bf16[16,2048]{1,0:T(8,128)(2,1)S(1)}, u32[]{:S(2)}, u32[]{:S(2)}) collective-permute-start(bf16[16,2048]{1,0:T(8,128)(2,1)S(1)} %get-tuple-element.19.p0), channel_id=1, source_target_pairs={{0,1},{1,2},{2,3},{3,0},{4,5},{5,6},{6,7},{7,4},{8,9},{9,10},{10,1... | collective-permute-start | bytes 196616 | tf_op jit(solution)/shard_map/ppermute | solution.py:404
  19.3 5.2 %collective-permute-start = (bf16[16,2048]{1,0:T(8,128)(2,1)S(1)}, bf16[16,2048]{1,0:T(8,128)(2,1)S(1)}, u32[]{:S(2)}, u32[]{:S(2)}) collective-permute-start(bf16[16,2048]{1,0:T(8,128)(2,1)S(1)} %get-tuple-element.19.p0), channel_id=1, source_target_pairs={{0,2},{1,3},{2,0},{3,1},{4,6},{5,7},{6,4},{7,5},{8,10},{9,11},{10,... | collective-permute-start | bytes 196616 | tf_op jit(solution)/shard_map/ppermute | solution.py:404
  25.9 37.8 %all-to-all-start = ((bf16[64,8,768]{2,1,0:T(8,128)(2,1)}), bf16[64,8,768]{2,1,0:T(8,128)(2,1)S(1)}, u32[]{:S(2)}, u32[]{:S(2)}) async-start(bf16[64,8,768]{2,1,0:T(8,128)(2,1)} %bitcast.22), calls=%async_computation | async-start | bytes 1572864 | tf_op jit(solution)/shard_map/all_to_all | solution.py:414
  38.5 48.7 %copy-start.8 = (f32[2048]{0:T(1024)S(1)}, f32[2048]{0:T(1024)}, u32[]{:S(2)}) copy-start(f32[2048]{0:T(1024)} %param.22) | copy-start | bytes 24580
  38.5 48.7 %copy-start.11 = (f32[16,6]{0,1:T(8,128)S(1)}, f32[16,6]{0,1:T(8,128)}, u32[]{:S(2)}) copy-start(f32[16,6]{0,1:T(8,128)} %param.30) | copy-start | bytes 1156
  38.5 48.7 %copy-start.12 = (bf16[2048]{0:T(1024)(128)(2,1)S(1)}, bf16[2048]{0:T(1024)(128)(2,1)}, u32[]{:S(2)}) copy-start(bf16[2048]{0:T(1024)(128)(2,1)} %param.37) | copy-start | bytes 12292
  38.6 10.2 %collective-permute-start.8 = (bf16[8,32,256]{2,1,0:T(8,128)(2,1)S(1)}, bf16[8,32,256]{2,1,0:T(8,128)(2,1)S(1)}, u32[]{:S(2)}, u32[]{:S(2)}) collective-permute-start(bf16[8,32,256]{2,1,0:T(8,128)(2,1)S(1)} %all-to-all-done.1.b0), channel_id=1, source_target_pairs={{0,24},{4,28},{8,0},{12,4},{16,8},{20,12},{24,16},{28,20},{32,56},... | collective-permute-start | bytes 393224 | tf_op jit(solution)/shard_map/ppermute | solution.py:398
  41.2 7.9 %collective-permute-start.6 = (bf16[8,32,256]{2,1,0:T(8,128)(2,1)S(1)}, bf16[8,32,256]{2,1,0:T(8,128)(2,1)S(1)}, u32[]{:S(2)}, u32[]{:S(2)}) collective-permute-start(bf16[8,32,256]{2,1,0:T(8,128)(2,1)S(1)} %all-to-all-done.1.b0), channel_id=1, source_target_pairs={{0,16},{4,20},{8,24},{12,28},{16,0},{20,4},{24,8},{28,12},{32,48},... | collective-permute-start | bytes 393224 | tf_op jit(solution)/shard_map/ppermute | solution.py:398
  41.8 14.3 %collective-permute-start.4 = (bf16[8,32,256]{2,1,0:T(8,128)(2,1)S(1)}, bf16[8,32,256]{2,1,0:T(8,128)(2,1)S(1)}, u32[]{:S(2)}, u32[]{:S(2)}) collective-permute-start(bf16[8,32,256]{2,1,0:T(8,128)(2,1)S(1)} %all-to-all-done.1.b0), channel_id=1, source_target_pairs={{0,8},{4,12},{8,16},{12,20},{16,24},{20,28},{24,0},{28,4},{32,40},... | collective-permute-start | bytes 393224 | tf_op jit(solution)/shard_map/ppermute | solution.py:398
  44.9 22.5 %collective-permute-start.13 = (bf16[384,512]{1,0:T(8,128)(2,1)}, bf16[384,512]{1,0:T(8,128)(2,1)}, u32[]{:S(2)}, u32[]{:S(2)}) collective-permute-start(bf16[384,512]{1,0:T(8,128)(2,1)} %get-tuple-element.27), channel_id=1, source_target_pairs={{0,1},{1,2},{2,3},{3,0},{4,5},{5,6},{6,7},{7,4},{8,9},{9,10},{10,1... | collective-permute-start | bytes 1179656 | tf_op jit(solution)/shard_map/ppermute | solution.py:427
  45.1 23.0 %collective-permute-start.14 = (bf16[384,512]{1,0:T(8,128)(2,1)}, bf16[384,512]{1,0:T(8,128)(2,1)}, u32[]{:S(2)}, u32[]{:S(2)}) collective-permute-start(bf16[384,512]{1,0:T(8,128)(2,1)} %get-tuple-element.28), channel_id=1, source_target_pairs={{0,2},{1,3},{2,0},{3,1},{4,6},{5,7},{6,4},{7,5},{8,10},{9,11},{10,... | collective-permute-start | bytes 1179656 | tf_op jit(solution)/shard_map/ppermute | solution.py:427
  48.7 19.4 %collective-permute-start.15 = (bf16[384,512]{1,0:T(8,128)(2,1)}, bf16[384,512]{1,0:T(8,128)(2,1)}, u32[]{:S(2)}, u32[]{:S(2)}) collective-permute-start(bf16[384,512]{1,0:T(8,128)(2,1)} %get-tuple-element.29), channel_id=1, source_target_pairs={{0,3},{1,0},{2,1},{3,2},{4,7},{5,4},{6,5},{7,6},{8,11},{9,8},{10,9... | collective-permute-start | bytes 1179656 | tf_op jit(solution)/shard_map/ppermute | solution.py:427
  49.1 7.4 %collective-permute-start.3 = (bf16[8,32,256]{2,1,0:T(8,128)(2,1)S(1)}, bf16[8,32,256]{2,1,0:T(8,128)(2,1)S(1)}, u32[]{:S(2)}, u32[]{:S(2)}) collective-permute-start(bf16[8,32,256]{2,1,0:T(8,128)(2,1)S(1)} %all-to-all-done.1.b0), channel_id=1, source_target_pairs={{0,4},{4,0},{8,12},{12,8},{16,20},{20,16},{24,28},{28,24},{32,36},... | collective-permute-start | bytes 393224 | tf_op jit(solution)/shard_map/ppermute | solution.py:398
  56.1 1.4 %collective-permute-start.9 = (bf16[8,32,256]{2,1,0:T(8,128)(2,1)S(1)}, bf16[8,32,256]{2,1,0:T(8,128)(2,1)S(1)}, u32[]{:S(2)}, u32[]{:S(2)}) collective-permute-start(bf16[8,32,256]{2,1,0:T(8,128)(2,1)S(1)} %collective-permute-done.8.b6), channel_id=1, source_target_pairs={{0,4},{4,0},{8,12},{12,8},{16,20},{20,16},{24,28},{28,24},{32,36},... | collective-permute-start | bytes 393224 | tf_op jit(solution)/shard_map/ppermute | solution.py:398
  57.2 1.5 %collective-permute-start.7 = (bf16[8,32,256]{2,1,0:T(8,128)(2,1)S(1)}, bf16[8,32,256]{2,1,0:T(8,128)(2,1)}, u32[]{:S(2)}, u32[]{:S(2)}) collective-permute-start(bf16[8,32,256]{2,1,0:T(8,128)(2,1)S(1)} %collective-permute-done.6.b4), channel_id=1, source_target_pairs={{0,4},{4,0},{8,12},{12,8},{16,20},{20,16},{24,28},{28,24},{32,36},... | collective-permute-start | bytes 393224 | tf_op jit(solution)/shard_map/ppermute | solution.py:398
  58.2 1.5 %collective-permute-start.5 = (bf16[8,32,256]{2,1,0:T(8,128)(2,1)S(1)}, bf16[8,32,256]{2,1,0:T(8,128)(2,1)}, u32[]{:S(2)}, u32[]{:S(2)}) collective-permute-start(bf16[8,32,256]{2,1,0:T(8,128)(2,1)S(1)} %collective-permute-done.4.b2), channel_id=1, source_target_pairs={{0,4},{4,0},{8,12},{12,8},{16,20},{20,16},{24,28},{28,24},{32,36},... | collective-permute-start | bytes 393224 | tf_op jit(solution)/shard_map/ppermute | solution.py:398
  64.8 6.9 %collective-permute-start.12 = (bf16[208,256]{1,0:T(8,128)(2,1)S(1)}, bf16[208,256]{1,0:T(8,128)(2,1)S(1)}, u32[]{:S(2)}, u32[]{:S(2)}) collective-permute-start(bf16[208,256]{1,0:T(8,128)(2,1)S(1)} %shard_map.198.h0.s0), channel_id=1, source_target_pairs={{0,3},{1,0},{2,1},{3,2},{4,7},{5,4},{6,5},{7,6},{8,11},{9,8},{10,9... | collective-permute-start | bytes 319496 | tf_op jit(solution)/shard_map/ppermute | solution.py:446
  67.4 5.5 %collective-permute-start.11 = (bf16[208,256]{1,0:T(8,128)(2,1)S(1)}, bf16[208,256]{1,0:T(8,128)(2,1)S(1)}, u32[]{:S(2)}, u32[]{:S(2)}) collective-permute-start(bf16[208,256]{1,0:T(8,128)(2,1)S(1)} %shard_map.198.h0.s0), channel_id=1, source_target_pairs={{0,2},{1,3},{2,0},{3,1},{4,6},{5,7},{6,4},{7,5},{8,10},{9,11},{10,... | collective-permute-start | bytes 319496 | tf_op jit(solution)/shard_map/ppermute | solution.py:446
  67.4 8.1 %collective-permute-start.10 = (bf16[208,256]{1,0:T(8,128)(2,1)S(1)}, bf16[208,256]{1,0:T(8,128)(2,1)S(1)}, u32[]{:S(2)}, u32[]{:S(2)}) collective-permute-start(bf16[208,256]{1,0:T(8,128)(2,1)S(1)} %shard_map.198.h0.s0), channel_id=1, source_target_pairs={{0,1},{1,2},{2,3},{3,0},{4,5},{5,6},{6,7},{7,4},{8,9},{9,10},{10,1... | collective-permute-start | bytes 319496 | tf_op jit(solution)/shard_map/ppermute | solution.py:446
  78.0 22.3 %all-to-all-start.2 = ((bf16[64,8,256]{2,1,0:T(8,128)(2,1)}), bf16[64,8,256]{2,1,0:T(8,128)(2,1)S(1)}, u32[]{:S(2)}, u32[]{:S(2)}) async-start(bf16[64,8,256]{2,1,0:T(8,128)(2,1)} %bitcast.7), calls=%async_computation.2 | async-start | bytes 524288 | tf_op jit(solution)/shard_map/all_to_all | solution.py:451
  (8 other events, 72.0 us)

commit v3 on v2

--- a/solution.py
+++ b/solution.py
@@ -8,6 +8,7 @@
 HEAD_DIM = 64
 EPS = 1e-06
 CAP = 3
+Z_ORDER = (0, -1, 1, -3, -4, -2, 3, 2)
 bf16 = jnp.bfloat16
 f32 = jnp.float32
 
@@ -60,9 +61,9 @@
     return copies
 
 
-def attend_kernel(len_hbm, bias_hbm, tok_hbm, gain_hbm, cache_hbm, wq_hbm, wo_hbm, sg_hbm, su_hbm,
-                  part_ref, joined_hbm,
-                  len_ref, bias_ref, tok_ref, gain_ref, cache_v, wq_v, wo_v, s_v, joined_v, sem_c, sem_w, sem_j):
+def attend_kernel(len_hbm, bias_hbm, tok_hbm, gain_hbm, cache_hbm, wq_hbm, wo_hbm, routes_hbm, sg_hbm, su_hbm,
+                  part_ref, pick_ref, joined_ref,
+                  len_ref, bias_ref, tok_ref, gain_ref, cache_v, wq_v, wo_v, s_v, routes_v, sem_c, sem_w):
     rows = tok_ref.shape[0]
     span = cache_v.shape[1]
     heads = 4
@@ -74,6 +75,8 @@
     ):
         small.append(pltpu.make_async_copy(src, dst, sem_w.at[i]))
     tok_c, gain_c, wq_c, wo_c, len_c, bias_c = small
+    routes_c = pltpu.make_async_copy(routes_hbm, routes_v, sem_w.at[6])
+    routes_c.start()
     tok_c.start()
     gain_c.start()
     wq_c.start()
@@ -85,9 +88,10 @@
     len_c.start()
     bias_c.start()
     wo_c.start()
-    width = sg_hbm.shape[1]
-    for c in copy_all([(sg_hbm, joined_v.at[:, :width]), (su_hbm, joined_v.at[:, width:])], sem_j, 8):
-        small.append(c)
+    half = sg_hbm.shape[1]
+    joins = copy_all([(sg_hbm, joined_ref.at[0, :, :half]), (su_hbm, joined_ref.at[0, :, half:])], sem_w, 7)
+    routes_c.wait()
+    make_pick(routes_v, pick_ref)
     tok_c.wait()
     gain_c.wait()
     x = tok_ref[...].astype(f32)
@@ -109,9 +113,6 @@
             cache_c[n].wait()
         keys = jnp.concatenate([cache_v[n] for n in range(4 * g, 4 * g + 4)], axis=1)
         s_v[16 * g : 16 * g + 16, :] = dot(wide_q[16 * g : 16 * g + 16, :], keys, ((1,), (1,)))
-    for c in small[6:]:
-        c.wait()
-    sends = copy_all([(joined_v, joined_hbm.at[j]) for j in range(joined_hbm.shape[0])], sem_j)
     rid = iota((hr, 128), 0)
     lens = jnp.zeros((hr, 128), jnp.int32)
     bias = jnp.zeros((hr, 128), f32)
@@ -156,24 +157,23 @@
     heads_out = dot(collect, ox).astype(bf16)
     wo_c.wait()
     part_ref[...] = dot(heads_out, wo_v[...]).astype(bf16)
-    for c in sends:
+    for c in joins:
         c.wait()
 
 
-def attend(tokens, lengths, cache, gain, wq, bias, wo, shared_gate, shared_up):
+def attend(tokens, lengths, cache, gain, wq, bias, wo, routes, shared_gate, shared_up):
     rows, d = tokens.shape
-    joined = (shared_gate.shape[0], 2 * shared_gate.shape[1])
+    n_pick = 8 * 64
     return call(
-        attend_kernel, [((rows, d), bf16), ((8, *joined), bf16)],
-        (lengths, bias, tokens, gain.reshape(1, -1), cache, wq, wo, shared_gate, shared_up),
-        in_specs=[HBM] * 9, out_specs=[VM, HBM],
+        attend_kernel, [((rows, d), bf16), ((n_pick, CAP * 8 * rows), bf16), ((1, shared_gate.shape[0], 256), bf16)],
+        (lengths, bias, tokens, gain.reshape(1, -1), cache, wq, wo, routes, shared_gate, shared_up),
+        in_specs=[HBM] * 10,
         scratch=[
             pltpu.SMEM(lengths.shape, jnp.int32), pltpu.SMEM(bias.shape, f32),
             pltpu.VMEM(tokens.shape, bf16), pltpu.VMEM((1, d), f32),
             pltpu.VMEM(cache.shape, bf16), pltpu.VMEM(wq.shape, bf16), pltpu.VMEM(wo.shape, bf16),
-            pltpu.VMEM((4 * rows, cache.shape[1]), f32),
-            pltpu.VMEM(joined, bf16),
-            pltpu.SemaphoreType.DMA((rows,)), pltpu.SemaphoreType.DMA((6,)), pltpu.SemaphoreType.DMA((10,)),
+            pltpu.VMEM((4 * rows, cache.shape[1]), f32), pltpu.VMEM(routes.shape, jnp.int32),
+            pltpu.SemaphoreType.DMA((rows,)), pltpu.SemaphoreType.DMA((9,)),
         ],
         limit_mib=16,
     )
@@ -197,7 +197,7 @@
     return slots, weight, spread
 
 
-def pick_kernel(routes_ref, pick_ref):
+def make_pick(routes_ref, pick_ref):
     rows = routes_ref.shape[1]
     slots, _, spread = slots_of(routes_ref, None)
     n = spread.shape[0]
@@ -232,6 +232,12 @@
         c.wait()
 
 
+def stack_kernel(near_ref, low_ref, high_ref, out_ref):
+    out_ref[0:3] = near_ref[...]
+    out_ref[3:6] = low_ref[...]
+    out_ref[6:8] = high_ref[0:2]
+
+
 def cut_kernel(part_ref, down_hbm, shared_hbm, o0, o1, o2, o3, all_v, sems):
     outs = (o0, o1, o2, o3)
     quarter = o0.shape[1]
@@ -256,12 +262,13 @@
     rows, d = normed_ref.shape
     wide = d // 8
     ep = ep_ref[0]
+    z = ep // 8
     y = (ep // 2) % 4
     c = ep % 2
     lane = iota((wide, wide), 1)
     there = ((y + 4 - lane // 64) % 4) * 64 + ((c + lane // 32) % 2) * 32 + lane % 32
     order = (iota((wide, wide), 0) == there).astype(bf16)
-    cols = [normed_ref[:, j * wide : (j + 1) * wide] for j in range(8)]
+    cols = [normed_ref[:, pl.ds(pl.multiple_of(((z + 8 + j) % 8) * wide, wide), wide)] for j in Z_ORDER]
     mine = dot(jnp.concatenate(cols, axis=0), order).astype(bf16)
     n = b0.shape[2]
     acc = jnp.zeros((rows, n), f32)
@@ -273,7 +280,7 @@
     hidden_ref[...] = hidden.astype(bf16)
 
 
-def expert_kernel(arrived_ref, wg_ref, wu_ref, sh_ref, hidden_ref, x_v):
+def expert_kernel(arrived_ref, wg_ref, wu_ref, hidden_ref, x_v):
     n = arrived_ref.shape[0]
     peers = n // 8
     wide = arrived_ref.shape[1] // CAP
@@ -289,10 +296,7 @@
     x = x_v[...]
     gate = dot(x, wg_ref[0])
     up = dot(x, wu_ref[0])
-    m = CAP * peers
-    hidden_ref[:m, :] = (silu(gate) * up).astype(bf16)
-    hidden_ref[m:, : sh_ref.shape[1]] = sh_ref[...]
-    hidden_ref[m:, sh_ref.shape[1] :] = jnp.zeros((sh_ref.shape[0], hidden_ref.shape[1] - sh_ref.shape[1]), bf16)
+    hidden_ref[...] = (silu(gate) * up).astype(bf16)
 
 
 def down_kernel(h0, h1, h2, h3, w0, w1, w2, w3, back_ref, w_v, sems):
@@ -397,13 +401,11 @@
             perm.append((i, (z + dz) % (nep // 8) * 8 + (y + dy) % 4 * 2 + (c + dc) % 2))
         return lax.ppermute(value, "ep", perm)
 
-    partial, copies = attend(
-        tokens, lengths, cache, attn_gain, query_weight, stick_bias, out_weight, shared_gate, shared_up
-    )
-    groups = [[z * 8 + r for z in range(nep // 8)] for r in range(8)]
+    partial, pick, joined = attend(
+        tokens, lengths, cache, attn_gain, query_weight, stick_bias, out_weight, routes.T, shared_gate, shared_up
+    )
     others = [lax.ppermute(partial, "tp", around(k, ntp)) for k in (2, 1, 3)]
-    column = lax.all_to_all(copies, "ep", 0, 0, axis_index_groups=groups, tiled=True)
-    (pick,) = call(pick_kernel, [((n_pick, CAP * 8 * rows), bf16)], (after(routes.T, partial),))
+    near = [joined, shift(joined, 1, 0, 0), shift(joined, -1, 0, 0)]
     normed_mix, residual, sent = call(
         mix_kernel, [((rows, d), bf16), ((rows, quarter), f32), ((n_pick, CAP * d // 8), bf16)],
         (part, tokens, partial, *others, ffn_gain.reshape(1, -1), pick),
@@ -413,11 +415,8 @@
     )
     arrived = lax.all_to_all(sent.reshape(nep, 8, -1), "ep", 0, 0, tiled=True)
     arrived = arrived.reshape(n_pick, -1)
-    column = after(column, sent)
-    planes = [column] + [shift(column, 0, k, 0) for k in range(1, 4)]
-    blocks = []
-    for block in planes:
-        blocks += [block, shift(block, 0, 0, 1)]
+    near = jnp.concatenate(after(near, sent))
+    low, high = shift(near, 3, 0, 0), shift(near, -3, 0, 0)
     f = expert_down.shape[1] + shared_down.shape[0]
     cuts = call(
         cut_kernel, [((f, quarter), bf16)] * 4, (part, after(expert_down, sent), shared_down),
@@ -434,24 +433,30 @@
         scratch=[pltpu.VMEM((rows, d), bf16), pltpu.VMEM((2 * HEAD_DIM, d), bf16), pltpu.VMEM((rows, d), bf16),
                  pltpu.SemaphoreType.DMA((4,))],
     )
-    (shared_hidden,) = call(
-        shared_kernel, [((rows, shared_gate.shape[1]), bf16)],
-        (lax.axis_index("ep").reshape(1), normed_mix, *blocks), in_specs=[SM] + [VM] * 9,
-    )
     m = CAP * nep
     (hidden,) = call(
-        expert_kernel, [((m + rows, expert_gate.shape[2]), bf16)],
-        (arrived, expert_gate, expert_up, shared_hidden), scratch=[pltpu.VMEM((m, d), bf16)],
+        expert_kernel, [((m, expert_gate.shape[2]), bf16)],
+        (arrived, expert_gate, expert_up), scratch=[pltpu.VMEM((m, d), bf16)],
     )
     hiddens = [hidden] + [lax.ppermute(hidden, "tp", around(k, ntp)) for k in range(1, ntp)]
+    (column,) = call(stack_kernel, [((8, *joined.shape[1:]), bf16)], (after(near, hidden), low, high))
+    planes = [column] + [shift(column, 0, k, 0) for k in range(1, 4)]
+    blocks = [column, shift(column, 0, 0, 1)]
     (back,) = call(
         down_kernel, [((n_pick, quarter // 2), bf16)], (*hiddens, *downs), in_specs=[VM] * 4 + [HBM] * 4,
         scratch=[pltpu.VMEM((ntp, expert_down.shape[1], quarter), bf16), pltpu.SemaphoreType.DMA((4,))],
     )
     returned = lax.all_to_all(back.reshape(nep, 8, -1), "ep", 0, 0, tiled=True)
     returned = returned.reshape(n_pick, -1)
+    for block in planes[1:]:
+        blocks += [block, shift(block, 0, 0, 1)]
+    (shared_hidden,) = call(
+        shared_kernel, [((rows, shared_gate.shape[1]), bf16)],
+        (lax.axis_index("ep").reshape(1), after(normed_mix, back), *blocks), in_specs=[SM] + [VM] * 9,
+    )
+    smalls = [shared_hidden] + [lax.ppermute(shared_hidden, "tp", around(k, ntp)) for k in range(1, ntp)]
     (base,) = call(
-        base_kernel, [((rows, quarter), f32)], (after(residual, back), mix_gate, *hiddens, *downs),
+        base_kernel, [((rows, quarter), f32)], (after(residual, back), mix_gate, *smalls, *downs),
         in_specs=[HBM] + [VM] * 5 + [HBM] * 4,
         scratch=[pltpu.VMEM((rows, quarter), f32), pltpu.VMEM((ntp, shared_down.shape[0], quarter), bf16),
                  pltpu.SemaphoreType.DMA((5,))],

time: 102 us -> 107 us (1.049)
  waiting for transfers between devices: 21.9 us -> 27.2 us
  starting transfers between devices: 53.5 us -> 58.5 us
  local copies, waits for them, and re-layouts: 4 us -> 0.06 us
  Pallas kernels: 20.8 us -> 19 us
    ppermute x7 -> x11, waiting for transfers between devices: 2.16 us -> 16.9 us  [shift(): return lax.ppermute(value, 'ep', perm)]
    all_to_all x1, waiting for transfers between devices: 9.5 us -> 0.01 us  [shards(): returned = lax.all_to_all(back.reshape(nep, 8, -1), 'ep', 0, 0, tiled=True)]
    all_to_all x1 -> x0, starting transfers between devices: 9.15 us -> none  [shards(): lax.all_to_all(copies, 'ep', 0, 0, axis_index_groups=groups, tiled=True)]
    ppermute x7 -> x11, starting transfers between devices: 11.1 us -> 20 us  [shift(): return lax.ppermute(value, 'ep', perm)]
    unnamed x26 -> x22, local copies, waits for them, and re-layouts: 4 us -> 0.06 us
    all_to_all x1, waiting for transfers between devices: 0.01 us -> 3.92 us  [shards(): arrived = lax.all_to_all(sent.reshape(nep, 8, -1), 'ep', 0, 0, tiled=True)]
    ppermute x3, waiting for transfers between devices: 7.41 us -> 3.81 us  [shards(): lax.ppermute(hidden, 'tp', around(k, ntp))]
    ppermute x0 -> x3, starting transfers between devices: none -> 3.19 us  [shards(): lax.ppermute(shared_hidden, 'tp', around(k, ntp))]
  transfers between devices with their start and end apart: 19 -> 25, of which waited for: 10 -> 10; matrix products, arithmetic and copies ran while one was open for 0% -> 0% of each run, Pallas kernels for 10% -> 7%
where the time goes in v3:
time: 107 us; the launch traced here: 106 us
  starting transfers between devices  58.5 us (55%)
  waiting for transfers between devices  27.2 us (25%)
  Pallas kernels  19 us (18%)
    ppermute x11, starting transfers between devices, shift(): return lax.ppermute(value, 'ep', perm)  20 us
    pallas_call x10, Pallas kernels, call(): pl.pallas_call(kernel, out_shape=tuple(shapes), in_specs=in_specs, out_sp...  19 us
    ppermute x11, waiting for transfers between devices, shift(): return lax.ppermute(value, 'ep', perm)  16.9 us
    all_to_all x1, starting transfers between devices, shards(): arrived = lax.all_to_all(sent.reshape(nep, 8, -1), 'ep', 0, 0, tiled=True)  13.1 us
    all_to_all x1, starting transfers between devices, shards(): returned = lax.all_to_all(back.reshape(nep, 8, -1), 'ep', 0, 0, tiled=True)  7.57 us
    ppermute x3, starting transfers between devices, shards(): others = [lax.ppermute(partial, 'tp', around(k, ntp)) for k in (2, 1, 3)]  6.32 us
    ppermute x3, starting transfers between devices, shards(): lax.ppermute(hidden, 'tp', around(k, ntp))  4.2 us
    ppermute x3, starting transfers between devices, shards(): lax.ppermute(cuts[k], 'tp', around(k, ntp))  4.2 us
  transfers between devices with their start and end apart: 25, of which 10 were waited for; matrix products, arithmetic and copies ran while one was open for 0% of the time, Pallas kernels for 7%

profile of v3, /device:TPU:1, one launch (start us, length us, event | category | flops | bytes accessed | tf_op | source)
XLA Modules:
  0.0 105.7 jit_solution(9895907857976594619)
XLA Ops:
  0.7 6.7 %shard_map.194 = (bf16[16,2048]{1,0:T(8,128)(2,1)S(1)}, bf16[512,384]{1,0:T(8,128)(2,1)S(1)}, bf16[1,32,256]{2,1,0:T(8,128)(2,1)S(1)}) custom-call(s32[16]{0:T(128)} %len_hbm.1, f32[4]{0:T(128)} %bias_hbm.1, bf16[16,2048]{1,0:T(8,128)(2,1)} %tok_hbm.2, f32[1,2048]{1,0:T(1,128)} %bitcast.15, bf16[16,1024,128]{2,1,0:T(8,128)(2,1)} %cache_hbm.1, ...), custom_call_target="tpu_custom_call" | custom-call | tf_op jit(solution)/shard_map/pallas_call | solution.py:47
  7.4 3.6 %collective-permute-start = (bf16[16,2048]{1,0:T(8,128)(2,1)S(1)}, bf16[16,2048]{1,0:T(8,128)(2,1)S(1)}, u32[]{:S(2)}, u32[]{:S(2)}) collective-permute-start(bf16[16,2048]{1,0:T(8,128)(2,1)S(1)} %get-tuple-element.23.p0), channel_id=1, source_target_pairs={{0,2},{1,3},{2,0},{3,1},{4,6},{5,7},{6,4},{7,5},{8,10},{9,11},{10,... | collective-permute-start | bytes 196616 | tf_op jit(solution)/shard_map/ppermute | solution.py:407
  11.4 2.4 %collective-permute-start.2 = (bf16[16,2048]{1,0:T(8,128)(2,1)S(1)}, bf16[16,2048]{1,0:T(8,128)(2,1)S(1)}, u32[]{:S(2)}, u32[]{:S(2)}) collective-permute-start(bf16[16,2048]{1,0:T(8,128)(2,1)S(1)} %get-tuple-element.23.p0), channel_id=1, source_target_pairs={{0,3},{1,0},{2,1},{3,2},{4,7},{5,4},{6,5},{7,6},{8,11},{9,8},{10,9... | collective-permute-start | bytes 196616 | tf_op jit(solution)/shard_map/ppermute | solution.py:407
  13.7 2.3 %collective-permute-done.1.p2 = bf16[16,2048]{1,0:T(8,128)(2,1)S(1)} collective-permute-done((bf16[16,2048]{1,0:T(8,128)(2,1)S(1)}, bf16[16,2048]{1,0:T(8,128)(2,1)S(1)}, u32[]{:S(2)}, u32[]{:S(2)}) %collective-permute-start.1) | collective-permute-done | bytes 65568 | tf_op jit(solution)/shard_map/ppermute | solution.py:407
  16.1 1.4 %shard_map.195 = (bf16[16,2048]{1,0:T(8,128)(2,1)}, f32[16,512]{1,0:T(8,128)}, bf16[512,768]{1,0:T(8,128)(2,1)}) custom-call(s32[1]{0:T(128)} %bitcast.part_ref, bf16[16,2048]{1,0:T(8,128)(2,1)S(1)} %copy-done.2, bf16[16,2048]{1,0:T(8,128)(2,1)S(1)} %get-tuple-element.23.p0, bf16[16,2048]{1,0:T(8,128)(2,1)S(1)} %collective-permute-done.p1, ...), custom_call_target="tpu_custom_call" | custom-call | tf_op jit(solution)/shard_map/pallas_call | solution.py:47
  17.5 13.1 %all-to-all-start = ((bf16[64,8,768]{2,1,0:T(8,128)(2,1)}), bf16[64,8,768]{2,1,0:T(8,128)(2,1)S(1)}, u32[]{:S(2)}, u32[]{:S(2)}) async-start(bf16[64,8,768]{2,1,0:T(8,128)(2,1)} %bitcast.22), calls=%async_computation | async-start | bytes 1572864 | tf_op jit(solution)/shard_map/all_to_all | solution.py:416
  30.6 2.6 %shard_map.197 = (bf16[384,512]{1,0:T(8,128)(2,1)}, bf16[384,512]{1,0:T(8,128)(2,1)}, bf16[384,512]{1,0:T(8,128)(2,1)}, bf16[384,512]{1,0:T(8,128)(2,1)}) custom-call(s32[1]{0:T(128)} %bitcast.part_ref, bf16[1,256,2048]{2,1,0:T(8,128)(2,1)} %down_hbm, bf16[128,2048]{1,0:T(8,128)(2,1)} %shared_hbm.1), custom_call_target="tpu_custom_call" | custom-call | tf_op jit(solution)/shard_map/pallas_call | solution.py:47
  33.3 4.1 %collective-permute-start.7 = (bf16[384,512]{1,0:T(8,128)(2,1)}, bf16[384,512]{1,0:T(8,128)(2,1)}, u32[]{:S(2)}, u32[]{:S(2)}) collective-permute-start(bf16[384,512]{1,0:T(8,128)(2,1)} %get-tuple-element.29), channel_id=1, source_target_pairs={{0,2},{1,3},{2,0},{3,1},{4,6},{5,7},{6,4},{7,5},{8,10},{9,11},{10,... | collective-permute-start | bytes 1179656 | tf_op jit(solution)/shard_map/ppermute | solution.py:426
  37.4 1.4 %collective-permute-start.9 = (bf16[1,32,256]{2,1,0:T(8,128)(2,1)S(1)}, bf16[1,32,256]{2,1,0:T(8,128)(2,1)S(1)}, u32[]{:S(2)}, u32[]{:S(2)}) collective-permute-start(bf16[1,32,256]{2,1,0:T(8,128)(2,1)S(1)} %get-tuple-element.39), channel_id=1, source_target_pairs={{0,32},{4,36},{8,40},{12,44},{16,48},{20,52},{24,56},{28,60},{32,6... | collective-permute-start | bytes 49160 | tf_op jit(solution)/shard_map/ppermute | solution.py:402
  38.8 1.5 %collective-permute-start.10 = (bf16[1,32,256]{2,1,0:T(8,128)(2,1)S(1)}, bf16[1,32,256]{2,1,0:T(8,128)(2,1)S(1)}, u32[]{:S(2)}, u32[]{:S(2)}) collective-permute-start(bf16[1,32,256]{2,1,0:T(8,128)(2,1)S(1)} %get-tuple-element.39), channel_id=1, source_target_pairs={{0,224},{4,228},{8,232},{12,236},{16,240},{20,244},{24,248},{28,25... | collective-permute-start | bytes 49160 | tf_op jit(solution)/shard_map/ppermute | solution.py:402
  40.2 9.2 %collective-permute-done.9 = bf16[1,32,256]{2,1,0:T(8,128)(2,1)S(1)} collective-permute-done((bf16[1,32,256]{2,1,0:T(8,128)(2,1)S(1)}, bf16[1,32,256]{2,1,0:T(8,128)(2,1)S(1)}, u32[]{:S(2)}, u32[]{:S(2)}) %collective-permute-start.9) | collective-permute-done | bytes 16416 | tf_op jit(solution)/shard_map/ppermute | solution.py:402
  49.6 3.9 %all-to-all-done = bf16[64,8,768]{2,1,0:T(8,128)(2,1)S(1)} async-done(((bf16[64,8,768]{2,1,0:T(8,128)(2,1)}), bf16[64,8,768]{2,1,0:T(8,128)(2,1)S(1)}, u32[]{:S(2)}, u32[]{:S(2)}) %all-to-all-start) | async-done | bytes 786464 | tf_op jit(solution)/shard_map/all_to_all | solution.py:416
  54.7 4.1 %collective-permute-start.4 = (bf16[192,256]{1,0:T(8,128)(2,1)S(1)}, bf16[192,256]{1,0:T(8,128)(2,1)S(1)}, u32[]{:S(2)}, u32[]{:S(2)}) collective-permute-start(bf16[192,256]{1,0:T(8,128)(2,1)S(1)} %shard_map.196.h0), channel_id=1, source_target_pairs={{0,2},{1,3},{2,0},{3,1},{4,6},{5,7},{6,4},{7,5},{8,10},{9,11},{10,... | collective-permute-start | bytes 294920 | tf_op jit(solution)/shard_map/ppermute | solution.py:441
  59.9 2.7 %collective-permute-done.4.h2 = bf16[192,256]{1,0:T(8,128)(2,1)S(1)} collective-permute-done((bf16[192,256]{1,0:T(8,128)(2,1)S(1)}, bf16[192,256]{1,0:T(8,128)(2,1)S(1)}, u32[]{:S(2)}, u32[]{:S(2)}) %collective-permute-start.4) | collective-permute-done | bytes 98336 | tf_op jit(solution)/shard_map/ppermute | solution.py:441
  62.7 2.5 %shard_map.198 = bf16[512,256]{1,0:T(8,128)(2,1)} custom-call(bf16[192,256]{1,0:T(8,128)(2,1)S(1)} %shard_map.196.h0, bf16[192,256]{1,0:T(8,128)(2,1)S(1)} %collective-permute-done.3.h1, bf16[192,256]{1,0:T(8,128)(2,1)S(1)} %collective-permute-done.4.h2, bf16[192,256]{1,0:T(8,128)(2,1)S(1)} %collective-permute-done.5.h3, ...), custom_call_target="tpu_custom_call" | custom-call | tf_op jit(solution)/shard_map/pallas_call | solution.py:47
  65.2 7.6 %all-to-all-start.1 = ((bf16[64,8,256]{2,1,0:T(8,128)(2,1)}), bf16[64,8,256]{2,1,0:T(8,128)(2,1)S(1)}, u32[]{:S(2)}, u32[]{:S(2)}) async-start(bf16[64,8,256]{2,1,0:T(8,128)(2,1)} %bitcast.6), calls=%async_computation.1 | async-start | bytes 524288 | tf_op jit(solution)/shard_map/all_to_all | solution.py:449
  72.8 3.3 %collective-permute-start.11 = (bf16[3,32,256]{2,1,0:T(8,128)(2,1)S(1)}, bf16[3,32,256]{2,1,0:T(8,128)(2,1)S(1)}, u32[]{:S(2)}, u32[]{:S(2)}) collective-permute-start(bf16[3,32,256]{2,1,0:T(8,128)(2,1)S(1)} %constant_dynamic-update-slice_fusion.near_ref), channel_id=1, source_target_pairs={{0,96},{4,100},{8,104},{12,108},{16,112},{20,116},{24,120},{28,124... | collective-permute-start | bytes 147464 | tf_op jit(solution)/shard_map/ppermute | solution.py:402
  76.0 1.4 %collective-permute-start.12 = (bf16[3,32,256]{2,1,0:T(8,128)(2,1)S(1)}, bf16[3,32,256]{2,1,0:T(8,128)(2,1)S(1)}, u32[]{:S(2)}, u32[]{:S(2)}) collective-permute-start(bf16[3,32,256]{2,1,0:T(8,128)(2,1)S(1)} %constant_dynamic-update-slice_fusion.near_ref), channel_id=1, source_target_pairs={{0,160},{4,164},{8,168},{12,172},{16,176},{20,180},{24,184},{28,18... | collective-permute-start | bytes 147464 | tf_op jit(solution)/shard_map/ppermute | solution.py:402
  77.5 6.5 %collective-permute-done.11.low_ref = bf16[3,32,256]{2,1,0:T(8,128)(2,1)S(1)} collective-permute-done((bf16[3,32,256]{2,1,0:T(8,128)(2,1)S(1)}, bf16[3,32,256]{2,1,0:T(8,128)(2,1)S(1)}, u32[]{:S(2)}, u32[]{:S(2)}) %collective-permute-start.11) | collective-permute-done | bytes 49184 | tf_op jit(solution)/shard_map/ppermute | solution.py:402
  84.9 2.5 %collective-permute-start.16 = (bf16[8,32,256]{2,1,0:T(8,128)(2,1)S(1)}, bf16[8,32,256]{2,1,0:T(8,128)(2,1)S(1)}, u32[]{:S(2)}, u32[]{:S(2)}) collective-permute-start(bf16[8,32,256]{2,1,0:T(8,128)(2,1)S(1)} %shard_map.200.b0), channel_id=1, source_target_pairs={{0,16},{4,20},{8,24},{12,28},{16,0},{20,4},{24,8},{28,12},{32,48},... | collective-permute-start | bytes 393224 | tf_op jit(solution)/shard_map/ppermute | solution.py:402
  88.4 4.6 %collective-permute-start.13 = (bf16[8,32,256]{2,1,0:T(8,128)(2,1)S(1)}, bf16[8,32,256]{2,1,0:T(8,128)(2,1)S(1)}, u32[]{:S(2)}, u32[]{:S(2)}) collective-permute-start(bf16[8,32,256]{2,1,0:T(8,128)(2,1)S(1)} %shard_map.200.b0), channel_id=1, source_target_pairs={{0,4},{4,0},{8,12},{12,8},{16,20},{20,16},{24,28},{28,24},{32,36},... | collective-permute-start | bytes 393224 | tf_op jit(solution)/shard_map/ppermute | solution.py:402
  93.3 2.5 %collective-permute-start.17 = (bf16[8,32,256]{2,1,0:T(8,128)(2,1)S(1)}, bf16[8,32,256]{2,1,0:T(8,128)(2,1)S(1)}, u32[]{:S(2)}, u32[]{:S(2)}) collective-permute-start(bf16[8,32,256]{2,1,0:T(8,128)(2,1)S(1)} %collective-permute-done.16.b4), channel_id=1, source_target_pairs={{0,4},{4,0},{8,12},{12,8},{16,20},{20,16},{24,28},{28,24},{32,36},... | collective-permute-start | bytes 393224 | tf_op jit(solution)/shard_map/ppermute | solution.py:402
  97.9 3.1 %collective-permute-start.21 = (bf16[16,128]{1,0:T(8,128)(2,1)S(1)}, bf16[16,128]{1,0:T(8,128)(2,1)S(1)}, u32[]{:S(2)}, u32[]{:S(2)}) collective-permute-start(bf16[16,128]{1,0:T(8,128)(2,1)S(1)} %shard_map.201.s0), channel_id=1, source_target_pairs={{0,2},{1,3},{2,0},{3,1},{4,6},{5,7},{6,4},{7,5},{8,10},{9,11},{10,... | collective-permute-start | bytes 12296 | tf_op jit(solution)/shard_map/ppermute | solution.py:457
  101.1 2.2 %shard_map.199 = (bf16[96,512]{1,0:T(8,128)(2,1)S(1)}, bf16[16,128]{1,0:T(8,128)(2,1)}, f32[16,128]{1,0:T(8,128)S(1)}) custom-call(s32[6,16]{1,0:T(8,128)S(1)} %bitcast.18, f32[6,16]{1,0:T(8,128)S(1)} %bitcast.20, bf16[16,2048]{1,0:T(8,128)(2,1)} %tok_hbm.2, f32[1,2048]{1,0:T(1,128)S(1)} %bitcast.16, bf16[64,2048]{1,0:T(8,128)(2,1)} %bitcast.23, ...), custom_call_target="tpu_custom_call" | custom-call | tf_op jit(solution)/shard_map/pallas_call | solution.py:47
  (59 shorter events, 9.5 us)
Async XLA Ops:
  7.4 6.3 %collective-permute-start = (bf16[16,2048]{1,0:T(8,128)(2,1)S(1)}, bf16[16,2048]{1,0:T(8,128)(2,1)S(1)}, u32[]{:S(2)}, u32[]{:S(2)}) collective-permute-start(bf16[16,2048]{1,0:T(8,128)(2,1)S(1)} %get-tuple-element.23.p0), channel_id=1, source_target_pairs={{0,2},{1,3},{2,0},{3,1},{4,6},{5,7},{6,4},{7,5},{8,10},{9,11},{10,... | collective-permute-start | bytes 196616 | tf_op jit(solution)/shard_map/ppermute | solution.py:407
  11.1 5.0 %collective-permute-start.1 = (bf16[16,2048]{1,0:T(8,128)(2,1)S(1)}, bf16[16,2048]{1,0:T(8,128)(2,1)S(1)}, u32[]{:S(2)}, u32[]{:S(2)}) collective-permute-start(bf16[16,2048]{1,0:T(8,128)(2,1)S(1)} %get-tuple-element.23.p0), channel_id=1, source_target_pairs={{0,1},{1,2},{2,3},{3,0},{4,5},{5,6},{6,7},{7,4},{8,9},{9,10},{10,1... | collective-permute-start | bytes 196616 | tf_op jit(solution)/shard_map/ppermute | solution.py:407
  11.4 4.7 %collective-permute-start.2 = (bf16[16,2048]{1,0:T(8,128)(2,1)S(1)}, bf16[16,2048]{1,0:T(8,128)(2,1)S(1)}, u32[]{:S(2)}, u32[]{:S(2)}) collective-permute-start(bf16[16,2048]{1,0:T(8,128)(2,1)S(1)} %get-tuple-element.23.p0), channel_id=1, source_target_pairs={{0,3},{1,0},{2,1},{3,2},{4,7},{5,4},{6,5},{7,6},{8,11},{9,8},{10,9... | collective-permute-start | bytes 196616 | tf_op jit(solution)/shard_map/ppermute | solution.py:407
  17.5 36.1 %all-to-all-start = ((bf16[64,8,768]{2,1,0:T(8,128)(2,1)}), bf16[64,8,768]{2,1,0:T(8,128)(2,1)S(1)}, u32[]{:S(2)}, u32[]{:S(2)}) async-start(bf16[64,8,768]{2,1,0:T(8,128)(2,1)} %bitcast.22), calls=%async_computation | async-start | bytes 1572864 | tf_op jit(solution)/shard_map/all_to_all | solution.py:416
  33.2 25.6 %collective-permute-start.6 = (bf16[384,512]{1,0:T(8,128)(2,1)}, bf16[384,512]{1,0:T(8,128)(2,1)S(1)}, u32[]{:S(2)}, u32[]{:S(2)}) collective-permute-start(bf16[384,512]{1,0:T(8,128)(2,1)} %get-tuple-element.28), channel_id=1, source_target_pairs={{0,1},{1,2},{2,3},{3,0},{4,5},{5,6},{6,7},{7,4},{8,9},{9,10},{10,1... | collective-permute-start | bytes 1179656 | tf_op jit(solution)/shard_map/ppermute | solution.py:426
  33.3 25.5 %collective-permute-start.7 = (bf16[384,512]{1,0:T(8,128)(2,1)}, bf16[384,512]{1,0:T(8,128)(2,1)}, u32[]{:S(2)}, u32[]{:S(2)}) collective-permute-start(bf16[384,512]{1,0:T(8,128)(2,1)} %get-tuple-element.29), channel_id=1, source_target_pairs={{0,2},{1,3},{2,0},{3,1},{4,6},{5,7},{6,4},{7,5},{8,10},{9,11},{10,... | collective-permute-start | bytes 1179656 | tf_op jit(solution)/shard_map/ppermute | solution.py:426
  37.4 21.4 %collective-permute-start.8 = (bf16[384,512]{1,0:T(8,128)(2,1)}, bf16[384,512]{1,0:T(8,128)(2,1)}, u32[]{:S(2)}, u32[]{:S(2)}) collective-permute-start(bf16[384,512]{1,0:T(8,128)(2,1)} %get-tuple-element.30), channel_id=1, source_target_pairs={{0,3},{1,0},{2,1},{3,2},{4,7},{5,4},{6,5},{7,6},{8,11},{9,8},{10,9... | collective-permute-start | bytes 1179656 | tf_op jit(solution)/shard_map/ppermute | solution.py:426
  37.4 12.1 %collective-permute-start.9 = (bf16[1,32,256]{2,1,0:T(8,128)(2,1)S(1)}, bf16[1,32,256]{2,1,0:T(8,128)(2,1)S(1)}, u32[]{:S(2)}, u32[]{:S(2)}) collective-permute-start(bf16[1,32,256]{2,1,0:T(8,128)(2,1)S(1)} %get-tuple-element.39), channel_id=1, source_target_pairs={{0,32},{4,36},{8,40},{12,44},{16,48},{20,52},{24,56},{28,60},{32,6... | collective-permute-start | bytes 49160 | tf_op jit(solution)/shard_map/ppermute | solution.py:402
  38.8 10.9 %collective-permute-start.10 = (bf16[1,32,256]{2,1,0:T(8,128)(2,1)S(1)}, bf16[1,32,256]{2,1,0:T(8,128)(2,1)S(1)}, u32[]{:S(2)}, u32[]{:S(2)}) collective-permute-start(bf16[1,32,256]{2,1,0:T(8,128)(2,1)S(1)} %get-tuple-element.39), channel_id=1, source_target_pairs={{0,224},{4,228},{8,232},{12,236},{16,240},{20,244},{24,248},{28,25... | collective-permute-start | bytes 49160 | tf_op jit(solution)/shard_map/ppermute | solution.py:402
  54.6 5.4 %collective-permute-start.3 = (bf16[192,256]{1,0:T(8,128)(2,1)S(1)}, bf16[192,256]{1,0:T(8,128)(2,1)S(1)}, u32[]{:S(2)}, u32[]{:S(2)}) collective-permute-start(bf16[192,256]{1,0:T(8,128)(2,1)S(1)} %shard_map.196.h0), channel_id=1, source_target_pairs={{0,1},{1,2},{2,3},{3,0},{4,5},{5,6},{6,7},{7,4},{8,9},{9,10},{10,1... | collective-permute-start | bytes 294920 | tf_op jit(solution)/shard_map/ppermute | solution.py:441
  54.7 8.0 %collective-permute-start.4 = (bf16[192,256]{1,0:T(8,128)(2,1)S(1)}, bf16[192,256]{1,0:T(8,128)(2,1)S(1)}, u32[]{:S(2)}, u32[]{:S(2)}) collective-permute-start(bf16[192,256]{1,0:T(8,128)(2,1)S(1)} %shard_map.196.h0), channel_id=1, source_target_pairs={{0,2},{1,3},{2,0},{3,1},{4,6},{5,7},{6,4},{7,5},{8,10},{9,11},{10,... | collective-permute-start | bytes 294920 | tf_op jit(solution)/shard_map/ppermute | solution.py:441
  58.8 3.9 %collective-permute-start.5 = (bf16[192,256]{1,0:T(8,128)(2,1)S(1)}, bf16[192,256]{1,0:T(8,128)(2,1)S(1)}, u32[]{:S(2)}, u32[]{:S(2)}) collective-permute-start(bf16[192,256]{1,0:T(8,128)(2,1)S(1)} %shard_map.196.h0), channel_id=1, source_target_pairs={{0,3},{1,0},{2,1},{3,2},{4,7},{5,4},{6,5},{7,6},{8,11},{9,8},{10,9... | collective-permute-start | bytes 294920 | tf_op jit(solution)/shard_map/ppermute | solution.py:441
  65.2 39.7 %all-to-all-start.1 = ((bf16[64,8,256]{2,1,0:T(8,128)(2,1)}), bf16[64,8,256]{2,1,0:T(8,128)(2,1)S(1)}, u32[]{:S(2)}, u32[]{:S(2)}) async-start(bf16[64,8,256]{2,1,0:T(8,128)(2,1)} %bitcast.6), calls=%async_computation.1 | async-start | bytes 524288 | tf_op jit(solution)/shard_map/all_to_all | solution.py:449
  72.8 11.2 %collective-permute-start.11 = (bf16[3,32,256]{2,1,0:T(8,128)(2,1)S(1)}, bf16[3,32,256]{2,1,0:T(8,128)(2,1)S(1)}, u32[]{:S(2)}, u32[]{:S(2)}) collective-permute-start(bf16[3,32,256]{2,1,0:T(8,128)(2,1)S(1)} %constant_dynamic-update-slice_fusion.near_ref), channel_id=1, source_target_pairs={{0,96},{4,100},{8,104},{12,108},{16,112},{20,116},{24,120},{28,124... | collective-permute-start | bytes 147464 | tf_op jit(solution)/shard_map/ppermute | solution.py:402
  76.0 7.9 %collective-permute-start.12 = (bf16[3,32,256]{2,1,0:T(8,128)(2,1)S(1)}, bf16[3,32,256]{2,1,0:T(8,128)(2,1)S(1)}, u32[]{:S(2)}, u32[]{:S(2)}) collective-permute-start(bf16[3,32,256]{2,1,0:T(8,128)(2,1)S(1)} %constant_dynamic-update-slice_fusion.near_ref), channel_id=1, source_target_pairs={{0,160},{4,164},{8,168},{12,172},{16,176},{20,180},{24,184},{28,18... | collective-permute-start | bytes 147464 | tf_op jit(solution)/shard_map/ppermute | solution.py:402
  84.0 9.0 %collective-permute-start.14 = (bf16[8,32,256]{2,1,0:T(8,128)(2,1)S(1)}, bf16[8,32,256]{2,1,0:T(8,128)(2,1)S(1)}, u32[]{:S(2)}, u32[]{:S(2)}) collective-permute-start(bf16[8,32,256]{2,1,0:T(8,128)(2,1)S(1)} %shard_map.200.b0), channel_id=1, source_target_pairs={{0,8},{4,12},{8,16},{12,20},{16,24},{20,28},{24,0},{28,4},{32,40},... | collective-permute-start | bytes 393224 | tf_op jit(solution)/shard_map/ppermute | solution.py:402
  84.9 8.4 %collective-permute-start.16 = (bf16[8,32,256]{2,1,0:T(8,128)(2,1)S(1)}, bf16[8,32,256]{2,1,0:T(8,128)(2,1)S(1)}, u32[]{:S(2)}, u32[]{:S(2)}) collective-permute-start(bf16[8,32,256]{2,1,0:T(8,128)(2,1)S(1)} %shard_map.200.b0), channel_id=1, source_target_pairs={{0,16},{4,20},{8,24},{12,28},{16,0},{20,4},{24,8},{28,12},{32,48},... | collective-permute-start | bytes 393224 | tf_op jit(solution)/shard_map/ppermute | solution.py:402
  87.4 8.4 %collective-permute-start.18 = (bf16[8,32,256]{2,1,0:T(8,128)(2,1)S(1)}, bf16[8,32,256]{2,1,0:T(8,128)(2,1)S(1)}, u32[]{:S(2)}, u32[]{:S(2)}) collective-permute-start(bf16[8,32,256]{2,1,0:T(8,128)(2,1)S(1)} %shard_map.200.b0), channel_id=1, source_target_pairs={{0,24},{4,28},{8,0},{12,4},{16,8},{20,12},{24,16},{28,20},{32,56},... | collective-permute-start | bytes 393224 | tf_op jit(solution)/shard_map/ppermute | solution.py:402
  88.4 8.1 %collective-permute-start.13 = (bf16[8,32,256]{2,1,0:T(8,128)(2,1)S(1)}, bf16[8,32,256]{2,1,0:T(8,128)(2,1)S(1)}, u32[]{:S(2)}, u32[]{:S(2)}) collective-permute-start(bf16[8,32,256]{2,1,0:T(8,128)(2,1)S(1)} %shard_map.200.b0), channel_id=1, source_target_pairs={{0,4},{4,0},{8,12},{12,8},{16,20},{20,16},{24,28},{28,24},{32,36},... | collective-permute-start | bytes 393224 | tf_op jit(solution)/shard_map/ppermute | solution.py:402
  93.0 3.4 %collective-permute-start.15 = (bf16[8,32,256]{2,1,0:T(8,128)(2,1)S(1)}, bf16[8,32,256]{2,1,0:T(8,128)(2,1)S(1)}, u32[]{:S(2)}, u32[]{:S(2)}) collective-permute-start(bf16[8,32,256]{2,1,0:T(8,128)(2,1)S(1)} %collective-permute-done.14.b2), channel_id=1, source_target_pairs={{0,4},{4,0},{8,12},{12,8},{16,20},{20,16},{24,28},{28,24},{32,36},... | collective-permute-start | bytes 393224 | tf_op jit(solution)/shard_map/ppermute | solution.py:402
  93.3 3.5 %collective-permute-start.17 = (bf16[8,32,256]{2,1,0:T(8,128)(2,1)S(1)}, bf16[8,32,256]{2,1,0:T(8,128)(2,1)S(1)}, u32[]{:S(2)}, u32[]{:S(2)}) collective-permute-start(bf16[8,32,256]{2,1,0:T(8,128)(2,1)S(1)} %collective-permute-done.16.b4), channel_id=1, source_target_pairs={{0,4},{4,0},{8,12},{12,8},{16,20},{20,16},{24,28},{28,24},{32,36},... | collective-permute-start | bytes 393224 | tf_op jit(solution)/shard_map/ppermute | solution.py:402
  97.9 5.4 %collective-permute-start.20 = (bf16[16,128]{1,0:T(8,128)(2,1)S(1)}, bf16[16,128]{1,0:T(8,128)(2,1)S(1)}, u32[]{:S(2)}, u32[]{:S(2)}) collective-permute-start(bf16[16,128]{1,0:T(8,128)(2,1)S(1)} %shard_map.201.s0), channel_id=1, source_target_pairs={{0,1},{1,2},{2,3},{3,0},{4,5},{5,6},{6,7},{7,4},{8,9},{9,10},{10,1... | collective-permute-start | bytes 12296 | tf_op jit(solution)/shard_map/ppermute | solution.py:457
  97.9 5.3 %collective-permute-start.21 = (bf16[16,128]{1,0:T(8,128)(2,1)S(1)}, bf16[16,128]{1,0:T(8,128)(2,1)S(1)}, u32[]{:S(2)}, u32[]{:S(2)}) collective-permute-start(bf16[16,128]{1,0:T(8,128)(2,1)S(1)} %shard_map.201.s0), channel_id=1, source_target_pairs={{0,2},{1,3},{2,0},{3,1},{4,6},{5,7},{6,4},{7,5},{8,10},{9,11},{10,... | collective-permute-start | bytes 12296 | tf_op jit(solution)/shard_map/ppermute | solution.py:457
  101.0 2.5 %collective-permute-start.22 = (bf16[16,128]{1,0:T(8,128)(2,1)S(1)}, bf16[16,128]{1,0:T(8,128)(2,1)S(1)}, u32[]{:S(2)}, u32[]{:S(2)}) collective-permute-start(bf16[16,128]{1,0:T(8,128)(2,1)S(1)} %shard_map.201.s0), channel_id=1, source_target_pairs={{0,3},{1,0},{2,1},{3,2},{4,7},{5,4},{6,5},{7,6},{8,11},{9,8},{10,9... | collective-permute-start | bytes 12296 | tf_op jit(solution)/shard_map/ppermute | solution.py:457
  (11 other events, 491.1 us)

commit v4 on v3

--- a/solution.py
+++ b/solution.py
@@ -238,12 +238,10 @@
     out_ref[6:8] = high_ref[0:2]
 
 
-def cut_kernel(part_ref, down_hbm, shared_hbm, o0, o1, o2, o3, all_v, sems):
+def cut_kernel(part_ref, down_hbm, o0, o1, o2, o3, all_v, sems):
     outs = (o0, o1, o2, o3)
     quarter = o0.shape[1]
-    f = down_hbm.shape[1]
-    first = copy_all([(down_hbm.at[0], all_v.at[:f, :]), (shared_hbm, all_v.at[f:, :])], sems, 4)
-    for c in first:
+    for c in copy_all([(down_hbm.at[0], all_v)], sems, 4):
         c.wait()
     pairs = []
     for k in (1, 3, 2, 0):
@@ -257,11 +255,14 @@
     return v / (1.0 + jnp.exp(-v))
 
 
-def shared_kernel(ep_ref, normed_ref, b0, b1, b2, b3, b4, b5, b6, b7, hidden_ref):
+def shared_kernel(at_ref, normed_ref, down_ref, residual_hbm, gate_ref, b0, b1, b2, b3, b4, b5, b6, b7,
+                  base_ref, o1, o2, o3, all_v, residual_v, sem):
     blocks = (b0, b1, b2, b3, b4, b5, b6, b7)
     rows, d = normed_ref.shape
     wide = d // 8
-    ep = ep_ref[0]
+    fetch = pltpu.make_async_copy(residual_hbm, residual_v, sem)
+    fetch.start()
+    ep = at_ref[0]
     z = ep // 8
     y = (ep // 2) % 4
     c = ep % 2
@@ -277,7 +278,13 @@
         acc = acc + dot(mine[j * rows : (j + 1) * rows, :], w)
     half = n // 2
     hidden = silu(acc[:, :half]) * acc[:, half:]
-    hidden_ref[...] = hidden.astype(bf16)
+    all_v[...] = dot(hidden.astype(bf16), down_ref[...])
+    quarter = o1.shape[1]
+    cols = [pl.ds(pl.multiple_of(((at_ref[1] + k) % 4) * quarter, quarter), quarter) for k in range(4)]
+    for k, o in enumerate((o1, o2, o3)):
+        o[...] = all_v[:, cols[k + 1]].astype(bf16)
+    fetch.wait()
+    base_ref[...] = residual_v[...] + gate_ref[:, :1] * all_v[:, cols[0]]
 
 
 def expert_kernel(arrived_ref, wg_ref, wu_ref, hidden_ref, x_v):
@@ -302,9 +309,8 @@
 def down_kernel(h0, h1, h2, h3, w0, w1, w2, w3, back_ref, w_v, sems):
     n = back_ref.shape[0]
     peers = n // 8
-    f = h0.shape[1]
     m = CAP * peers
-    copies = copy_all([(w.at[:f, :], w_v.at[k]) for k, w in enumerate((w0, w1, w2, w3))], sems)
+    copies = copy_all([(w, w_v.at[k]) for k, w in enumerate((w0, w1, w2, w3))], sems)
     a = iota((n, 2 * m), 0)
     b = iota((n, 2 * m), 1)
     order = ((a % 8 == b // peers) & (a // 8 == b % peers)).astype(bf16)
@@ -351,27 +357,16 @@
     gate_ref[...] = jnp.broadcast_to(1.0 / (1.0 + jnp.exp(-logit)), gate_ref.shape)
 
 
-def base_kernel(residual_hbm, gate_ref, s0, s1, s2, s3, w0, w1, w2, w3, base_ref, residual_v, w_v, sems):
-    at = w0.shape[0] - w_v.shape[1]
-    copies = copy_all([(w.at[at:, :], w_v.at[k]) for k, w in enumerate((w0, w1, w2, w3))], sems)
-    copies += copy_all([(residual_hbm, residual_v)], sems, 4)
-    acc = None
-    for k, h in enumerate((s0, s1, s2, s3)):
-        copies[k].wait()
-        part = dot(h[h.shape[0] - base_ref.shape[0] :, : w_v.shape[1]], w_v[k])
-        acc = part if acc is None else acc + part
-    copies[4].wait()
-    base_ref[...] = residual_v[...] + gate_ref[:, :1] * acc
-
-
-def final_kernel(back_ref, mix_ref, base_ref, out_ref):
+def final_kernel(back_ref, mix_ref, gate_ref, base_ref, s1, s2, s3, out_ref):
     rows = out_ref.shape[0]
     half = out_ref.shape[1] // 2
+    shared = s1[...].astype(f32) + (s2[...].astype(f32) + s3[...].astype(f32))
+    base = base_ref[...] + gate_ref[:, :1] * shared
     for h in range(2):
         r = dot(mix_ref[h * 3 * rows : (h + 1) * 3 * rows, :], back_ref[...])
         routed = (r[2 * rows :] + r[rows : 2 * rows]) + r[:rows]
         cols = slice(h * half, (h + 1) * half)
-        out_ref[:, cols] = (base_ref[:, cols] + routed).astype(bf16)
+        out_ref[:, cols] = (base[:, cols] + routed).astype(bf16)
 
 
 def around(k, size):
@@ -417,11 +412,11 @@
     arrived = arrived.reshape(n_pick, -1)
     near = jnp.concatenate(after(near, sent))
     low, high = shift(near, 3, 0, 0), shift(near, -3, 0, 0)
-    f = expert_down.shape[1] + shared_down.shape[0]
+    f = expert_down.shape[1]
     cuts = call(
-        cut_kernel, [((f, quarter), bf16)] * 4, (part, after(expert_down, sent), shared_down),
-        in_specs=[SM, HBM, HBM], out_specs=[HBM] * 4,
-        scratch=[pltpu.VMEM((f, d), bf16), pltpu.SemaphoreType.DMA((6,))],
+        cut_kernel, [((f, quarter), bf16)] * 4, (part, after(expert_down, sent)),
+        in_specs=[SM, HBM], out_specs=[HBM] * 4,
+        scratch=[pltpu.VMEM((f, d), bf16), pltpu.SemaphoreType.DMA((5,))],
     )
     downs = [cuts[0]] + [lax.ppermute(cuts[k], "tp", around(k, ntp)) for k in range(1, ntp)]
     mix, new_kv, mix_gate = call(
@@ -450,18 +445,18 @@
     returned = returned.reshape(n_pick, -1)
     for block in planes[1:]:
         blocks += [block, shift(block, 0, 0, 1)]
-    (shared_hidden,) = call(
-        shared_kernel, [((rows, shared_gate.shape[1]), bf16)],
-        (lax.axis_index("ep").reshape(1), after(normed_mix, back), *blocks), in_specs=[SM] + [VM] * 9,
-    )
-    smalls = [shared_hidden] + [lax.ppermute(shared_hidden, "tp", around(k, ntp)) for k in range(1, ntp)]
-    (base,) = call(
-        base_kernel, [((rows, quarter), f32)], (after(residual, back), mix_gate, *smalls, *downs),
-        in_specs=[HBM] + [VM] * 5 + [HBM] * 4,
-        scratch=[pltpu.VMEM((rows, quarter), f32), pltpu.VMEM((ntp, shared_down.shape[0], quarter), bf16),
-                 pltpu.SemaphoreType.DMA((5,))],
-    )
-    (layer_out,) = call(final_kernel, [((rows, quarter), bf16)], (returned, mix, base))
+    shares = call(
+        shared_kernel, [((rows, quarter), f32)] + [((rows, quarter), bf16)] * 3,
+        (jnp.stack([lax.axis_index("ep"), part[0]]), after(normed_mix, back), shared_down, residual,
+         mix_gate, *blocks),
+        in_specs=[SM, VM, VM, HBM] + [VM] * 9,
+        scratch=[pltpu.VMEM((rows, d), f32), pltpu.VMEM((rows, quarter), f32), pltpu.SemaphoreType.DMA],
+    )
+    shares = [shares[0]] + [lax.ppermute(shares[k], "tp", around(k, ntp)) for k in range(1, ntp)]
+    (layer_out,) = call(
+        final_kernel, [((rows, quarter), bf16)],
+        (returned, mix, mix_gate, *shares),
+    )
     return (layer_out, new_kv)
 
 

time: 107 us -> 108 us (level)
  waiting for transfers between devices: 27.2 us -> 28.7 us
    ppermute x3, waiting for transfers between devices: 0.22 us -> 2.22 us  [shards(): lax.ppermute(shares[k], 'tp', around(k, ntp))]
    pallas_call x10 -> x9, Pallas kernels: 19 us -> 18.6 us  [call(): pl.pallas_call(kernel, out_shape=tuple(shapes), in_specs=in_specs, out_sp...]
where the time goes in v4:
time: 108 us; the launch traced here: 107 us
  starting transfers between devices  58.6 us (54%)
  waiting for transfers between devices  28.7 us (27%)
  Pallas kernels  18.6 us (17%)
    ppermute x11, starting transfers between devices, shift(): return lax.ppermute(value, 'ep', perm)  20 us
    pallas_call x9, Pallas kernels, call(): pl.pallas_call(kernel, out_shape=tuple(shapes), in_specs=in_specs, out_sp...  18.6 us
    ppermute x11, waiting for transfers between devices, shift(): return lax.ppermute(value, 'ep', perm)  16.3 us
    all_to_all x1, starting transfers between devices, shards(): arrived = lax.all_to_all(sent.reshape(nep, 8, -1), 'ep', 0, 0, tiled=True)  13.2 us
    all_to_all x1, starting transfers between devices, shards(): returned = lax.all_to_all(back.reshape(nep, 8, -1), 'ep', 0, 0, tiled=True)  7.35 us
    ppermute x3, starting transfers between devices, shards(): others = [lax.ppermute(partial, 'tp', around(k, ntp)) for k in (2, 1, 3)]  6.32 us
    ppermute x3, starting transfers between devices, shards(): lax.ppermute(hidden, 'tp', around(k, ntp))  4.2 us
    ppermute x3, starting transfers between devices, shards(): lax.ppermute(cuts[k], 'tp', around(k, ntp))  4.2 us
  transfers between devices with their start and end apart: 25, of which 10 were waited for; matrix products, arithmetic and copies ran while one was open for 0% of the time, Pallas kernels for 7%

profile of v4, /device:TPU:1, one launch (start us, length us, event | category | flops | bytes accessed | tf_op | source)
XLA Modules:
  0.0 106.9 jit_solution(2038402683072941323)
XLA Ops:
  0.7 6.7 %shard_map.194 = (bf16[16,2048]{1,0:T(8,128)(2,1)S(1)}, bf16[512,384]{1,0:T(8,128)(2,1)S(1)}, bf16[1,32,256]{2,1,0:T(8,128)(2,1)S(1)}) custom-call(s32[16]{0:T(128)} %len_hbm.1, f32[4]{0:T(128)} %bias_hbm.1, bf16[16,2048]{1,0:T(8,128)(2,1)} %tok_hbm.2, f32[1,2048]{1,0:T(1,128)} %bitcast.15, bf16[16,1024,128]{2,1,0:T(8,128)(2,1)} %cache_hbm.1, ...), custom_call_target="tpu_custom_call" | custom-call | tf_op jit(solution)/shard_map/pallas_call | solution.py:47
  7.4 3.6 %collective-permute-start = (bf16[16,2048]{1,0:T(8,128)(2,1)S(1)}, bf16[16,2048]{1,0:T(8,128)(2,1)S(1)}, u32[]{:S(2)}, u32[]{:S(2)}) collective-permute-start(bf16[16,2048]{1,0:T(8,128)(2,1)S(1)} %get-tuple-element.26.p0), channel_id=1, source_target_pairs={{0,2},{1,3},{2,0},{3,1},{4,6},{5,7},{6,4},{7,5},{8,10},{9,11},{10,... | collective-permute-start | bytes 196616 | tf_op jit(solution)/shard_map/ppermute | solution.py:402
  11.4 2.4 %collective-permute-start.2 = (bf16[16,2048]{1,0:T(8,128)(2,1)S(1)}, bf16[16,2048]{1,0:T(8,128)(2,1)S(1)}, u32[]{:S(2)}, u32[]{:S(2)}) collective-permute-start(bf16[16,2048]{1,0:T(8,128)(2,1)S(1)} %get-tuple-element.26.p0), channel_id=1, source_target_pairs={{0,3},{1,0},{2,1},{3,2},{4,7},{5,4},{6,5},{7,6},{8,11},{9,8},{10,9... | collective-permute-start | bytes 196616 | tf_op jit(solution)/shard_map/ppermute | solution.py:402
  13.7 2.3 %collective-permute-done.1.p2 = bf16[16,2048]{1,0:T(8,128)(2,1)S(1)} collective-permute-done((bf16[16,2048]{1,0:T(8,128)(2,1)S(1)}, bf16[16,2048]{1,0:T(8,128)(2,1)S(1)}, u32[]{:S(2)}, u32[]{:S(2)}) %collective-permute-start.1) | collective-permute-done | bytes 65568 | tf_op jit(solution)/shard_map/ppermute | solution.py:402
  16.1 1.4 %shard_map.195 = (bf16[16,2048]{1,0:T(8,128)(2,1)}, f32[16,512]{1,0:T(8,128)}, bf16[512,768]{1,0:T(8,128)(2,1)}) custom-call(s32[1]{0:T(128)} %bitcast.part_ref, bf16[16,2048]{1,0:T(8,128)(2,1)S(1)} %copy-done.2, bf16[16,2048]{1,0:T(8,128)(2,1)S(1)} %get-tuple-element.26.p0, bf16[16,2048]{1,0:T(8,128)(2,1)S(1)} %collective-permute-done.p1, ...), custom_call_target="tpu_custom_call" | custom-call | tf_op jit(solution)/shard_map/pallas_call | solution.py:47
  17.6 13.2 %all-to-all-start = ((bf16[64,8,768]{2,1,0:T(8,128)(2,1)}), bf16[64,8,768]{2,1,0:T(8,128)(2,1)S(1)}, u32[]{:S(2)}, u32[]{:S(2)}) async-start(bf16[64,8,768]{2,1,0:T(8,128)(2,1)} %bitcast.22), calls=%async_computation | async-start | bytes 1572864 | tf_op jit(solution)/shard_map/all_to_all | solution.py:411
  30.8 2.2 %shard_map.197 = (bf16[256,512]{1,0:T(8,128)(2,1)}, bf16[256,512]{1,0:T(8,128)(2,1)}, bf16[256,512]{1,0:T(8,128)(2,1)}, bf16[256,512]{1,0:T(8,128)(2,1)}) custom-call(s32[1]{0:T(128)} %bitcast.part_ref, bf16[1,256,2048]{2,1,0:T(8,128)(2,1)} %down_hbm), custom_call_target="tpu_custom_call" | custom-call | tf_op jit(solution)/shard_map/pallas_call | solution.py:47
  33.1 4.1 %collective-permute-start.7 = (bf16[256,512]{1,0:T(8,128)(2,1)}, bf16[256,512]{1,0:T(8,128)(2,1)}, u32[]{:S(2)}, u32[]{:S(2)}) collective-permute-start(bf16[256,512]{1,0:T(8,128)(2,1)} %get-tuple-element.32), channel_id=1, source_target_pairs={{0,2},{1,3},{2,0},{3,1},{4,6},{5,7},{6,4},{7,5},{8,10},{9,11},{10,... | collective-permute-start | bytes 786440 | tf_op jit(solution)/shard_map/ppermute | solution.py:421
  38.6 1.5 %collective-permute-start.10 = (bf16[1,32,256]{2,1,0:T(8,128)(2,1)S(1)}, bf16[1,32,256]{2,1,0:T(8,128)(2,1)S(1)}, u32[]{:S(2)}, u32[]{:S(2)}) collective-permute-start(bf16[1,32,256]{2,1,0:T(8,128)(2,1)S(1)} %get-tuple-element.41), channel_id=1, source_target_pairs={{0,224},{4,228},{8,232},{12,236},{16,240},{20,244},{24,248},{28,25... | collective-permute-start | bytes 49160 | tf_op jit(solution)/shard_map/ppermute | solution.py:397
  40.1 9.6 %collective-permute-done.9 = bf16[1,32,256]{2,1,0:T(8,128)(2,1)S(1)} collective-permute-done((bf16[1,32,256]{2,1,0:T(8,128)(2,1)S(1)}, bf16[1,32,256]{2,1,0:T(8,128)(2,1)S(1)}, u32[]{:S(2)}, u32[]{:S(2)}) %collective-permute-start.9) | collective-permute-done | bytes 16416 | tf_op jit(solution)/shard_map/ppermute | solution.py:397
  49.9 3.9 %all-to-all-done = bf16[64,8,768]{2,1,0:T(8,128)(2,1)S(1)} async-done(((bf16[64,8,768]{2,1,0:T(8,128)(2,1)}), bf16[64,8,768]{2,1,0:T(8,128)(2,1)S(1)}, u32[]{:S(2)}, u32[]{:S(2)}) %all-to-all-start) | async-done | bytes 786464 | tf_op jit(solution)/shard_map/all_to_all | solution.py:411
  54.9 4.1 %collective-permute-start.4 = (bf16[192,256]{1,0:T(8,128)(2,1)S(1)}, bf16[192,256]{1,0:T(8,128)(2,1)S(1)}, u32[]{:S(2)}, u32[]{:S(2)}) collective-permute-start(bf16[192,256]{1,0:T(8,128)(2,1)S(1)} %shard_map.196.h0), channel_id=1, source_target_pairs={{0,2},{1,3},{2,0},{3,1},{4,6},{5,7},{6,4},{7,5},{8,10},{9,11},{10,... | collective-permute-start | bytes 294920 | tf_op jit(solution)/shard_map/ppermute | solution.py:436
  60.2 2.7 %collective-permute-done.4.h2 = bf16[192,256]{1,0:T(8,128)(2,1)S(1)} collective-permute-done((bf16[192,256]{1,0:T(8,128)(2,1)S(1)}, bf16[192,256]{1,0:T(8,128)(2,1)S(1)}, u32[]{:S(2)}, u32[]{:S(2)}) %collective-permute-start.4) | collective-permute-done | bytes 98336 | tf_op jit(solution)/shard_map/ppermute | solution.py:436
  62.9 2.5 %shard_map.198 = bf16[512,256]{1,0:T(8,128)(2,1)} custom-call(bf16[192,256]{1,0:T(8,128)(2,1)S(1)} %shard_map.196.h0, bf16[192,256]{1,0:T(8,128)(2,1)S(1)} %collective-permute-done.3.h1, bf16[192,256]{1,0:T(8,128)(2,1)S(1)} %collective-permute-done.4.h2, bf16[192,256]{1,0:T(8,128)(2,1)S(1)} %collective-permute-done.5.h3, ...), custom_call_target="tpu_custom_call" | custom-call | tf_op jit(solution)/shard_map/pallas_call | solution.py:47
  65.4 7.3 %all-to-all-start.1 = ((bf16[64,8,256]{2,1,0:T(8,128)(2,1)}), bf16[64,8,256]{2,1,0:T(8,128)(2,1)S(1)}, u32[]{:S(2)}, u32[]{:S(2)}) async-start(bf16[64,8,256]{2,1,0:T(8,128)(2,1)} %bitcast.6), calls=%async_computation.1 | async-start | bytes 524288 | tf_op jit(solution)/shard_map/all_to_all | solution.py:444
  72.8 3.3 %collective-permute-start.11 = (bf16[3,32,256]{2,1,0:T(8,128)(2,1)S(1)}, bf16[3,32,256]{2,1,0:T(8,128)(2,1)S(1)}, u32[]{:S(2)}, u32[]{:S(2)}) collective-permute-start(bf16[3,32,256]{2,1,0:T(8,128)(2,1)S(1)} %constant_dynamic-update-slice_fusion.near_ref), channel_id=1, source_target_pairs={{0,96},{4,100},{8,104},{12,108},{16,112},{20,116},{24,120},{28,124... | collective-permute-start | bytes 147464 | tf_op jit(solution)/shard_map/ppermute | solution.py:397
  76.0 1.4 %collective-permute-start.12 = (bf16[3,32,256]{2,1,0:T(8,128)(2,1)S(1)}, bf16[3,32,256]{2,1,0:T(8,128)(2,1)S(1)}, u32[]{:S(2)}, u32[]{:S(2)}) collective-permute-start(bf16[3,32,256]{2,1,0:T(8,128)(2,1)S(1)} %constant_dynamic-update-slice_fusion.near_ref), channel_id=1, source_target_pairs={{0,160},{4,164},{8,168},{12,172},{16,176},{20,180},{24,184},{28,18... | collective-permute-start | bytes 147464 | tf_op jit(solution)/shard_map/ppermute | solution.py:397
  77.4 6.5 %collective-permute-done.11.low_ref = bf16[3,32,256]{2,1,0:T(8,128)(2,1)S(1)} collective-permute-done((bf16[3,32,256]{2,1,0:T(8,128)(2,1)S(1)}, bf16[3,32,256]{2,1,0:T(8,128)(2,1)S(1)}, u32[]{:S(2)}, u32[]{:S(2)}) %collective-permute-start.11) | collective-permute-done | bytes 49184 | tf_op jit(solution)/shard_map/ppermute | solution.py:397
  84.9 2.5 %collective-permute-start.16 = (bf16[8,32,256]{2,1,0:T(8,128)(2,1)S(1)}, bf16[8,32,256]{2,1,0:T(8,128)(2,1)S(1)}, u32[]{:S(2)}, u32[]{:S(2)}) collective-permute-start(bf16[8,32,256]{2,1,0:T(8,128)(2,1)S(1)} %shard_map.200.b0), channel_id=1, source_target_pairs={{0,16},{4,20},{8,24},{12,28},{16,0},{20,4},{24,8},{28,12},{32,48},... | collective-permute-start | bytes 393224 | tf_op jit(solution)/shard_map/ppermute | solution.py:397
  88.3 4.6 %collective-permute-start.13 = (bf16[8,32,256]{2,1,0:T(8,128)(2,1)S(1)}, bf16[8,32,256]{2,1,0:T(8,128)(2,1)S(1)}, u32[]{:S(2)}, u32[]{:S(2)}) collective-permute-start(bf16[8,32,256]{2,1,0:T(8,128)(2,1)S(1)} %shard_map.200.b0), channel_id=1, source_target_pairs={{0,4},{4,0},{8,12},{12,8},{16,20},{20,16},{24,28},{28,24},{32,36},... | collective-permute-start | bytes 393224 | tf_op jit(solution)/shard_map/ppermute | solution.py:397
  93.2 2.5 %collective-permute-start.17 = (bf16[8,32,256]{2,1,0:T(8,128)(2,1)S(1)}, bf16[8,32,256]{2,1,0:T(8,128)(2,1)S(1)}, u32[]{:S(2)}, u32[]{:S(2)}) collective-permute-start(bf16[8,32,256]{2,1,0:T(8,128)(2,1)S(1)} %collective-permute-done.16.b4), channel_id=1, source_target_pairs={{0,4},{4,0},{8,12},{12,8},{16,20},{20,16},{24,28},{28,24},{32,36},... | collective-permute-start | bytes 393224 | tf_op jit(solution)/shard_map/ppermute | solution.py:397
  96.5 2.2 %shard_map.199 = (bf16[96,512]{1,0:T(8,128)(2,1)S(1)}, bf16[16,128]{1,0:T(8,128)(2,1)}, f32[16,128]{1,0:T(8,128)S(1)}) custom-call(s32[6,16]{1,0:T(8,128)S(1)} %bitcast.18, f32[6,16]{1,0:T(8,128)S(1)} %bitcast.20, bf16[16,2048]{1,0:T(8,128)(2,1)} %tok_hbm.2, f32[1,2048]{1,0:T(1,128)S(1)} %bitcast.16, bf16[64,2048]{1,0:T(8,128)(2,1)} %bitcast.23, ...), custom_call_target="tpu_custom_call" | custom-call | tf_op jit(solution)/shard_map/pallas_call | solution.py:47
  98.7 1.7 %shard_map.201 = (f32[16,512]{1,0:T(8,128)S(1)}, bf16[16,512]{1,0:T(8,128)(2,1)S(1)}, bf16[16,512]{1,0:T(8,128)(2,1)S(1)}, bf16[16,512]{1,0:T(8,128)(2,1)S(1)}) custom-call(s32[2]{0:T(128)S(1)} %pad_add_fusion.at_ref, bf16[16,2048]{1,0:T(8,128)(2,1)S(1)} %copy-done.4, bf16[128,2048]{1,0:T(8,128)(2,1)S(1)} %copy-done.3, ...), custom_call_target="tpu_custom_call" | custom-call | tf_op jit(solution)/shard_map/pallas_call | solution.py:47
  100.6 2.9 %collective-permute-start.21 = (bf16[16,512]{1,0:T(8,128)(2,1)S(1)}, bf16[16,512]{1,0:T(8,128)(2,1)S(1)}, u32[]{:S(2)}, u32[]{:S(2)}) collective-permute-start(bf16[16,512]{1,0:T(8,128)(2,1)S(1)} %get-tuple-element.47), channel_id=1, source_target_pairs={{0,2},{1,3},{2,0},{3,1},{4,6},{5,7},{6,4},{7,5},{8,10},{9,11},{10,... | collective-permute-start | bytes 49160 | tf_op jit(solution)/shard_map/ppermute | solution.py:455
  (59 shorter events, 10.6 us)
Async XLA Ops:
  7.4 6.3 %collective-permute-start = (bf16[16,2048]{1,0:T(8,128)(2,1)S(1)}, bf16[16,2048]{1,0:T(8,128)(2,1)S(1)}, u32[]{:S(2)}, u32[]{:S(2)}) collective-permute-start(bf16[16,2048]{1,0:T(8,128)(2,1)S(1)} %get-tuple-element.26.p0), channel_id=1, source_target_pairs={{0,2},{1,3},{2,0},{3,1},{4,6},{5,7},{6,4},{7,5},{8,10},{9,11},{10,... | collective-permute-start | bytes 196616 | tf_op jit(solution)/shard_map/ppermute | solution.py:402
  11.1 5.0 %collective-permute-start.1 = (bf16[16,2048]{1,0:T(8,128)(2,1)S(1)}, bf16[16,2048]{1,0:T(8,128)(2,1)S(1)}, u32[]{:S(2)}, u32[]{:S(2)}) collective-permute-start(bf16[16,2048]{1,0:T(8,128)(2,1)S(1)} %get-tuple-element.26.p0), channel_id=1, source_target_pairs={{0,1},{1,2},{2,3},{3,0},{4,5},{5,6},{6,7},{7,4},{8,9},{9,10},{10,1... | collective-permute-start | bytes 196616 | tf_op jit(solution)/shard_map/ppermute | solution.py:402
  11.4 4.7 %collective-permute-start.2 = (bf16[16,2048]{1,0:T(8,128)(2,1)S(1)}, bf16[16,2048]{1,0:T(8,128)(2,1)S(1)}, u32[]{:S(2)}, u32[]{:S(2)}) collective-permute-start(bf16[16,2048]{1,0:T(8,128)(2,1)S(1)} %get-tuple-element.26.p0), channel_id=1, source_target_pairs={{0,3},{1,0},{2,1},{3,2},{4,7},{5,4},{6,5},{7,6},{8,11},{9,8},{10,9... | collective-permute-start | bytes 196616 | tf_op jit(solution)/shard_map/ppermute | solution.py:402
  17.6 36.2 %all-to-all-start = ((bf16[64,8,768]{2,1,0:T(8,128)(2,1)}), bf16[64,8,768]{2,1,0:T(8,128)(2,1)S(1)}, u32[]{:S(2)}, u32[]{:S(2)}) async-start(bf16[64,8,768]{2,1,0:T(8,128)(2,1)} %bitcast.22), calls=%async_computation | async-start | bytes 1572864 | tf_op jit(solution)/shard_map/all_to_all | solution.py:411
  33.0 26.0 %collective-permute-start.6 = (bf16[256,512]{1,0:T(8,128)(2,1)}, bf16[256,512]{1,0:T(8,128)(2,1)}, u32[]{:S(2)}, u32[]{:S(2)}) collective-permute-start(bf16[256,512]{1,0:T(8,128)(2,1)} %get-tuple-element.31), channel_id=1, source_target_pairs={{0,1},{1,2},{2,3},{3,0},{4,5},{5,6},{6,7},{7,4},{8,9},{9,10},{10,1... | collective-permute-start | bytes 786440 | tf_op jit(solution)/shard_map/ppermute | solution.py:421
  33.1 25.9 %collective-permute-start.7 = (bf16[256,512]{1,0:T(8,128)(2,1)}, bf16[256,512]{1,0:T(8,128)(2,1)}, u32[]{:S(2)}, u32[]{:S(2)}) collective-permute-start(bf16[256,512]{1,0:T(8,128)(2,1)} %get-tuple-element.32), channel_id=1, source_target_pairs={{0,2},{1,3},{2,0},{3,1},{4,6},{5,7},{6,4},{7,5},{8,10},{9,11},{10,... | collective-permute-start | bytes 786440 | tf_op jit(solution)/shard_map/ppermute | solution.py:421
  37.2 21.8 %collective-permute-start.8 = (bf16[256,512]{1,0:T(8,128)(2,1)}, bf16[256,512]{1,0:T(8,128)(2,1)}, u32[]{:S(2)}, u32[]{:S(2)}) collective-permute-start(bf16[256,512]{1,0:T(8,128)(2,1)} %get-tuple-element.33), channel_id=1, source_target_pairs={{0,3},{1,0},{2,1},{3,2},{4,7},{5,4},{6,5},{7,6},{8,11},{9,8},{10,9... | collective-permute-start | bytes 786440 | tf_op jit(solution)/shard_map/ppermute | solution.py:421
  37.2 12.5 %collective-permute-start.9 = (bf16[1,32,256]{2,1,0:T(8,128)(2,1)S(1)}, bf16[1,32,256]{2,1,0:T(8,128)(2,1)S(1)}, u32[]{:S(2)}, u32[]{:S(2)}) collective-permute-start(bf16[1,32,256]{2,1,0:T(8,128)(2,1)S(1)} %get-tuple-element.41), channel_id=1, source_target_pairs={{0,32},{4,36},{8,40},{12,44},{16,48},{20,52},{24,56},{28,60},{32,6... | collective-permute-start | bytes 49160 | tf_op jit(solution)/shard_map/ppermute | solution.py:397
  38.6 11.3 %collective-permute-start.10 = (bf16[1,32,256]{2,1,0:T(8,128)(2,1)S(1)}, bf16[1,32,256]{2,1,0:T(8,128)(2,1)S(1)}, u32[]{:S(2)}, u32[]{:S(2)}) collective-permute-start(bf16[1,32,256]{2,1,0:T(8,128)(2,1)S(1)} %get-tuple-element.41), channel_id=1, source_target_pairs={{0,224},{4,228},{8,232},{12,236},{16,240},{20,244},{24,248},{28,25... | collective-permute-start | bytes 49160 | tf_op jit(solution)/shard_map/ppermute | solution.py:397
  54.8 5.4 %collective-permute-start.3 = (bf16[192,256]{1,0:T(8,128)(2,1)S(1)}, bf16[192,256]{1,0:T(8,128)(2,1)S(1)}, u32[]{:S(2)}, u32[]{:S(2)}) collective-permute-start(bf16[192,256]{1,0:T(8,128)(2,1)S(1)} %shard_map.196.h0), channel_id=1, source_target_pairs={{0,1},{1,2},{2,3},{3,0},{4,5},{5,6},{6,7},{7,4},{8,9},{9,10},{10,1... | collective-permute-start | bytes 294920 | tf_op jit(solution)/shard_map/ppermute | solution.py:436
  54.9 8.0 %collective-permute-start.4 = (bf16[192,256]{1,0:T(8,128)(2,1)S(1)}, bf16[192,256]{1,0:T(8,128)(2,1)S(1)}, u32[]{:S(2)}, u32[]{:S(2)}) collective-permute-start(bf16[192,256]{1,0:T(8,128)(2,1)S(1)} %shard_map.196.h0), channel_id=1, source_target_pairs={{0,2},{1,3},{2,0},{3,1},{4,6},{5,7},{6,4},{7,5},{8,10},{9,11},{10,... | collective-permute-start | bytes 294920 | tf_op jit(solution)/shard_map/ppermute | solution.py:436
  59.0 3.9 %collective-permute-start.5 = (bf16[192,256]{1,0:T(8,128)(2,1)S(1)}, bf16[192,256]{1,0:T(8,128)(2,1)S(1)}, u32[]{:S(2)}, u32[]{:S(2)}) collective-permute-start(bf16[192,256]{1,0:T(8,128)(2,1)S(1)} %shard_map.196.h0), channel_id=1, source_target_pairs={{0,3},{1,0},{2,1},{3,2},{4,7},{5,4},{6,5},{7,6},{8,11},{9,8},{10,9... | collective-permute-start | bytes 294920 | tf_op jit(solution)/shard_map/ppermute | solution.py:436
  65.4 40.7 %all-to-all-start.1 = ((bf16[64,8,256]{2,1,0:T(8,128)(2,1)}), bf16[64,8,256]{2,1,0:T(8,128)(2,1)S(1)}, u32[]{:S(2)}, u32[]{:S(2)}) async-start(bf16[64,8,256]{2,1,0:T(8,128)(2,1)} %bitcast.6), calls=%async_computation.1 | async-start | bytes 524288 | tf_op jit(solution)/shard_map/all_to_all | solution.py:444
  72.8 11.2 %collective-permute-start.11 = (bf16[3,32,256]{2,1,0:T(8,128)(2,1)S(1)}, bf16[3,32,256]{2,1,0:T(8,128)(2,1)S(1)}, u32[]{:S(2)}, u32[]{:S(2)}) collective-permute-start(bf16[3,32,256]{2,1,0:T(8,128)(2,1)S(1)} %constant_dynamic-update-slice_fusion.near_ref), channel_id=1, source_target_pairs={{0,96},{4,100},{8,104},{12,108},{16,112},{20,116},{24,120},{28,124... | collective-permute-start | bytes 147464 | tf_op jit(solution)/shard_map/ppermute | solution.py:397
  76.0 7.9 %collective-permute-start.12 = (bf16[3,32,256]{2,1,0:T(8,128)(2,1)S(1)}, bf16[3,32,256]{2,1,0:T(8,128)(2,1)S(1)}, u32[]{:S(2)}, u32[]{:S(2)}) collective-permute-start(bf16[3,32,256]{2,1,0:T(8,128)(2,1)S(1)} %constant_dynamic-update-slice_fusion.near_ref), channel_id=1, source_target_pairs={{0,160},{4,164},{8,168},{12,172},{16,176},{20,180},{24,184},{28,18... | collective-permute-start | bytes 147464 | tf_op jit(solution)/shard_map/ppermute | solution.py:397
  84.0 9.0 %collective-permute-start.14 = (bf16[8,32,256]{2,1,0:T(8,128)(2,1)S(1)}, bf16[8,32,256]{2,1,0:T(8,128)(2,1)S(1)}, u32[]{:S(2)}, u32[]{:S(2)}) collective-permute-start(bf16[8,32,256]{2,1,0:T(8,128)(2,1)S(1)} %shard_map.200.b0), channel_id=1, source_target_pairs={{0,8},{4,12},{8,16},{12,20},{16,24},{20,28},{24,0},{28,4},{32,40},... | collective-permute-start | bytes 393224 | tf_op jit(solution)/shard_map/ppermute | solution.py:397
  84.9 8.4 %collective-permute-start.16 = (bf16[8,32,256]{2,1,0:T(8,128)(2,1)S(1)}, bf16[8,32,256]{2,1,0:T(8,128)(2,1)S(1)}, u32[]{:S(2)}, u32[]{:S(2)}) collective-permute-start(bf16[8,32,256]{2,1,0:T(8,128)(2,1)S(1)} %shard_map.200.b0), channel_id=1, source_target_pairs={{0,16},{4,20},{8,24},{12,28},{16,0},{20,4},{24,8},{28,12},{32,48},... | collective-permute-start | bytes 393224 | tf_op jit(solution)/shard_map/ppermute | solution.py:397
  87.4 8.4 %collective-permute-start.18 = (bf16[8,32,256]{2,1,0:T(8,128)(2,1)S(1)}, bf16[8,32,256]{2,1,0:T(8,128)(2,1)S(1)}, u32[]{:S(2)}, u32[]{:S(2)}) collective-permute-start(bf16[8,32,256]{2,1,0:T(8,128)(2,1)S(1)} %shard_map.200.b0), channel_id=1, source_target_pairs={{0,24},{4,28},{8,0},{12,4},{16,8},{20,12},{24,16},{28,20},{32,56},... | collective-permute-start | bytes 393224 | tf_op jit(solution)/shard_map/ppermute | solution.py:397
  88.3 10.3 %collective-permute-start.13 = (bf16[8,32,256]{2,1,0:T(8,128)(2,1)S(1)}, bf16[8,32,256]{2,1,0:T(8,128)(2,1)S(1)}, u32[]{:S(2)}, u32[]{:S(2)}) collective-permute-start(bf16[8,32,256]{2,1,0:T(8,128)(2,1)S(1)} %shard_map.200.b0), channel_id=1, source_target_pairs={{0,4},{4,0},{8,12},{12,8},{16,20},{20,16},{24,28},{28,24},{32,36},... | collective-permute-start | bytes 393224 | tf_op jit(solution)/shard_map/ppermute | solution.py:397
  93.0 5.7 %collective-permute-start.15 = (bf16[8,32,256]{2,1,0:T(8,128)(2,1)S(1)}, bf16[8,32,256]{2,1,0:T(8,128)(2,1)S(1)}, u32[]{:S(2)}, u32[]{:S(2)}) collective-permute-start(bf16[8,32,256]{2,1,0:T(8,128)(2,1)S(1)} %collective-permute-done.14.b2), channel_id=1, source_target_pairs={{0,4},{4,0},{8,12},{12,8},{16,20},{20,16},{24,28},{28,24},{32,36},... | collective-permute-start | bytes 393224 | tf_op jit(solution)/shard_map/ppermute | solution.py:397
  93.2 5.5 %collective-permute-start.17 = (bf16[8,32,256]{2,1,0:T(8,128)(2,1)S(1)}, bf16[8,32,256]{2,1,0:T(8,128)(2,1)S(1)}, u32[]{:S(2)}, u32[]{:S(2)}) collective-permute-start(bf16[8,32,256]{2,1,0:T(8,128)(2,1)S(1)} %collective-permute-done.16.b4), channel_id=1, source_target_pairs={{0,4},{4,0},{8,12},{12,8},{16,20},{20,16},{24,28},{28,24},{32,36},... | collective-permute-start | bytes 393224 | tf_op jit(solution)/shard_map/ppermute | solution.py:397
  95.8 2.9 %collective-permute-start.19 = (bf16[8,32,256]{2,1,0:T(8,128)(2,1)S(1)}, bf16[8,32,256]{2,1,0:T(8,128)(2,1)S(1)}, u32[]{:S(2)}, u32[]{:S(2)}) collective-permute-start(bf16[8,32,256]{2,1,0:T(8,128)(2,1)S(1)} %collective-permute-done.18.b6), channel_id=1, source_target_pairs={{0,4},{4,0},{8,12},{12,8},{16,20},{20,16},{24,28},{28,24},{32,36},... | collective-permute-start | bytes 393224 | tf_op jit(solution)/shard_map/ppermute | solution.py:397
  100.5 3.9 %collective-permute-start.20 = (bf16[16,512]{1,0:T(8,128)(2,1)S(1)}, bf16[16,512]{1,0:T(8,128)(2,1)S(1)}, u32[]{:S(2)}, u32[]{:S(2)}) collective-permute-start(bf16[16,512]{1,0:T(8,128)(2,1)S(1)} %get-tuple-element.46), channel_id=1, source_target_pairs={{0,1},{1,2},{2,3},{3,0},{4,5},{5,6},{6,7},{7,4},{8,9},{9,10},{10,1... | collective-permute-start | bytes 49160 | tf_op jit(solution)/shard_map/ppermute | solution.py:455
  100.6 4.2 %collective-permute-start.21 = (bf16[16,512]{1,0:T(8,128)(2,1)S(1)}, bf16[16,512]{1,0:T(8,128)(2,1)S(1)}, u32[]{:S(2)}, u32[]{:S(2)}) collective-permute-start(bf16[16,512]{1,0:T(8,128)(2,1)S(1)} %get-tuple-element.47), channel_id=1, source_target_pairs={{0,2},{1,3},{2,0},{3,1},{4,6},{5,7},{6,4},{7,5},{8,10},{9,11},{10,... | collective-permute-start | bytes 49160 | tf_op jit(solution)/shard_map/ppermute | solution.py:455
  (11 other events, 618.1 us)

commit v5 on v4

--- a/solution.py
+++ b/solution.py
@@ -82,18 +82,19 @@
     wq_c.start()
     cache_c = []
     for n in range(rows):
-        c = pltpu.make_async_copy(cache_hbm.at[n], cache_v.at[n], sem_c.at[n])
+        cache_c.append(pltpu.make_async_copy(cache_hbm.at[n], cache_v.at[n], sem_c.at[n]))
+    for c in cache_c[:8]:
         c.start()
-        cache_c.append(c)
     len_c.start()
     bias_c.start()
-    wo_c.start()
     half = sg_hbm.shape[1]
     joins = copy_all([(sg_hbm, joined_ref.at[0, :, :half]), (su_hbm, joined_ref.at[0, :, half:])], sem_w, 7)
     routes_c.wait()
     make_pick(routes_v, pick_ref)
     tok_c.wait()
     gain_c.wait()
+    for c in cache_c[8:12]:
+        c.start()
     x = tok_ref[...].astype(f32)
     ms = jnp.mean(x * x, axis=-1, keepdims=True)
     normed = (x * lax.rsqrt(ms + EPS) * gain_ref[...]).astype(bf16)
@@ -102,17 +103,19 @@
     row = iota((hr, heads * HEAD_DIM), 0)
     fold = ((iota((256, 128), 0) % HEAD_DIM) == iota((256, 128), 1)).astype(bf16)
     wq_c.wait()
+    for c in cache_c[12:]:
+        c.start()
+    wo_c.start()
     q = dot(normed, wq_v[...]).astype(bf16)
     qx = jnp.where(lane // HEAD_DIM == row % heads, dot(expand, q), 0.0).astype(bf16)
-    qk = (dot(qx, fold) * (HEAD_DIM**-0.5)).astype(bf16)
-    wide_q = jnp.concatenate([qk] * 4, axis=1)
-    own_seq = iota(wide_q.shape, 1) // 128 == (iota(wide_q.shape, 0) // heads) % 4
-    wide_q = jnp.where(own_seq, wide_q.astype(f32), 0.0).astype(bf16)
+    fold4 = ((iota((256, 256), 0) % HEAD_DIM) == (iota((256, 256), 1) % HEAD_DIM)).astype(bf16)
+    narrow_q = dot(qx, fold4) * (HEAD_DIM**-0.5)
+    narrow_q = jnp.where(lane // HEAD_DIM == (row // heads) % 4, narrow_q, 0.0).astype(bf16)
     for g in range(rows // 4):
         for n in range(4 * g, 4 * g + 4):
             cache_c[n].wait()
-        keys = jnp.concatenate([cache_v[n] for n in range(4 * g, 4 * g + 4)], axis=1)
-        s_v[16 * g : 16 * g + 16, :] = dot(wide_q[16 * g : 16 * g + 16, :], keys, ((1,), (1,)))
+        keys = jnp.concatenate([cache_v[n][:, :HEAD_DIM] for n in range(4 * g, 4 * g + 4)], axis=1)
+        s_v[16 * g : 16 * g + 16, :] = dot(narrow_q[16 * g : 16 * g + 16, :], keys, ((1,), (1,)))
     rid = iota((hr, 128), 0)
     lens = jnp.zeros((hr, 128), jnp.int32)
     bias = jnp.zeros((hr, 128), f32)
@@ -287,7 +290,8 @@
     base_ref[...] = residual_v[...] + gate_ref[:, :1] * all_v[:, cols[0]]
 
 
-def expert_kernel(arrived_ref, wg_ref, wu_ref, hidden_ref, x_v):
+def expert_kernel(arrived_ref, wg_ref, wu_ref, d0, d1, d2, d3, hidden_ref, downs_ref, x_v, sems):
+    fetches = copy_all([(w, downs_ref.at[k]) for k, w in enumerate((d0, d1, d2, d3))], sems)
     n = arrived_ref.shape[0]
     peers = n // 8
     wide = arrived_ref.shape[1] // CAP
@@ -304,20 +308,20 @@
     gate = dot(x, wg_ref[0])
     up = dot(x, wu_ref[0])
     hidden_ref[...] = (silu(gate) * up).astype(bf16)
-
-
-def down_kernel(h0, h1, h2, h3, w0, w1, w2, w3, back_ref, w_v, sems):
-    n = back_ref.shape[0]
+    for c in fetches:
+        c.wait()
+
+
+def down_kernel(h0, h1, h2, h3, w_ref, back_hbm, back_v, sems):
+    n = back_v.shape[0]
     peers = n // 8
     m = CAP * peers
-    copies = copy_all([(w, w_v.at[k]) for k, w in enumerate((w0, w1, w2, w3))], sems)
     a = iota((n, 2 * m), 0)
     b = iota((n, 2 * m), 1)
     order = ((a % 8 == b // peers) & (a // 8 == b % peers)).astype(bf16)
     acc = None
     for k, h in enumerate((h0, h1, h2, h3)):
-        copies[k].wait()
-        part = dot(h[:m, :], w_v[k])
+        part = dot(h[...], w_ref[k])
         acc = part if acc is None else acc + part
     out = acc.astype(bf16)
     half = out.shape[1] // 2
@@ -325,7 +329,13 @@
         out[k * peers : (k + 1) * peers, h * half : (h + 1) * half] for k in range(CAP) for h in range(2)
     ]
     rhs = jnp.concatenate(pieces, axis=0)
-    back_ref[...] = dot(order, rhs).astype(bf16)
+    sends = []
+    for i in range(2):
+        at = slice(i * n // 2, (i + 1) * n // 2)
+        back_v[at, :] = dot(order[at, :], rhs).astype(bf16)
+        sends += copy_all([(back_v.at[at, :], back_hbm.at[at, :])], sems, 4 + i)
+    for c in sends:
+        c.wait()
 
 
 def side_kernel(routes_ref, rw_ref, tok_hbm, gain_ref, kw_hbm, vw_hbm, mixed_hbm, gv_ref,
@@ -429,17 +439,18 @@
                  pltpu.SemaphoreType.DMA((4,))],
     )
     m = CAP * nep
-    (hidden,) = call(
-        expert_kernel, [((m, expert_gate.shape[2]), bf16)],
-        (arrived, expert_gate, expert_up), scratch=[pltpu.VMEM((m, d), bf16)],
+    hidden, downs = call(
+        expert_kernel, [((m, f), bf16), ((ntp, f, quarter), bf16)],
+        (arrived, expert_gate, expert_up, *downs), in_specs=[VM] * 3 + [HBM] * 4,
+        scratch=[pltpu.VMEM((m, d), bf16), pltpu.SemaphoreType.DMA((4,))],
     )
     hiddens = [hidden] + [lax.ppermute(hidden, "tp", around(k, ntp)) for k in range(1, ntp)]
     (column,) = call(stack_kernel, [((8, *joined.shape[1:]), bf16)], (after(near, hidden), low, high))
     planes = [column] + [shift(column, 0, k, 0) for k in range(1, 4)]
     blocks = [column, shift(column, 0, 0, 1)]
     (back,) = call(
-        down_kernel, [((n_pick, quarter // 2), bf16)], (*hiddens, *downs), in_specs=[VM] * 4 + [HBM] * 4,
-        scratch=[pltpu.VMEM((ntp, expert_down.shape[1], quarter), bf16), pltpu.SemaphoreType.DMA((4,))],
+        down_kernel, [((n_pick, quarter // 2), bf16)], (*hiddens, downs), out_specs=[HBM],
+        scratch=[pltpu.VMEM((n_pick, quarter // 2), bf16), pltpu.SemaphoreType.DMA((6,))],
     )
     returned = lax.all_to_all(back.reshape(nep, 8, -1), "ep", 0, 0, tiled=True)
     returned = returned.reshape(n_pick, -1)

time: 108 us -> 111 us (1.028)
  waiting for transfers between devices: 28.7 us -> 35.2 us
  starting transfers between devices: 58.6 us -> 55.8 us
  Pallas kernels: 18.6 us -> 17 us
  local copies, waits for them, and re-layouts: 0.06 us -> 1.44 us
    ppermute x11, waiting for transfers between devices: 16.3 us -> 20.1 us  [shift(): return lax.ppermute(value, 'ep', perm)]
    ppermute x3, waiting for transfers between devices: 3.82 us -> 6.92 us  [shards(): lax.ppermute(hidden, 'tp', around(k, ntp))]
    pallas_call x9, Pallas kernels: 18.6 us -> 17 us  [call(): pl.pallas_call(kernel, out_shape=tuple(shapes), in_specs=in_specs, out_sp...]
    unnamed x22 -> x26, local copies, waits for them, and re-layouts: 0.06 us -> 1.44 us
    all_to_all x1, waiting for transfers between devices: 3.92 us -> 2.63 us  [shards(): arrived = lax.all_to_all(sent.reshape(nep, 8, -1), 'ep', 0, 0, tiled=True)]
    ppermute x3, starting transfers between devices: 6.32 us -> 5.1 us  [shards(): others = [lax.ppermute(partial, 'tp', around(k, ntp)) for k in (2, 1, 3)]]
  transfers between devices with their start and end apart: 25 -> 25, of which waited for: 10 -> 14; matrix products, arithmetic and copies ran while one was open for 0% -> 0% of each run, Pallas kernels for 7% -> 6%
where the time goes in v5:
time: 111 us; the launch traced here: 110 us
  starting transfers between devices  55.8 us (50%)
  waiting for transfers between devices  35.2 us (32%)
  Pallas kernels  17 us (15%)
  local copies, waits for them, and re-layouts  1.44 us (1%)
    ppermute x11, waiting for transfers between devices, shift(): return lax.ppermute(value, 'ep', perm)  20.1 us
    ppermute x11, starting transfers between devices, shift(): return lax.ppermute(value, 'ep', perm)  19.6 us
    pallas_call x9, Pallas kernels, call(): pl.pallas_call(kernel, out_shape=tuple(shapes), in_specs=in_specs, out_sp...  17 us
    all_to_all x1, starting transfers between devices, shards(): arrived = lax.all_to_all(sent.reshape(nep, 8, -1), 'ep', 0, 0, tiled=True)  13.7 us
    all_to_all x1, starting transfers between devices, shards(): returned = lax.all_to_all(back.reshape(nep, 8, -1), 'ep', 0, 0, tiled=True)  7.64 us
    ppermute x3, waiting for transfers between devices, shards(): lax.ppermute(hidden, 'tp', around(k, ntp))  6.92 us
    ppermute x3, starting transfers between devices, shards(): others = [lax.ppermute(partial, 'tp', around(k, ntp)) for k in (2, 1, 3)]  5.1 us
    ppermute x3, starting transfers between devices, shards(): lax.ppermute(cuts[k], 'tp', around(k, ntp))  3.74 us
  transfers between devices with their start and end apart: 25, of which 14 were waited for; matrix products, arithmetic and copies ran while one was open for 0% of the time, Pallas kernels for 6%

profile of v5, /device:TPU:1, one launch (start us, length us, event | category | flops | bytes accessed | tf_op | source)
XLA Modules:
  0.0 110.5 jit_solution(10898443475522753778)
XLA Ops:
  0.7 5.9 %shard_map.194 = (bf16[16,2048]{1,0:T(8,128)(2,1)S(1)}, bf16[512,384]{1,0:T(8,128)(2,1)S(1)}, bf16[1,32,256]{2,1,0:T(8,128)(2,1)S(1)}) custom-call(s32[16]{0:T(128)} %len_hbm.1, f32[4]{0:T(128)} %bias_hbm.1, bf16[16,2048]{1,0:T(8,128)(2,1)} %tok_hbm.2, f32[1,2048]{1,0:T(1,128)} %bitcast.15, bf16[16,1024,128]{2,1,0:T(8,128)(2,1)} %cache_hbm.1, ...), custom_call_target="tpu_custom_call" | custom-call | tf_op jit(solution)/shard_map/pallas_call | solution.py:47
  6.6 3.4 %collective-permute-start.2 = (bf16[16,2048]{1,0:T(8,128)(2,1)S(1)}, bf16[16,2048]{1,0:T(8,128)(2,1)S(1)}, u32[]{:S(2)}, u32[]{:S(2)}) collective-permute-start(bf16[16,2048]{1,0:T(8,128)(2,1)S(1)} %get-tuple-element.28.p0), channel_id=1, source_target_pairs={{0,3},{1,0},{2,1},{3,2},{4,7},{5,4},{6,5},{7,6},{8,11},{9,8},{10,9... | collective-permute-start | bytes 196616 | tf_op jit(solution)/shard_map/ppermute | solution.py:412
  10.0 1.7 %collective-permute-start = (bf16[16,2048]{1,0:T(8,128)(2,1)S(1)}, bf16[16,2048]{1,0:T(8,128)(2,1)S(1)}, u32[]{:S(2)}, u32[]{:S(2)}) collective-permute-start(bf16[16,2048]{1,0:T(8,128)(2,1)S(1)} %get-tuple-element.28.p0), channel_id=1, source_target_pairs={{0,2},{1,3},{2,0},{3,1},{4,6},{5,7},{6,4},{7,5},{8,10},{9,11},{10,... | collective-permute-start | bytes 196616 | tf_op jit(solution)/shard_map/ppermute | solution.py:412
  11.7 3.2 %collective-permute-done.1.p2 = bf16[16,2048]{1,0:T(8,128)(2,1)S(1)} collective-permute-done((bf16[16,2048]{1,0:T(8,128)(2,1)S(1)}, bf16[16,2048]{1,0:T(8,128)(2,1)S(1)}, u32[]{:S(2)}, u32[]{:S(2)}) %collective-permute-start.1) | collective-permute-done | bytes 65568 | tf_op jit(solution)/shard_map/ppermute | solution.py:412
  16.5 13.7 %all-to-all-start = ((bf16[64,8,768]{2,1,0:T(8,128)(2,1)}), bf16[64,8,768]{2,1,0:T(8,128)(2,1)S(1)}, u32[]{:S(2)}, u32[]{:S(2)}) async-start(bf16[64,8,768]{2,1,0:T(8,128)(2,1)} %bitcast.23), calls=%async_computation | async-start | bytes 1572864 | tf_op jit(solution)/shard_map/all_to_all | solution.py:421
  30.3 2.3 %shard_map.196 = (bf16[256,512]{1,0:T(8,128)(2,1)}, bf16[256,512]{1,0:T(8,128)(2,1)}, bf16[256,512]{1,0:T(8,128)(2,1)}, bf16[256,512]{1,0:T(8,128)(2,1)}) custom-call(s32[1]{0:T(128)} %bitcast.part_ref, bf16[1,256,2048]{2,1,0:T(8,128)(2,1)} %down_hbm), custom_call_target="tpu_custom_call" | custom-call | tf_op jit(solution)/shard_map/pallas_call | solution.py:47
  32.7 3.7 %collective-permute-start.4 = (bf16[256,512]{1,0:T(8,128)(2,1)}, bf16[256,512]{1,0:T(8,128)(2,1)S(1)}, u32[]{:S(2)}, u32[]{:S(2)}) collective-permute-start(bf16[256,512]{1,0:T(8,128)(2,1)} %get-tuple-element.34), channel_id=1, source_target_pairs={{0,2},{1,3},{2,0},{3,1},{4,6},{5,7},{6,4},{7,5},{8,10},{9,11},{10,... | collective-permute-start | bytes 786440 | tf_op jit(solution)/shard_map/ppermute | solution.py:431
  36.4 2.8 %collective-permute-start.10 = (bf16[1,32,256]{2,1,0:T(8,128)(2,1)S(1)}, bf16[1,32,256]{2,1,0:T(8,128)(2,1)S(1)}, u32[]{:S(2)}, u32[]{:S(2)}) collective-permute-start(bf16[1,32,256]{2,1,0:T(8,128)(2,1)S(1)} %get-tuple-element.45), channel_id=1, source_target_pairs={{0,224},{4,228},{8,232},{12,236},{16,240},{20,244},{24,248},{28,25... | collective-permute-start | bytes 49160 | tf_op jit(solution)/shard_map/ppermute | solution.py:407
  39.2 10.0 %collective-permute-done.10 = bf16[1,32,256]{2,1,0:T(8,128)(2,1)S(1)} collective-permute-done((bf16[1,32,256]{2,1,0:T(8,128)(2,1)S(1)}, bf16[1,32,256]{2,1,0:T(8,128)(2,1)S(1)}, u32[]{:S(2)}, u32[]{:S(2)}) %collective-permute-start.10) | collective-permute-done | bytes 16416 | tf_op jit(solution)/shard_map/ppermute | solution.py:407
  50.6 2.6 %all-to-all-done = bf16[64,8,768]{2,1,0:T(8,128)(2,1)S(1)} async-done(((bf16[64,8,768]{2,1,0:T(8,128)(2,1)}), bf16[64,8,768]{2,1,0:T(8,128)(2,1)S(1)}, u32[]{:S(2)}, u32[]{:S(2)}) %all-to-all-start) | async-done | bytes 786464 | tf_op jit(solution)/shard_map/all_to_all | solution.py:421
  54.5 2.6 %collective-permute-start.8 = (bf16[192,256]{1,0:T(8,128)(2,1)S(1)}, bf16[192,256]{1,0:T(8,128)(2,1)S(1)}, u32[]{:S(2)}, u32[]{:S(2)}) collective-permute-start(bf16[192,256]{1,0:T(8,128)(2,1)S(1)} %get-tuple-element.36.h0), channel_id=1, source_target_pairs={{0,3},{1,0},{2,1},{3,2},{4,7},{5,4},{6,5},{7,6},{8,11},{9,8},{10,9... | collective-permute-start | bytes 294920 | tf_op jit(solution)/shard_map/ppermute | solution.py:447
  59.2 2.9 %collective-permute-done.7.h2 = bf16[192,256]{1,0:T(8,128)(2,1)S(1)} collective-permute-done((bf16[192,256]{1,0:T(8,128)(2,1)S(1)}, bf16[192,256]{1,0:T(8,128)(2,1)S(1)}, u32[]{:S(2)}, u32[]{:S(2)}) %collective-permute-start.7) | collective-permute-done | bytes 98336 | tf_op jit(solution)/shard_map/ppermute | solution.py:447
  62.2 2.5 %collective-permute-done.6.h1 = bf16[192,256]{1,0:T(8,128)(2,1)S(1)} collective-permute-done((bf16[192,256]{1,0:T(8,128)(2,1)S(1)}, bf16[192,256]{1,0:T(8,128)(2,1)S(1)}, u32[]{:S(2)}, u32[]{:S(2)}) %collective-permute-start.6) | collective-permute-done | bytes 98336 | tf_op jit(solution)/shard_map/ppermute | solution.py:447
  66.1 7.6 %all-to-all-start.1 = ((bf16[64,8,256]{2,1,0:T(8,128)(2,1)}), bf16[64,8,256]{2,1,0:T(8,128)(2,1)S(1)}, u32[]{:S(2)}, u32[]{:S(2)}) async-start(bf16[64,8,256]{2,1,0:T(8,128)(2,1)} %bitcast.22), calls=%async_computation.1 | async-start | bytes 524288 | tf_op jit(solution)/shard_map/all_to_all | solution.py:455
  73.8 4.6 %collective-permute-start.12 = (bf16[3,32,256]{2,1,0:T(8,128)(2,1)S(1)}, bf16[3,32,256]{2,1,0:T(8,128)(2,1)S(1)}, u32[]{:S(2)}, u32[]{:S(2)}) collective-permute-start(bf16[3,32,256]{2,1,0:T(8,128)(2,1)S(1)} %constant_dynamic-update-slice_fusion.near_ref), channel_id=1, source_target_pairs={{0,160},{4,164},{8,168},{12,172},{16,176},{20,180},{24,184},{28,18... | collective-permute-start | bytes 147464 | tf_op jit(solution)/shard_map/ppermute | solution.py:407
  78.4 4.2 %collective-permute-done.12.high_ref = bf16[3,32,256]{2,1,0:T(8,128)(2,1)S(1)} collective-permute-done((bf16[3,32,256]{2,1,0:T(8,128)(2,1)S(1)}, bf16[3,32,256]{2,1,0:T(8,128)(2,1)S(1)}, u32[]{:S(2)}, u32[]{:S(2)}) %collective-permute-start.12) | collective-permute-done | bytes 49184 | tf_op jit(solution)/shard_map/ppermute | solution.py:407
  82.5 3.0 %collective-permute-done.11.low_ref = bf16[3,32,256]{2,1,0:T(8,128)(2,1)S(1)} collective-permute-done((bf16[3,32,256]{2,1,0:T(8,128)(2,1)S(1)}, bf16[3,32,256]{2,1,0:T(8,128)(2,1)S(1)}, u32[]{:S(2)}, u32[]{:S(2)}) %collective-permute-start.11) | collective-permute-done | bytes 49184 | tf_op jit(solution)/shard_map/ppermute | solution.py:407
  85.5 4.9 %collective-permute-start.18 = (bf16[8,32,256]{2,1,0:T(8,128)(2,1)S(1)}, bf16[8,32,256]{2,1,0:T(8,128)(2,1)S(1)}, u32[]{:S(2)}, u32[]{:S(2)}) collective-permute-start(bf16[8,32,256]{2,1,0:T(8,128)(2,1)S(1)} %shard_map.200.b0), channel_id=1, source_target_pairs={{0,24},{4,28},{8,0},{12,4},{16,8},{20,12},{24,16},{28,20},{32,56},... | collective-permute-start | bytes 393224 | tf_op jit(solution)/shard_map/ppermute | solution.py:407
  91.2 2.0 %collective-permute-start.13 = (bf16[8,32,256]{2,1,0:T(8,128)(2,1)S(1)}, bf16[8,32,256]{2,1,0:T(8,128)(2,1)S(1)}, u32[]{:S(2)}, u32[]{:S(2)}) collective-permute-start(bf16[8,32,256]{2,1,0:T(8,128)(2,1)S(1)} %shard_map.200.b0), channel_id=1, source_target_pairs={{0,4},{4,0},{8,12},{12,8},{16,20},{20,16},{24,28},{28,24},{32,36},... | collective-permute-start | bytes 393224 | tf_op jit(solution)/shard_map/ppermute | solution.py:407
  93.2 2.3 %collective-permute-done.18.b6 = bf16[8,32,256]{2,1,0:T(8,128)(2,1)S(1)} collective-permute-done((bf16[8,32,256]{2,1,0:T(8,128)(2,1)S(1)}, bf16[8,32,256]{2,1,0:T(8,128)(2,1)S(1)}, u32[]{:S(2)}, u32[]{:S(2)}) %collective-permute-start.18) | collective-permute-done | bytes 131104 | tf_op jit(solution)/shard_map/ppermute | solution.py:407
  96.9 2.3 %collective-permute-start.17 = (bf16[8,32,256]{2,1,0:T(8,128)(2,1)S(1)}, bf16[8,32,256]{2,1,0:T(8,128)(2,1)S(1)}, u32[]{:S(2)}, u32[]{:S(2)}) collective-permute-start(bf16[8,32,256]{2,1,0:T(8,128)(2,1)S(1)} %collective-permute-done.16.b4), channel_id=1, source_target_pairs={{0,4},{4,0},{8,12},{12,8},{16,20},{20,16},{24,28},{28,24},{32,36},... | collective-permute-start | bytes 393224 | tf_op jit(solution)/shard_map/ppermute | solution.py:407
  100.7 2.2 %shard_map.199 = (bf16[96,512]{1,0:T(8,128)(2,1)S(1)}, bf16[16,128]{1,0:T(8,128)(2,1)}, f32[16,128]{1,0:T(8,128)S(1)}) custom-call(s32[6,16]{1,0:T(8,128)S(1)} %bitcast.18, f32[6,16]{1,0:T(8,128)S(1)} %bitcast.20, bf16[16,2048]{1,0:T(8,128)(2,1)} %tok_hbm.2, f32[1,2048]{1,0:T(1,128)S(1)} %bitcast.16, bf16[64,2048]{1,0:T(8,128)(2,1)} %bitcast.24, ...), custom_call_target="tpu_custom_call" | custom-call | tf_op jit(solution)/shard_map/pallas_call | solution.py:47
  103.0 1.7 %shard_map.201 = (f32[16,512]{1,0:T(8,128)S(1)}, bf16[16,512]{1,0:T(8,128)(2,1)S(1)}, bf16[16,512]{1,0:T(8,128)(2,1)S(1)}, bf16[16,512]{1,0:T(8,128)(2,1)S(1)}) custom-call(s32[2]{0:T(128)S(1)} %pad_add_fusion.at_ref, bf16[16,2048]{1,0:T(8,128)(2,1)S(1)} %copy-done.4, bf16[128,2048]{1,0:T(8,128)(2,1)S(1)} %copy-done.3, ...), custom_call_target="tpu_custom_call" | custom-call | tf_op jit(solution)/shard_map/pallas_call | solution.py:47
  104.8 1.8 %collective-permute-start.21 = (bf16[16,512]{1,0:T(8,128)(2,1)S(1)}, bf16[16,512]{1,0:T(8,128)(2,1)S(1)}, u32[]{:S(2)}, u32[]{:S(2)}) collective-permute-start(bf16[16,512]{1,0:T(8,128)(2,1)S(1)} %get-tuple-element.51), channel_id=1, source_target_pairs={{0,2},{1,3},{2,0},{3,1},{4,6},{5,7},{6,4},{7,5},{8,10},{9,11},{10,... | collective-permute-start | bytes 49160 | tf_op jit(solution)/shard_map/ppermute | solution.py:466
  (63 shorter events, 15.6 us)
Async XLA Ops:
  6.6 5.1 %collective-permute-start.2 = (bf16[16,2048]{1,0:T(8,128)(2,1)S(1)}, bf16[16,2048]{1,0:T(8,128)(2,1)S(1)}, u32[]{:S(2)}, u32[]{:S(2)}) collective-permute-start(bf16[16,2048]{1,0:T(8,128)(2,1)S(1)} %get-tuple-element.28.p0), channel_id=1, source_target_pairs={{0,3},{1,0},{2,1},{3,2},{4,7},{5,4},{6,5},{7,6},{8,11},{9,8},{10,9... | collective-permute-start | bytes 196616 | tf_op jit(solution)/shard_map/ppermute | solution.py:412
  10.0 4.9 %collective-permute-start.1 = (bf16[16,2048]{1,0:T(8,128)(2,1)S(1)}, bf16[16,2048]{1,0:T(8,128)(2,1)S(1)}, u32[]{:S(2)}, u32[]{:S(2)}) collective-permute-start(bf16[16,2048]{1,0:T(8,128)(2,1)S(1)} %get-tuple-element.28.p0), channel_id=1, source_target_pairs={{0,1},{1,2},{2,3},{3,0},{4,5},{5,6},{6,7},{7,4},{8,9},{9,10},{10,1... | collective-permute-start | bytes 196616 | tf_op jit(solution)/shard_map/ppermute | solution.py:412
  10.0 5.1 %collective-permute-start = (bf16[16,2048]{1,0:T(8,128)(2,1)S(1)}, bf16[16,2048]{1,0:T(8,128)(2,1)S(1)}, u32[]{:S(2)}, u32[]{:S(2)}) collective-permute-start(bf16[16,2048]{1,0:T(8,128)(2,1)S(1)} %get-tuple-element.28.p0), channel_id=1, source_target_pairs={{0,2},{1,3},{2,0},{3,1},{4,6},{5,7},{6,4},{7,5},{8,10},{9,11},{10,... | collective-permute-start | bytes 196616 | tf_op jit(solution)/shard_map/ppermute | solution.py:412
  16.5 36.7 %all-to-all-start = ((bf16[64,8,768]{2,1,0:T(8,128)(2,1)}), bf16[64,8,768]{2,1,0:T(8,128)(2,1)S(1)}, u32[]{:S(2)}, u32[]{:S(2)}) async-start(bf16[64,8,768]{2,1,0:T(8,128)(2,1)} %bitcast.23), calls=%async_computation | async-start | bytes 1572864 | tf_op jit(solution)/shard_map/all_to_all | solution.py:421
  32.6 16.6 %collective-permute-start.3 = (bf16[256,512]{1,0:T(8,128)(2,1)}, bf16[256,512]{1,0:T(8,128)(2,1)S(1)}, u32[]{:S(2)}, u32[]{:S(2)}) collective-permute-start(bf16[256,512]{1,0:T(8,128)(2,1)} %get-tuple-element.33), channel_id=1, source_target_pairs={{0,1},{1,2},{2,3},{3,0},{4,5},{5,6},{6,7},{7,4},{8,9},{9,10},{10,1... | collective-permute-start | bytes 786440 | tf_op jit(solution)/shard_map/ppermute | solution.py:431
  32.7 16.5 %collective-permute-start.4 = (bf16[256,512]{1,0:T(8,128)(2,1)}, bf16[256,512]{1,0:T(8,128)(2,1)S(1)}, u32[]{:S(2)}, u32[]{:S(2)}) collective-permute-start(bf16[256,512]{1,0:T(8,128)(2,1)} %get-tuple-element.34), channel_id=1, source_target_pairs={{0,2},{1,3},{2,0},{3,1},{4,6},{5,7},{6,4},{7,5},{8,10},{9,11},{10,... | collective-permute-start | bytes 786440 | tf_op jit(solution)/shard_map/ppermute | solution.py:431
  36.4 14.3 %collective-permute-start.5 = (bf16[256,512]{1,0:T(8,128)(2,1)}, bf16[256,512]{1,0:T(8,128)(2,1)}, u32[]{:S(2)}, u32[]{:S(2)}) collective-permute-start(bf16[256,512]{1,0:T(8,128)(2,1)} %get-tuple-element.35), channel_id=1, source_target_pairs={{0,3},{1,0},{2,1},{3,2},{4,7},{5,4},{6,5},{7,6},{8,11},{9,8},{10,9... | collective-permute-start | bytes 786440 | tf_op jit(solution)/shard_map/ppermute | solution.py:431
  36.4 12.9 %collective-permute-start.10 = (bf16[1,32,256]{2,1,0:T(8,128)(2,1)S(1)}, bf16[1,32,256]{2,1,0:T(8,128)(2,1)S(1)}, u32[]{:S(2)}, u32[]{:S(2)}) collective-permute-start(bf16[1,32,256]{2,1,0:T(8,128)(2,1)S(1)} %get-tuple-element.45), channel_id=1, source_target_pairs={{0,224},{4,228},{8,232},{12,236},{16,240},{20,244},{24,248},{28,25... | collective-permute-start | bytes 49160 | tf_op jit(solution)/shard_map/ppermute | solution.py:407
  39.2 10.0 %collective-permute-start.9 = (bf16[1,32,256]{2,1,0:T(8,128)(2,1)S(1)}, bf16[1,32,256]{2,1,0:T(8,128)(2,1)S(1)}, u32[]{:S(2)}, u32[]{:S(2)}) collective-permute-start(bf16[1,32,256]{2,1,0:T(8,128)(2,1)S(1)} %get-tuple-element.45), channel_id=1, source_target_pairs={{0,32},{4,36},{8,40},{12,44},{16,48},{20,52},{24,56},{28,60},{32,6... | collective-permute-start | bytes 49160 | tf_op jit(solution)/shard_map/ppermute | solution.py:407
  54.5 4.7 %collective-permute-start.8 = (bf16[192,256]{1,0:T(8,128)(2,1)S(1)}, bf16[192,256]{1,0:T(8,128)(2,1)S(1)}, u32[]{:S(2)}, u32[]{:S(2)}) collective-permute-start(bf16[192,256]{1,0:T(8,128)(2,1)S(1)} %get-tuple-element.36.h0), channel_id=1, source_target_pairs={{0,3},{1,0},{2,1},{3,2},{4,7},{5,4},{6,5},{7,6},{8,11},{9,8},{10,9... | collective-permute-start | bytes 294920 | tf_op jit(solution)/shard_map/ppermute | solution.py:447
  57.1 5.1 %collective-permute-start.7 = (bf16[192,256]{1,0:T(8,128)(2,1)S(1)}, bf16[192,256]{1,0:T(8,128)(2,1)S(1)}, u32[]{:S(2)}, u32[]{:S(2)}) collective-permute-start(bf16[192,256]{1,0:T(8,128)(2,1)S(1)} %get-tuple-element.36.h0), channel_id=1, source_target_pairs={{0,2},{1,3},{2,0},{3,1},{4,6},{5,7},{6,4},{7,5},{8,10},{9,11},{10,... | collective-permute-start | bytes 294920 | tf_op jit(solution)/shard_map/ppermute | solution.py:447
  57.1 7.6 %collective-permute-start.6 = (bf16[192,256]{1,0:T(8,128)(2,1)S(1)}, bf16[192,256]{1,0:T(8,128)(2,1)S(1)}, u32[]{:S(2)}, u32[]{:S(2)}) collective-permute-start(bf16[192,256]{1,0:T(8,128)(2,1)S(1)} %get-tuple-element.36.h0), channel_id=1, source_target_pairs={{0,1},{1,2},{2,3},{3,0},{4,5},{5,6},{6,7},{7,4},{8,9},{9,10},{10,1... | collective-permute-start | bytes 294920 | tf_op jit(solution)/shard_map/ppermute | solution.py:447
  66.1 43.5 %all-to-all-start.1 = ((bf16[64,8,256]{2,1,0:T(8,128)(2,1)}), bf16[64,8,256]{2,1,0:T(8,128)(2,1)S(1)}, u32[]{:S(2)}, u32[]{:S(2)}) async-start(bf16[64,8,256]{2,1,0:T(8,128)(2,1)} %bitcast.22), calls=%async_computation.1 | async-start | bytes 524288 | tf_op jit(solution)/shard_map/all_to_all | solution.py:455
  73.8 8.8 %collective-permute-start.12 = (bf16[3,32,256]{2,1,0:T(8,128)(2,1)S(1)}, bf16[3,32,256]{2,1,0:T(8,128)(2,1)S(1)}, u32[]{:S(2)}, u32[]{:S(2)}) collective-permute-start(bf16[3,32,256]{2,1,0:T(8,128)(2,1)S(1)} %constant_dynamic-update-slice_fusion.near_ref), channel_id=1, source_target_pairs={{0,160},{4,164},{8,168},{12,172},{16,176},{20,180},{24,184},{28,18... | collective-permute-start | bytes 147464 | tf_op jit(solution)/shard_map/ppermute | solution.py:407
  78.4 7.1 %collective-permute-start.11 = (bf16[3,32,256]{2,1,0:T(8,128)(2,1)S(1)}, bf16[3,32,256]{2,1,0:T(8,128)(2,1)S(1)}, u32[]{:S(2)}, u32[]{:S(2)}) collective-permute-start(bf16[3,32,256]{2,1,0:T(8,128)(2,1)S(1)} %constant_dynamic-update-slice_fusion.near_ref), channel_id=1, source_target_pairs={{0,96},{4,100},{8,104},{12,108},{16,112},{20,116},{24,120},{28,124... | collective-permute-start | bytes 147464 | tf_op jit(solution)/shard_map/ppermute | solution.py:407
  85.5 10.0 %collective-permute-start.18 = (bf16[8,32,256]{2,1,0:T(8,128)(2,1)S(1)}, bf16[8,32,256]{2,1,0:T(8,128)(2,1)S(1)}, u32[]{:S(2)}, u32[]{:S(2)}) collective-permute-start(bf16[8,32,256]{2,1,0:T(8,128)(2,1)S(1)} %shard_map.200.b0), channel_id=1, source_target_pairs={{0,24},{4,28},{8,0},{12,4},{16,8},{20,12},{24,16},{28,20},{32,56},... | collective-permute-start | bytes 393224 | tf_op jit(solution)/shard_map/ppermute | solution.py:407
  90.4 6.5 %collective-permute-start.16 = (bf16[8,32,256]{2,1,0:T(8,128)(2,1)S(1)}, bf16[8,32,256]{2,1,0:T(8,128)(2,1)S(1)}, u32[]{:S(2)}, u32[]{:S(2)}) collective-permute-start(bf16[8,32,256]{2,1,0:T(8,128)(2,1)S(1)} %shard_map.200.b0), channel_id=1, source_target_pairs={{0,16},{4,20},{8,24},{12,28},{16,0},{20,4},{24,8},{28,12},{32,48},... | collective-permute-start | bytes 393224 | tf_op jit(solution)/shard_map/ppermute | solution.py:407
  90.7 9.1 %collective-permute-start.14 = (bf16[8,32,256]{2,1,0:T(8,128)(2,1)S(1)}, bf16[8,32,256]{2,1,0:T(8,128)(2,1)S(1)}, u32[]{:S(2)}, u32[]{:S(2)}) collective-permute-start(bf16[8,32,256]{2,1,0:T(8,128)(2,1)S(1)} %shard_map.200.b0), channel_id=1, source_target_pairs={{0,8},{4,12},{8,16},{12,20},{16,24},{20,28},{24,0},{28,4},{32,40},... | collective-permute-start | bytes 393224 | tf_op jit(solution)/shard_map/ppermute | solution.py:407
  91.2 11.7 %collective-permute-start.13 = (bf16[8,32,256]{2,1,0:T(8,128)(2,1)S(1)}, bf16[8,32,256]{2,1,0:T(8,128)(2,1)S(1)}, u32[]{:S(2)}, u32[]{:S(2)}) collective-permute-start(bf16[8,32,256]{2,1,0:T(8,128)(2,1)S(1)} %shard_map.200.b0), channel_id=1, source_target_pairs={{0,4},{4,0},{8,12},{12,8},{16,20},{20,16},{24,28},{28,24},{32,36},... | collective-permute-start | bytes 393224 | tf_op jit(solution)/shard_map/ppermute | solution.py:407
  95.5 7.4 %collective-permute-start.19 = (bf16[8,32,256]{2,1,0:T(8,128)(2,1)S(1)}, bf16[8,32,256]{2,1,0:T(8,128)(2,1)S(1)}, u32[]{:S(2)}, u32[]{:S(2)}) collective-permute-start(bf16[8,32,256]{2,1,0:T(8,128)(2,1)S(1)} %collective-permute-done.18.b6), channel_id=1, source_target_pairs={{0,4},{4,0},{8,12},{12,8},{16,20},{20,16},{24,28},{28,24},{32,36},... | collective-permute-start | bytes 393224 | tf_op jit(solution)/shard_map/ppermute | solution.py:407
  96.9 6.0 %collective-permute-start.17 = (bf16[8,32,256]{2,1,0:T(8,128)(2,1)S(1)}, bf16[8,32,256]{2,1,0:T(8,128)(2,1)S(1)}, u32[]{:S(2)}, u32[]{:S(2)}) collective-permute-start(bf16[8,32,256]{2,1,0:T(8,128)(2,1)S(1)} %collective-permute-done.16.b4), channel_id=1, source_target_pairs={{0,4},{4,0},{8,12},{12,8},{16,20},{20,16},{24,28},{28,24},{32,36},... | collective-permute-start | bytes 393224 | tf_op jit(solution)/shard_map/ppermute | solution.py:407
  99.8 3.1 %collective-permute-start.15 = (bf16[8,32,256]{2,1,0:T(8,128)(2,1)S(1)}, bf16[8,32,256]{2,1,0:T(8,128)(2,1)S(1)}, u32[]{:S(2)}, u32[]{:S(2)}) collective-permute-start(bf16[8,32,256]{2,1,0:T(8,128)(2,1)S(1)} %collective-permute-done.14.b2), channel_id=1, source_target_pairs={{0,4},{4,0},{8,12},{12,8},{16,20},{20,16},{24,28},{28,24},{32,36},... | collective-permute-start | bytes 393224 | tf_op jit(solution)/shard_map/ppermute | solution.py:407
  104.7 3.9 %collective-permute-start.20 = (bf16[16,512]{1,0:T(8,128)(2,1)S(1)}, bf16[16,512]{1,0:T(8,128)(2,1)S(1)}, u32[]{:S(2)}, u32[]{:S(2)}) collective-permute-start(bf16[16,512]{1,0:T(8,128)(2,1)S(1)} %get-tuple-element.50), channel_id=1, source_target_pairs={{0,1},{1,2},{2,3},{3,0},{4,5},{5,6},{6,7},{7,4},{8,9},{9,10},{10,1... | collective-permute-start | bytes 49160 | tf_op jit(solution)/shard_map/ppermute | solution.py:466
  104.8 4.2 %collective-permute-start.21 = (bf16[16,512]{1,0:T(8,128)(2,1)S(1)}, bf16[16,512]{1,0:T(8,128)(2,1)S(1)}, u32[]{:S(2)}, u32[]{:S(2)}) collective-permute-start(bf16[16,512]{1,0:T(8,128)(2,1)S(1)} %get-tuple-element.51), channel_id=1, source_target_pairs={{0,2},{1,3},{2,0},{3,1},{4,6},{5,7},{6,4},{7,5},{8,10},{9,11},{10,... | collective-permute-start | bytes 49160 | tf_op jit(solution)/shard_map/ppermute | solution.py:466
  (13 other events, 565.8 us)

commit v6 on v5

--- a/solution.py
+++ b/solution.py
@@ -8,7 +8,7 @@
 HEAD_DIM = 64
 EPS = 1e-06
 CAP = 3
-Z_ORDER = (0, -1, 1, -3, -4, -2, 3, 2)
+Z_ORDER = (0, -1, -2, -3, -4, -5, 2, 1)
 bf16 = jnp.bfloat16
 f32 = jnp.float32
 
@@ -235,10 +235,9 @@
         c.wait()
 
 
-def stack_kernel(near_ref, low_ref, high_ref, out_ref):
-    out_ref[0:3] = near_ref[...]
-    out_ref[3:6] = low_ref[...]
-    out_ref[6:8] = high_ref[0:2]
+def stack_kernel(r0, r1, r2, r3, out_ref):
+    for i, r in enumerate((r0, r1, r2, r3)):
+        out_ref[2 * i : 2 * i + 2] = r[...]
 
 
 def cut_kernel(part_ref, down_hbm, o0, o1, o2, o3, all_v, sems):
@@ -409,8 +408,9 @@
     partial, pick, joined = attend(
         tokens, lengths, cache, attn_gain, query_weight, stick_bias, out_weight, routes.T, shared_gate, shared_up
     )
-    others = [lax.ppermute(partial, "tp", around(k, ntp)) for k in (2, 1, 3)]
-    near = [joined, shift(joined, 1, 0, 0), shift(joined, -1, 0, 0)]
+    others = [lax.ppermute(partial, "tp", around(2, ntp))]
+    others += [lax.ppermute(partial, "tp", around(k, ntp)) for k in (1, 3)]
+    near = [joined, shift(joined, 1, 0, 0)]
     normed_mix, residual, sent = call(
         mix_kernel, [((rows, d), bf16), ((rows, quarter), f32), ((n_pick, CAP * d // 8), bf16)],
         (part, tokens, partial, *others, ffn_gain.reshape(1, -1), pick),
@@ -421,7 +421,7 @@
     arrived = lax.all_to_all(sent.reshape(nep, 8, -1), "ep", 0, 0, tiled=True)
     arrived = arrived.reshape(n_pick, -1)
     near = jnp.concatenate(after(near, sent))
-    low, high = shift(near, 3, 0, 0), shift(near, -3, 0, 0)
+    far = [shift(near, k, 0, 0) for k in (2, 4, -2)]
     f = expert_down.shape[1]
     cuts = call(
         cut_kernel, [((f, quarter), bf16)] * 4, (part, after(expert_down, sent)),
@@ -445,7 +445,7 @@
         scratch=[pltpu.VMEM((m, d), bf16), pltpu.SemaphoreType.DMA((4,))],
     )
     hiddens = [hidden] + [lax.ppermute(hidden, "tp", around(k, ntp)) for k in range(1, ntp)]
-    (column,) = call(stack_kernel, [((8, *joined.shape[1:]), bf16)], (after(near, hidden), low, high))
+    (column,) = call(stack_kernel, [((8, *joined.shape[1:]), bf16)], (after(near, hidden), *far))
     planes = [column] + [shift(column, 0, k, 0) for k in range(1, 4)]
     blocks = [column, shift(column, 0, 0, 1)]
     (back,) = call(
@@ -463,7 +463,8 @@
         in_specs=[SM, VM, VM, HBM] + [VM] * 9,
         scratch=[pltpu.VMEM((rows, d), f32), pltpu.VMEM((rows, quarter), f32), pltpu.SemaphoreType.DMA],
     )
-    shares = [shares[0]] + [lax.ppermute(shares[k], "tp", around(k, ntp)) for k in range(1, ntp)]
+    far_share = lax.ppermute(shares[2], "tp", around(2, ntp))
+    shares = [shares[0], far_share] + [lax.ppermute(shares[k], "tp", around(k, ntp)) for k in (1, 3)]
     (layer_out,) = call(
         final_kernel, [((rows, quarter), bf16)],
         (returned, mix, mix_gate, *shares),

time: 111 us -> 109 us (0.982)
  waiting for transfers between devices: 35.2 us -> 31.8 us
  starting transfers between devices: 55.8 us -> 57.8 us
    ppermute x11, waiting for transfers between devices: 20.1 us -> 7.81 us  [shift(): return lax.ppermute(value, 'ep', perm)]
    ppermute x3, waiting for transfers between devices: 0.01 us -> 11.8 us  [shards(): lax.ppermute(cuts[k], 'tp', around(k, ntp))]
    ppermute x3, waiting for transfers between devices: 6.92 us -> 3.27 us  [shards(): lax.ppermute(hidden, 'tp', around(k, ntp))]
    ppermute x11, starting transfers between devices: 19.6 us -> 21.7 us  [shift(): return lax.ppermute(value, 'ep', perm)]
    all_to_all x1, waiting for transfers between devices: 2.63 us -> 4.44 us  [shards(): arrived = lax.all_to_all(sent.reshape(nep, 8, -1), 'ep', 0, 0, tiled=True)]
    all_to_all x1, starting transfers between devices: 7.64 us -> 6.28 us  [shards(): returned = lax.all_to_all(back.reshape(nep, 8, -1), 'ep', 0, 0, tiled=True)]
    ppermute x3 -> x2, waiting for transfers between devices: 2.17 us -> 0.85 us  [shards(): lax.ppermute(shares[k], 'tp', around(k, ntp))]
    ppermute x3 -> x4, starting transfers between devices: 5.1 us -> 6.34 us  [the longest x2 3.38 us: shards(): others += [lax.ppermute(partial, 'tp', around(k, ntp)) for k in (1, 3)]]
  transfers between devices with their start and end apart: 25 -> 25, of which waited for: 14 -> 12; matrix products, arithmetic and copies ran while one was open for 0% -> 0% of each run, Pallas kernels for 6% -> 6%
where the time goes in v6:
time: 109 us; the launch traced here: 108 us
  starting transfers between devices  57.8 us (53%)
  waiting for transfers between devices  31.8 us (29%)
  Pallas kernels  17 us (16%)
    ppermute x11, starting transfers between devices, shift(): return lax.ppermute(value, 'ep', perm)  21.7 us
    pallas_call x9, Pallas kernels, call(): pl.pallas_call(kernel, out_shape=tuple(shapes), in_specs=in_specs, out_sp...  17 us
    all_to_all x1, starting transfers between devices, shards(): arrived = lax.all_to_all(sent.reshape(nep, 8, -1), 'ep', 0, 0, tiled=True)  13.8 us
    ppermute x3, waiting for transfers between devices, shards(): lax.ppermute(cuts[k], 'tp', around(k, ntp))  11.8 us
    ppermute x11, waiting for transfers between devices, shift(): return lax.ppermute(value, 'ep', perm)  7.81 us
    all_to_all x1, starting transfers between devices, shards(): returned = lax.all_to_all(back.reshape(nep, 8, -1), 'ep', 0, 0, tiled=True)  6.28 us
    all_to_all x1, waiting for transfers between devices, shards(): arrived = lax.all_to_all(sent.reshape(nep, 8, -1), 'ep', 0, 0, tiled=True)  4.44 us
    ppermute x3, starting transfers between devices, shards(): lax.ppermute(cuts[k], 'tp', around(k, ntp))  3.73 us
  transfers between devices with their start and end apart: 25, of which 12 were waited for; matrix products, arithmetic and copies ran while one was open for 0% of the time, Pallas kernels for 6%

profile of v6, /device:TPU:1, one launch (start us, length us, event | category | flops | bytes accessed | tf_op | source)
XLA Modules:
  0.0 108.4 jit_solution(6745169321405153243)
XLA Ops:
  0.7 5.9 %shard_map.194 = (bf16[16,2048]{1,0:T(8,128)(2,1)S(1)}, bf16[512,384]{1,0:T(8,128)(2,1)S(1)}, bf16[1,32,256]{2,1,0:T(8,128)(2,1)S(1)}) custom-call(s32[16]{0:T(128)} %len_hbm.1, f32[4]{0:T(128)} %bias_hbm.1, bf16[16,2048]{1,0:T(8,128)(2,1)} %tok_hbm.2, f32[1,2048]{1,0:T(1,128)} %bitcast.15, bf16[16,1024,128]{2,1,0:T(8,128)(2,1)} %cache_hbm.1, ...), custom_call_target="tpu_custom_call" | custom-call | tf_op jit(solution)/shard_map/pallas_call | solution.py:47
  6.6 3.4 %collective-permute-start.2 = (bf16[16,2048]{1,0:T(8,128)(2,1)S(1)}, bf16[16,2048]{1,0:T(8,128)(2,1)S(1)}, u32[]{:S(2)}, u32[]{:S(2)}) collective-permute-start(bf16[16,2048]{1,0:T(8,128)(2,1)S(1)} %get-tuple-element.27.p0), channel_id=1, source_target_pairs={{0,3},{1,0},{2,1},{3,2},{4,7},{5,4},{6,5},{7,6},{8,11},{9,8},{10,9... | collective-permute-start | bytes 196616 | tf_op jit(solution)/shard_map/ppermute | solution.py:412
  11.7 3.2 %collective-permute-done.1.p2 = bf16[16,2048]{1,0:T(8,128)(2,1)S(1)} collective-permute-done((bf16[16,2048]{1,0:T(8,128)(2,1)S(1)}, bf16[16,2048]{1,0:T(8,128)(2,1)S(1)}, u32[]{:S(2)}, u32[]{:S(2)}) %collective-permute-start.1) | collective-permute-done | bytes 65568 | tf_op jit(solution)/shard_map/ppermute | solution.py:412
  16.6 13.8 %all-to-all-start = ((bf16[64,8,768]{2,1,0:T(8,128)(2,1)}), bf16[64,8,768]{2,1,0:T(8,128)(2,1)S(1)}, u32[]{:S(2)}, u32[]{:S(2)}) async-start(bf16[64,8,768]{2,1,0:T(8,128)(2,1)} %bitcast.23), calls=%async_computation | async-start | bytes 1572864 | tf_op jit(solution)/shard_map/all_to_all | solution.py:421
  30.4 2.3 %shard_map.196 = (bf16[256,512]{1,0:T(8,128)(2,1)}, bf16[256,512]{1,0:T(8,128)(2,1)}, bf16[256,512]{1,0:T(8,128)(2,1)}, bf16[256,512]{1,0:T(8,128)(2,1)}) custom-call(s32[1]{0:T(128)} %bitcast.part_ref, bf16[1,256,2048]{2,1,0:T(8,128)(2,1)} %down_hbm), custom_call_target="tpu_custom_call" | custom-call | tf_op jit(solution)/shard_map/pallas_call | solution.py:47
  32.9 3.6 %collective-permute-start.4 = (bf16[256,512]{1,0:T(8,128)(2,1)}, bf16[256,512]{1,0:T(8,128)(2,1)S(1)}, u32[]{:S(2)}, u32[]{:S(2)}) collective-permute-start(bf16[256,512]{1,0:T(8,128)(2,1)} %get-tuple-element.33), channel_id=1, source_target_pairs={{0,2},{1,3},{2,0},{3,1},{4,6},{5,7},{6,4},{7,5},{8,10},{9,11},{10,... | collective-permute-start | bytes 786440 | tf_op jit(solution)/shard_map/ppermute | solution.py:431
  36.5 5.2 %collective-permute-done.3.d1 = bf16[256,512]{1,0:T(8,128)(2,1)S(1)} collective-permute-done((bf16[256,512]{1,0:T(8,128)(2,1)}, bf16[256,512]{1,0:T(8,128)(2,1)S(1)}, u32[]{:S(2)}, u32[]{:S(2)}) %collective-permute-start.3) | collective-permute-done | bytes 262176 | tf_op jit(solution)/shard_map/ppermute | solution.py:431
  41.7 6.6 %collective-permute-done.4.d2 = bf16[256,512]{1,0:T(8,128)(2,1)S(1)} collective-permute-done((bf16[256,512]{1,0:T(8,128)(2,1)}, bf16[256,512]{1,0:T(8,128)(2,1)S(1)}, u32[]{:S(2)}, u32[]{:S(2)}) %collective-permute-start.4) | collective-permute-done | bytes 262176 | tf_op jit(solution)/shard_map/ppermute | solution.py:431
  49.0 4.4 %all-to-all-done = bf16[64,8,768]{2,1,0:T(8,128)(2,1)S(1)} async-done(((bf16[64,8,768]{2,1,0:T(8,128)(2,1)}), bf16[64,8,768]{2,1,0:T(8,128)(2,1)S(1)}, u32[]{:S(2)}, u32[]{:S(2)}) %all-to-all-start) | async-done | bytes 786464 | tf_op jit(solution)/shard_map/all_to_all | solution.py:421
  54.7 2.6 %collective-permute-start.8 = (bf16[192,256]{1,0:T(8,128)(2,1)S(1)}, bf16[192,256]{1,0:T(8,128)(2,1)S(1)}, u32[]{:S(2)}, u32[]{:S(2)}) collective-permute-start(bf16[192,256]{1,0:T(8,128)(2,1)S(1)} %get-tuple-element.35.h0), channel_id=1, source_target_pairs={{0,3},{1,0},{2,1},{3,2},{4,7},{5,4},{6,5},{7,6},{8,11},{9,8},{10,9... | collective-permute-start | bytes 294920 | tf_op jit(solution)/shard_map/ppermute | solution.py:447
  58.8 2.9 %collective-permute-done.9 = bf16[1,32,256]{2,1,0:T(8,128)(2,1)S(1)} collective-permute-done((bf16[1,32,256]{2,1,0:T(8,128)(2,1)S(1)}, bf16[1,32,256]{2,1,0:T(8,128)(2,1)S(1)}, u32[]{:S(2)}, u32[]{:S(2)}) %collective-permute-start.9) | collective-permute-done | bytes 16416 | tf_op jit(solution)/shard_map/ppermute | solution.py:406
  62.3 2.7 %collective-permute-done.6.h1 = bf16[192,256]{1,0:T(8,128)(2,1)S(1)} collective-permute-done((bf16[192,256]{1,0:T(8,128)(2,1)S(1)}, bf16[192,256]{1,0:T(8,128)(2,1)S(1)}, u32[]{:S(2)}, u32[]{:S(2)}) %collective-permute-start.6) | collective-permute-done | bytes 98336 | tf_op jit(solution)/shard_map/ppermute | solution.py:447
  66.4 6.3 %all-to-all-start.1 = ((bf16[64,8,256]{2,1,0:T(8,128)(2,1)}), bf16[64,8,256]{2,1,0:T(8,128)(2,1)S(1)}, u32[]{:S(2)}, u32[]{:S(2)}) async-start(bf16[64,8,256]{2,1,0:T(8,128)(2,1)} %bitcast.22), calls=%async_computation.1 | async-start | bytes 524288 | tf_op jit(solution)/shard_map/all_to_all | solution.py:455
  72.7 3.8 %collective-permute-start.12 = (bf16[2,32,256]{2,1,0:T(8,128)(2,1)S(1)}, bf16[2,32,256]{2,1,0:T(8,128)(2,1)S(1)}, u32[]{:S(2)}, u32[]{:S(2)}) collective-permute-start(bf16[2,32,256]{2,1,0:T(8,128)(2,1)S(1)} %constant_dynamic-update-slice_fusion.r0), channel_id=1, source_target_pairs={{0,192},{4,196},{8,200},{12,204},{16,208},{20,212},{24,216},{28,22... | collective-permute-start | bytes 98312 | tf_op jit(solution)/shard_map/ppermute | solution.py:406
  76.4 1.9 %collective-permute-start.11 = (bf16[2,32,256]{2,1,0:T(8,128)(2,1)S(1)}, bf16[2,32,256]{2,1,0:T(8,128)(2,1)S(1)}, u32[]{:S(2)}, u32[]{:S(2)}) collective-permute-start(bf16[2,32,256]{2,1,0:T(8,128)(2,1)S(1)} %constant_dynamic-update-slice_fusion.r0), channel_id=1, source_target_pairs={{0,128},{4,132},{8,136},{12,140},{16,144},{20,148},{24,152},{28,15... | collective-permute-start | bytes 98312 | tf_op jit(solution)/shard_map/ppermute | solution.py:406
  78.3 2.2 %collective-permute-start.10 = (bf16[2,32,256]{2,1,0:T(8,128)(2,1)S(1)}, bf16[2,32,256]{2,1,0:T(8,128)(2,1)S(1)}, u32[]{:S(2)}, u32[]{:S(2)}) collective-permute-start(bf16[2,32,256]{2,1,0:T(8,128)(2,1)S(1)} %constant_dynamic-update-slice_fusion.r0), channel_id=1, source_target_pairs={{0,64},{4,68},{8,72},{12,76},{16,80},{20,84},{24,88},{28,92},{32,9... | collective-permute-start | bytes 98312 | tf_op jit(solution)/shard_map/ppermute | solution.py:406
  81.6 3.7 %collective-permute-done.11.r2 = bf16[2,32,256]{2,1,0:T(8,128)(2,1)S(1)} collective-permute-done((bf16[2,32,256]{2,1,0:T(8,128)(2,1)S(1)}, bf16[2,32,256]{2,1,0:T(8,128)(2,1)S(1)}, u32[]{:S(2)}, u32[]{:S(2)}) %collective-permute-start.11) | collective-permute-done | bytes 32800 | tf_op jit(solution)/shard_map/ppermute | solution.py:406
  85.4 2.9 %collective-permute-start.18 = (bf16[8,32,256]{2,1,0:T(8,128)(2,1)S(1)}, bf16[8,32,256]{2,1,0:T(8,128)(2,1)S(1)}, u32[]{:S(2)}, u32[]{:S(2)}) collective-permute-start(bf16[8,32,256]{2,1,0:T(8,128)(2,1)S(1)} %shard_map.200.b0), channel_id=1, source_target_pairs={{0,24},{4,28},{8,0},{12,4},{16,8},{20,12},{24,16},{28,20},{32,56},... | collective-permute-start | bytes 393224 | tf_op jit(solution)/shard_map/ppermute | solution.py:406
  89.1 2.3 %collective-permute-start.13 = (bf16[8,32,256]{2,1,0:T(8,128)(2,1)S(1)}, bf16[8,32,256]{2,1,0:T(8,128)(2,1)S(1)}, u32[]{:S(2)}, u32[]{:S(2)}) collective-permute-start(bf16[8,32,256]{2,1,0:T(8,128)(2,1)S(1)} %shard_map.200.b0), channel_id=1, source_target_pairs={{0,4},{4,0},{8,12},{12,8},{16,20},{20,16},{24,28},{28,24},{32,36},... | collective-permute-start | bytes 393224 | tf_op jit(solution)/shard_map/ppermute | solution.py:406
  91.5 3.4 %collective-permute-start.19 = (bf16[8,32,256]{2,1,0:T(8,128)(2,1)S(1)}, bf16[8,32,256]{2,1,0:T(8,128)(2,1)S(1)}, u32[]{:S(2)}, u32[]{:S(2)}) collective-permute-start(bf16[8,32,256]{2,1,0:T(8,128)(2,1)S(1)} %collective-permute-done.18.b6), channel_id=1, source_target_pairs={{0,4},{4,0},{8,12},{12,8},{16,20},{20,16},{24,28},{28,24},{32,36},... | collective-permute-start | bytes 393224 | tf_op jit(solution)/shard_map/ppermute | solution.py:406
  94.9 2.3 %collective-permute-start.17 = (bf16[8,32,256]{2,1,0:T(8,128)(2,1)S(1)}, bf16[8,32,256]{2,1,0:T(8,128)(2,1)S(1)}, u32[]{:S(2)}, u32[]{:S(2)}) collective-permute-start(bf16[8,32,256]{2,1,0:T(8,128)(2,1)S(1)} %collective-permute-done.16.b4), channel_id=1, source_target_pairs={{0,4},{4,0},{8,12},{12,8},{16,20},{20,16},{24,28},{28,24},{32,36},... | collective-permute-start | bytes 393224 | tf_op jit(solution)/shard_map/ppermute | solution.py:406
  98.5 2.2 %shard_map.199 = (bf16[96,512]{1,0:T(8,128)(2,1)S(1)}, bf16[16,128]{1,0:T(8,128)(2,1)}, f32[16,128]{1,0:T(8,128)S(1)}) custom-call(s32[6,16]{1,0:T(8,128)S(1)} %bitcast.18, f32[6,16]{1,0:T(8,128)S(1)} %bitcast.20, bf16[16,2048]{1,0:T(8,128)(2,1)} %tok_hbm.2, f32[1,2048]{1,0:T(1,128)S(1)} %bitcast.16, bf16[64,2048]{1,0:T(8,128)(2,1)} %bitcast.24, ...), custom_call_target="tpu_custom_call" | custom-call | tf_op jit(solution)/shard_map/pallas_call | solution.py:47
  100.8 1.7 %shard_map.201 = (f32[16,512]{1,0:T(8,128)S(1)}, bf16[16,512]{1,0:T(8,128)(2,1)S(1)}, bf16[16,512]{1,0:T(8,128)(2,1)S(1)}, bf16[16,512]{1,0:T(8,128)(2,1)S(1)}) custom-call(s32[2]{0:T(128)S(1)} %pad_add_fusion.at_ref, bf16[16,2048]{1,0:T(8,128)(2,1)S(1)} %copy-done.4, bf16[128,2048]{1,0:T(8,128)(2,1)S(1)} %copy-done.3, ...), custom_call_target="tpu_custom_call" | custom-call | tf_op jit(solution)/shard_map/pallas_call | solution.py:47
  103.7 2.7 %collective-permute-start.22 = (bf16[16,512]{1,0:T(8,128)(2,1)S(1)}, bf16[16,512]{1,0:T(8,128)(2,1)S(1)}, u32[]{:S(2)}, u32[]{:S(2)}) collective-permute-start(bf16[16,512]{1,0:T(8,128)(2,1)S(1)} %get-tuple-element.50), channel_id=1, source_target_pairs={{0,3},{1,0},{2,1},{3,2},{4,7},{5,4},{6,5},{7,6},{8,11},{9,8},{10,9... | collective-permute-start | bytes 49160 | tf_op jit(solution)/shard_map/ppermute | solution.py:467
  (62 shorter events, 15.4 us)
Async XLA Ops:
  6.6 5.1 %collective-permute-start.2 = (bf16[16,2048]{1,0:T(8,128)(2,1)S(1)}, bf16[16,2048]{1,0:T(8,128)(2,1)S(1)}, u32[]{:S(2)}, u32[]{:S(2)}) collective-permute-start(bf16[16,2048]{1,0:T(8,128)(2,1)S(1)} %get-tuple-element.27.p0), channel_id=1, source_target_pairs={{0,3},{1,0},{2,1},{3,2},{4,7},{5,4},{6,5},{7,6},{8,11},{9,8},{10,9... | collective-permute-start | bytes 196616 | tf_op jit(solution)/shard_map/ppermute | solution.py:412
  10.0 4.9 %collective-permute-start.1 = (bf16[16,2048]{1,0:T(8,128)(2,1)S(1)}, bf16[16,2048]{1,0:T(8,128)(2,1)S(1)}, u32[]{:S(2)}, u32[]{:S(2)}) collective-permute-start(bf16[16,2048]{1,0:T(8,128)(2,1)S(1)} %get-tuple-element.27.p0), channel_id=1, source_target_pairs={{0,1},{1,2},{2,3},{3,0},{4,5},{5,6},{6,7},{7,4},{8,9},{9,10},{10,1... | collective-permute-start | bytes 196616 | tf_op jit(solution)/shard_map/ppermute | solution.py:412
  10.0 5.1 %collective-permute-start = (bf16[16,2048]{1,0:T(8,128)(2,1)S(1)}, bf16[16,2048]{1,0:T(8,128)(2,1)S(1)}, u32[]{:S(2)}, u32[]{:S(2)}) collective-permute-start(bf16[16,2048]{1,0:T(8,128)(2,1)S(1)} %get-tuple-element.27.p0), channel_id=1, source_target_pairs={{0,2},{1,3},{2,0},{3,1},{4,6},{5,7},{6,4},{7,5},{8,10},{9,11},{10,... | collective-permute-start | bytes 196616 | tf_op jit(solution)/shard_map/ppermute | solution.py:411
  16.6 36.9 %all-to-all-start = ((bf16[64,8,768]{2,1,0:T(8,128)(2,1)}), bf16[64,8,768]{2,1,0:T(8,128)(2,1)S(1)}, u32[]{:S(2)}, u32[]{:S(2)}) async-start(bf16[64,8,768]{2,1,0:T(8,128)(2,1)} %bitcast.23), calls=%async_computation | async-start | bytes 1572864 | tf_op jit(solution)/shard_map/all_to_all | solution.py:421
  32.8 8.9 %collective-permute-start.3 = (bf16[256,512]{1,0:T(8,128)(2,1)}, bf16[256,512]{1,0:T(8,128)(2,1)S(1)}, u32[]{:S(2)}, u32[]{:S(2)}) collective-permute-start(bf16[256,512]{1,0:T(8,128)(2,1)} %get-tuple-element.32), channel_id=1, source_target_pairs={{0,1},{1,2},{2,3},{3,0},{4,5},{5,6},{6,7},{7,4},{8,9},{9,10},{10,1... | collective-permute-start | bytes 786440 | tf_op jit(solution)/shard_map/ppermute | solution.py:431
  32.9 15.4 %collective-permute-start.4 = (bf16[256,512]{1,0:T(8,128)(2,1)}, bf16[256,512]{1,0:T(8,128)(2,1)S(1)}, u32[]{:S(2)}, u32[]{:S(2)}) collective-permute-start(bf16[256,512]{1,0:T(8,128)(2,1)} %get-tuple-element.33), channel_id=1, source_target_pairs={{0,2},{1,3},{2,0},{3,1},{4,6},{5,7},{6,4},{7,5},{8,10},{9,11},{10,... | collective-permute-start | bytes 786440 | tf_op jit(solution)/shard_map/ppermute | solution.py:431
  36.5 12.5 %collective-permute-start.5 = (bf16[256,512]{1,0:T(8,128)(2,1)}, bf16[256,512]{1,0:T(8,128)(2,1)}, u32[]{:S(2)}, u32[]{:S(2)}) collective-permute-start(bf16[256,512]{1,0:T(8,128)(2,1)} %get-tuple-element.34), channel_id=1, source_target_pairs={{0,3},{1,0},{2,1},{3,2},{4,7},{5,4},{6,5},{7,6},{8,11},{9,8},{10,9... | collective-permute-start | bytes 786440 | tf_op jit(solution)/shard_map/ppermute | solution.py:431
  54.7 7.0 %collective-permute-start.8 = (bf16[192,256]{1,0:T(8,128)(2,1)S(1)}, bf16[192,256]{1,0:T(8,128)(2,1)S(1)}, u32[]{:S(2)}, u32[]{:S(2)}) collective-permute-start(bf16[192,256]{1,0:T(8,128)(2,1)S(1)} %get-tuple-element.35.h0), channel_id=1, source_target_pairs={{0,3},{1,0},{2,1},{3,2},{4,7},{5,4},{6,5},{7,6},{8,11},{9,8},{10,9... | collective-permute-start | bytes 294920 | tf_op jit(solution)/shard_map/ppermute | solution.py:447
  57.2 5.1 %collective-permute-start.7 = (bf16[192,256]{1,0:T(8,128)(2,1)S(1)}, bf16[192,256]{1,0:T(8,128)(2,1)S(1)}, u32[]{:S(2)}, u32[]{:S(2)}) collective-permute-start(bf16[192,256]{1,0:T(8,128)(2,1)S(1)} %get-tuple-element.35.h0), channel_id=1, source_target_pairs={{0,2},{1,3},{2,0},{3,1},{4,6},{5,7},{6,4},{7,5},{8,10},{9,11},{10,... | collective-permute-start | bytes 294920 | tf_op jit(solution)/shard_map/ppermute | solution.py:447
  57.2 7.7 %collective-permute-start.6 = (bf16[192,256]{1,0:T(8,128)(2,1)S(1)}, bf16[192,256]{1,0:T(8,128)(2,1)S(1)}, u32[]{:S(2)}, u32[]{:S(2)}) collective-permute-start(bf16[192,256]{1,0:T(8,128)(2,1)S(1)} %get-tuple-element.35.h0), channel_id=1, source_target_pairs={{0,1},{1,2},{2,3},{3,0},{4,5},{5,6},{6,7},{7,4},{8,9},{9,10},{10,1... | collective-permute-start | bytes 294920 | tf_op jit(solution)/shard_map/ppermute | solution.py:447
  57.9 3.8 %collective-permute-start.9 = (bf16[1,32,256]{2,1,0:T(8,128)(2,1)S(1)}, bf16[1,32,256]{2,1,0:T(8,128)(2,1)S(1)}, u32[]{:S(2)}, u32[]{:S(2)}) collective-permute-start(bf16[1,32,256]{2,1,0:T(8,128)(2,1)S(1)} %get-tuple-element.44), channel_id=1, source_target_pairs={{0,32},{4,36},{8,40},{12,44},{16,48},{20,52},{24,56},{28,60},{32,6... | collective-permute-start | bytes 49160 | tf_op jit(solution)/shard_map/ppermute | solution.py:406
  66.4 41.2 %all-to-all-start.1 = ((bf16[64,8,256]{2,1,0:T(8,128)(2,1)}), bf16[64,8,256]{2,1,0:T(8,128)(2,1)S(1)}, u32[]{:S(2)}, u32[]{:S(2)}) async-start(bf16[64,8,256]{2,1,0:T(8,128)(2,1)} %bitcast.22), calls=%async_computation.1 | async-start | bytes 524288 | tf_op jit(solution)/shard_map/all_to_all | solution.py:455
  72.7 8.9 %collective-permute-start.12 = (bf16[2,32,256]{2,1,0:T(8,128)(2,1)S(1)}, bf16[2,32,256]{2,1,0:T(8,128)(2,1)S(1)}, u32[]{:S(2)}, u32[]{:S(2)}) collective-permute-start(bf16[2,32,256]{2,1,0:T(8,128)(2,1)S(1)} %constant_dynamic-update-slice_fusion.r0), channel_id=1, source_target_pairs={{0,192},{4,196},{8,200},{12,204},{16,208},{20,212},{24,216},{28,22... | collective-permute-start | bytes 98312 | tf_op jit(solution)/shard_map/ppermute | solution.py:406
  76.4 8.9 %collective-permute-start.11 = (bf16[2,32,256]{2,1,0:T(8,128)(2,1)S(1)}, bf16[2,32,256]{2,1,0:T(8,128)(2,1)S(1)}, u32[]{:S(2)}, u32[]{:S(2)}) collective-permute-start(bf16[2,32,256]{2,1,0:T(8,128)(2,1)S(1)} %constant_dynamic-update-slice_fusion.r0), channel_id=1, source_target_pairs={{0,128},{4,132},{8,136},{12,140},{16,144},{20,148},{24,152},{28,15... | collective-permute-start | bytes 98312 | tf_op jit(solution)/shard_map/ppermute | solution.py:406
  78.3 7.0 %collective-permute-start.10 = (bf16[2,32,256]{2,1,0:T(8,128)(2,1)S(1)}, bf16[2,32,256]{2,1,0:T(8,128)(2,1)S(1)}, u32[]{:S(2)}, u32[]{:S(2)}) collective-permute-start(bf16[2,32,256]{2,1,0:T(8,128)(2,1)S(1)} %constant_dynamic-update-slice_fusion.r0), channel_id=1, source_target_pairs={{0,64},{4,68},{8,72},{12,76},{16,80},{20,84},{24,88},{28,92},{32,9... | collective-permute-start | bytes 98312 | tf_op jit(solution)/shard_map/ppermute | solution.py:406
  85.4 6.1 %collective-permute-start.18 = (bf16[8,32,256]{2,1,0:T(8,128)(2,1)S(1)}, bf16[8,32,256]{2,1,0:T(8,128)(2,1)S(1)}, u32[]{:S(2)}, u32[]{:S(2)}) collective-permute-start(bf16[8,32,256]{2,1,0:T(8,128)(2,1)S(1)} %shard_map.200.b0), channel_id=1, source_target_pairs={{0,24},{4,28},{8,0},{12,4},{16,8},{20,12},{24,16},{28,20},{32,56},... | collective-permute-start | bytes 393224 | tf_op jit(solution)/shard_map/ppermute | solution.py:406
  88.3 6.6 %collective-permute-start.16 = (bf16[8,32,256]{2,1,0:T(8,128)(2,1)S(1)}, bf16[8,32,256]{2,1,0:T(8,128)(2,1)S(1)}, u32[]{:S(2)}, u32[]{:S(2)}) collective-permute-start(bf16[8,32,256]{2,1,0:T(8,128)(2,1)S(1)} %shard_map.200.b0), channel_id=1, source_target_pairs={{0,16},{4,20},{8,24},{12,28},{16,0},{20,4},{24,8},{28,12},{32,48},... | collective-permute-start | bytes 393224 | tf_op jit(solution)/shard_map/ppermute | solution.py:406
  88.5 8.7 %collective-permute-start.14 = (bf16[8,32,256]{2,1,0:T(8,128)(2,1)S(1)}, bf16[8,32,256]{2,1,0:T(8,128)(2,1)S(1)}, u32[]{:S(2)}, u32[]{:S(2)}) collective-permute-start(bf16[8,32,256]{2,1,0:T(8,128)(2,1)S(1)} %shard_map.200.b0), channel_id=1, source_target_pairs={{0,8},{4,12},{8,16},{12,20},{16,24},{20,28},{24,0},{28,4},{32,40},... | collective-permute-start | bytes 393224 | tf_op jit(solution)/shard_map/ppermute | solution.py:406
  89.1 11.6 %collective-permute-start.13 = (bf16[8,32,256]{2,1,0:T(8,128)(2,1)S(1)}, bf16[8,32,256]{2,1,0:T(8,128)(2,1)S(1)}, u32[]{:S(2)}, u32[]{:S(2)}) collective-permute-start(bf16[8,32,256]{2,1,0:T(8,128)(2,1)S(1)} %shard_map.200.b0), channel_id=1, source_target_pairs={{0,4},{4,0},{8,12},{12,8},{16,20},{20,16},{24,28},{28,24},{32,36},... | collective-permute-start | bytes 393224 | tf_op jit(solution)/shard_map/ppermute | solution.py:406
  91.5 9.3 %collective-permute-start.19 = (bf16[8,32,256]{2,1,0:T(8,128)(2,1)S(1)}, bf16[8,32,256]{2,1,0:T(8,128)(2,1)S(1)}, u32[]{:S(2)}, u32[]{:S(2)}) collective-permute-start(bf16[8,32,256]{2,1,0:T(8,128)(2,1)S(1)} %collective-permute-done.18.b6), channel_id=1, source_target_pairs={{0,4},{4,0},{8,12},{12,8},{16,20},{20,16},{24,28},{28,24},{32,36},... | collective-permute-start | bytes 393224 | tf_op jit(solution)/shard_map/ppermute | solution.py:406
  94.9 5.8 %collective-permute-start.17 = (bf16[8,32,256]{2,1,0:T(8,128)(2,1)S(1)}, bf16[8,32,256]{2,1,0:T(8,128)(2,1)S(1)}, u32[]{:S(2)}, u32[]{:S(2)}) collective-permute-start(bf16[8,32,256]{2,1,0:T(8,128)(2,1)S(1)} %collective-permute-done.16.b4), channel_id=1, source_target_pairs={{0,4},{4,0},{8,12},{12,8},{16,20},{20,16},{24,28},{28,24},{32,36},... | collective-permute-start | bytes 393224 | tf_op jit(solution)/shard_map/ppermute | solution.py:406
  102.5 4.2 %collective-permute-start.20 = (bf16[16,512]{1,0:T(8,128)(2,1)S(1)}, bf16[16,512]{1,0:T(8,128)(2,1)S(1)}, u32[]{:S(2)}, u32[]{:S(2)}) collective-permute-start(bf16[16,512]{1,0:T(8,128)(2,1)S(1)} %get-tuple-element.48), channel_id=1, source_target_pairs={{0,2},{1,3},{2,0},{3,1},{4,6},{5,7},{6,4},{7,5},{8,10},{9,11},{10,... | collective-permute-start | bytes 49160 | tf_op jit(solution)/shard_map/ppermute | solution.py:466
  103.7 3.8 %collective-permute-start.21 = (bf16[16,512]{1,0:T(8,128)(2,1)S(1)}, bf16[16,512]{1,0:T(8,128)(2,1)S(1)}, u32[]{:S(2)}, u32[]{:S(2)}) collective-permute-start(bf16[16,512]{1,0:T(8,128)(2,1)S(1)} %get-tuple-element.49), channel_id=1, source_target_pairs={{0,1},{1,2},{2,3},{3,0},{4,5},{5,6},{6,7},{7,4},{8,9},{9,10},{10,1... | collective-permute-start | bytes 49160 | tf_op jit(solution)/shard_map/ppermute | solution.py:467
  103.7 3.8 %collective-permute-start.22 = (bf16[16,512]{1,0:T(8,128)(2,1)S(1)}, bf16[16,512]{1,0:T(8,128)(2,1)S(1)}, u32[]{:S(2)}, u32[]{:S(2)}) collective-permute-start(bf16[16,512]{1,0:T(8,128)(2,1)S(1)} %get-tuple-element.50), channel_id=1, source_target_pairs={{0,3},{1,0},{2,1},{3,2},{4,7},{5,4},{6,5},{7,6},{8,11},{9,8},{10,9... | collective-permute-start | bytes 49160 | tf_op jit(solution)/shard_map/ppermute | solution.py:467
  (13 other events, 613.9 us)

commit v7 on v6

--- a/solution.py
+++ b/solution.py
@@ -337,12 +337,13 @@
         c.wait()
 
 
-def side_kernel(routes_ref, rw_ref, tok_hbm, gain_ref, kw_hbm, vw_hbm, mixed_hbm, gv_ref,
-                mix_ref, kv_ref, gate_ref, tok_ref, both_ref, mixed_ref, sems):
+def side_kernel(routes_hbm, rw_hbm, tok_hbm, gain_hbm, kw_hbm, vw_hbm, mixed_hbm, gv_hbm,
+                mix_ref, kv_ref, gate_ref, tok_ref, both_ref, mixed_ref, routes_ref, rw_ref, gain_ref, gv_ref, sems):
     rows = tok_ref.shape[0]
     n = kw_hbm.shape[0]
     copies = copy_all([(tok_hbm, tok_ref), (kw_hbm, both_ref.at[:n, :]), (vw_hbm, both_ref.at[n:, :]),
-                       (mixed_hbm, mixed_ref)], sems)
+                       (mixed_hbm, mixed_ref), (routes_hbm, routes_ref), (rw_hbm, rw_ref), (gain_hbm, gain_ref),
+                       (gv_hbm, gv_ref)], sems)
     for c in copies:
         c.wait()
     x = tok_ref[...].astype(f32)
@@ -434,9 +435,10 @@
         [((6 * rows, n_pick), bf16), ((rows, 2 * HEAD_DIM), bf16), ((rows, 128), f32)],
         (routes.T, route_weights.T, after(tokens, sent), attn_gain.reshape(1, -1), key_weight.T, value_weight.T,
          normed_mix, gate_vector.reshape(-1, 128)),
-        in_specs=[VM, VM, HBM, VM, HBM, HBM, HBM, VM],
+        in_specs=[HBM] * 8,
         scratch=[pltpu.VMEM((rows, d), bf16), pltpu.VMEM((2 * HEAD_DIM, d), bf16), pltpu.VMEM((rows, d), bf16),
-                 pltpu.SemaphoreType.DMA((4,))],
+                 pltpu.VMEM(routes.T.shape, jnp.int32), pltpu.VMEM(routes.T.shape, f32), pltpu.VMEM((1, d), f32),
+                 pltpu.VMEM((d // 128, 128), bf16), pltpu.SemaphoreType.DMA((8,))],
     )
     m = CAP * nep
     hidden, downs = call(

time: 109 us -> 109 us (level)
  no operation moved by 1% of the time
where the time goes in v7:
time: 109 us; the launch traced here: 108 us
  starting transfers between devices  57.7 us (53%)
  waiting for transfers between devices  31.8 us (29%)
  Pallas kernels  17 us (16%)
    ppermute x11, starting transfers between devices, shift(): return lax.ppermute(value, 'ep', perm)  21.7 us
    pallas_call x9, Pallas kernels, call(): pl.pallas_call(kernel, out_shape=tuple(shapes), in_specs=in_specs, out_sp...  17 us
    all_to_all x1, starting transfers between devices, shards(): arrived = lax.all_to_all(sent.reshape(nep, 8, -1), 'ep', 0, 0, tiled=True)  13.7 us
    ppermute x3, waiting for transfers between devices, shards(): lax.ppermute(cuts[k], 'tp', around(k, ntp))  11.8 us
    ppermute x11, waiting for transfers between devices, shift(): return lax.ppermute(value, 'ep', perm)  7.81 us
    all_to_all x1, starting transfers between devices, shards(): returned = lax.all_to_all(back.reshape(nep, 8, -1), 'ep', 0, 0, tiled=True)  6.28 us
    all_to_all x1, waiting for transfers between devices, shards(): arrived = lax.all_to_all(sent.reshape(nep, 8, -1), 'ep', 0, 0, tiled=True)  4.44 us
    ppermute x3, starting transfers between devices, shards(): lax.ppermute(cuts[k], 'tp', around(k, ntp))  3.73 us
  transfers between devices with their start and end apart: 25, of which 12 were waited for; matrix products, arithmetic and copies ran while one was open for 0% of the time, Pallas kernels for 6%

profile of v7, /device:TPU:1, one launch (start us, length us, event | category | flops | bytes accessed | tf_op | source)
XLA Modules:
  0.0 108.2 jit_solution(6972079724297677254)
XLA Ops:
  0.7 5.9 %shard_map.194 = (bf16[16,2048]{1,0:T(8,128)(2,1)S(1)}, bf16[512,384]{1,0:T(8,128)(2,1)S(1)}, bf16[1,32,256]{2,1,0:T(8,128)(2,1)S(1)}) custom-call(s32[16]{0:T(128)} %len_hbm.1, f32[4]{0:T(128)} %bias_hbm.1, bf16[16,2048]{1,0:T(8,128)(2,1)} %tok_hbm.2, f32[1,2048]{1,0:T(1,128)} %bitcast.20, bf16[16,1024,128]{2,1,0:T(8,128)(2,1)} %cache_hbm.1, ...), custom_call_target="tpu_custom_call" | custom-call | tf_op jit(solution)/shard_map/pallas_call | solution.py:47
  6.6 3.4 %collective-permute-start.2 = (bf16[16,2048]{1,0:T(8,128)(2,1)S(1)}, bf16[16,2048]{1,0:T(8,128)(2,1)S(1)}, u32[]{:S(2)}, u32[]{:S(2)}) collective-permute-start(bf16[16,2048]{1,0:T(8,128)(2,1)S(1)} %get-tuple-element.27.p0), channel_id=1, source_target_pairs={{0,3},{1,0},{2,1},{3,2},{4,7},{5,4},{6,5},{7,6},{8,11},{9,8},{10,9... | collective-permute-start | bytes 196616 | tf_op jit(solution)/shard_map/ppermute | solution.py:413
  11.7 3.2 %collective-permute-done.1.p2 = bf16[16,2048]{1,0:T(8,128)(2,1)S(1)} collective-permute-done((bf16[16,2048]{1,0:T(8,128)(2,1)S(1)}, bf16[16,2048]{1,0:T(8,128)(2,1)S(1)}, u32[]{:S(2)}, u32[]{:S(2)}) %collective-permute-start.1) | collective-permute-done | bytes 65568 | tf_op jit(solution)/shard_map/ppermute | solution.py:413
  16.5 13.7 %all-to-all-start = ((bf16[64,8,768]{2,1,0:T(8,128)(2,1)}), bf16[64,8,768]{2,1,0:T(8,128)(2,1)S(1)}, u32[]{:S(2)}, u32[]{:S(2)}) async-start(bf16[64,8,768]{2,1,0:T(8,128)(2,1)} %bitcast.17), calls=%async_computation | async-start | bytes 1572864 | tf_op jit(solution)/shard_map/all_to_all | solution.py:422
  30.2 2.3 %shard_map.196 = (bf16[256,512]{1,0:T(8,128)(2,1)}, bf16[256,512]{1,0:T(8,128)(2,1)}, bf16[256,512]{1,0:T(8,128)(2,1)}, bf16[256,512]{1,0:T(8,128)(2,1)}) custom-call(s32[1]{0:T(128)} %bitcast.part_ref, bf16[1,256,2048]{2,1,0:T(8,128)(2,1)} %down_hbm), custom_call_target="tpu_custom_call" | custom-call | tf_op jit(solution)/shard_map/pallas_call | solution.py:47
  32.6 3.6 %collective-permute-start.4 = (bf16[256,512]{1,0:T(8,128)(2,1)}, bf16[256,512]{1,0:T(8,128)(2,1)S(1)}, u32[]{:S(2)}, u32[]{:S(2)}) collective-permute-start(bf16[256,512]{1,0:T(8,128)(2,1)} %get-tuple-element.33), channel_id=1, source_target_pairs={{0,2},{1,3},{2,0},{3,1},{4,6},{5,7},{6,4},{7,5},{8,10},{9,11},{10,... | collective-permute-start | bytes 786440 | tf_op jit(solution)/shard_map/ppermute | solution.py:432
  36.3 5.2 %collective-permute-done.3.d1 = bf16[256,512]{1,0:T(8,128)(2,1)S(1)} collective-permute-done((bf16[256,512]{1,0:T(8,128)(2,1)}, bf16[256,512]{1,0:T(8,128)(2,1)S(1)}, u32[]{:S(2)}, u32[]{:S(2)}) %collective-permute-start.3) | collective-permute-done | bytes 262176 | tf_op jit(solution)/shard_map/ppermute | solution.py:432
  41.5 6.6 %collective-permute-done.4.d2 = bf16[256,512]{1,0:T(8,128)(2,1)S(1)} collective-permute-done((bf16[256,512]{1,0:T(8,128)(2,1)}, bf16[256,512]{1,0:T(8,128)(2,1)S(1)}, u32[]{:S(2)}, u32[]{:S(2)}) %collective-permute-start.4) | collective-permute-done | bytes 262176 | tf_op jit(solution)/shard_map/ppermute | solution.py:432
  48.8 4.4 %all-to-all-done = bf16[64,8,768]{2,1,0:T(8,128)(2,1)S(1)} async-done(((bf16[64,8,768]{2,1,0:T(8,128)(2,1)}), bf16[64,8,768]{2,1,0:T(8,128)(2,1)S(1)}, u32[]{:S(2)}, u32[]{:S(2)}) %all-to-all-start) | async-done | bytes 786464 | tf_op jit(solution)/shard_map/all_to_all | solution.py:422
  54.5 2.6 %collective-permute-start.8 = (bf16[192,256]{1,0:T(8,128)(2,1)S(1)}, bf16[192,256]{1,0:T(8,128)(2,1)S(1)}, u32[]{:S(2)}, u32[]{:S(2)}) collective-permute-start(bf16[192,256]{1,0:T(8,128)(2,1)S(1)} %get-tuple-element.35.h0), channel_id=1, source_target_pairs={{0,3},{1,0},{2,1},{3,2},{4,7},{5,4},{6,5},{7,6},{8,11},{9,8},{10,9... | collective-permute-start | bytes 294920 | tf_op jit(solution)/shard_map/ppermute | solution.py:449
  58.6 2.9 %collective-permute-done.9 = bf16[1,32,256]{2,1,0:T(8,128)(2,1)S(1)} collective-permute-done((bf16[1,32,256]{2,1,0:T(8,128)(2,1)S(1)}, bf16[1,32,256]{2,1,0:T(8,128)(2,1)S(1)}, u32[]{:S(2)}, u32[]{:S(2)}) %collective-permute-start.9) | collective-permute-done | bytes 16416 | tf_op jit(solution)/shard_map/ppermute | solution.py:407
  62.1 2.7 %collective-permute-done.6.h1 = bf16[192,256]{1,0:T(8,128)(2,1)S(1)} collective-permute-done((bf16[192,256]{1,0:T(8,128)(2,1)S(1)}, bf16[192,256]{1,0:T(8,128)(2,1)S(1)}, u32[]{:S(2)}, u32[]{:S(2)}) %collective-permute-start.6) | collective-permute-done | bytes 98336 | tf_op jit(solution)/shard_map/ppermute | solution.py:449
  66.2 6.3 %all-to-all-start.1 = ((bf16[64,8,256]{2,1,0:T(8,128)(2,1)}), bf16[64,8,256]{2,1,0:T(8,128)(2,1)S(1)}, u32[]{:S(2)}, u32[]{:S(2)}) async-start(bf16[64,8,256]{2,1,0:T(8,128)(2,1)} %bitcast.16), calls=%async_computation.1 | async-start | bytes 524288 | tf_op jit(solution)/shard_map/all_to_all | solution.py:457
  72.5 3.8 %collective-permute-start.12 = (bf16[2,32,256]{2,1,0:T(8,128)(2,1)S(1)}, bf16[2,32,256]{2,1,0:T(8,128)(2,1)S(1)}, u32[]{:S(2)}, u32[]{:S(2)}) collective-permute-start(bf16[2,32,256]{2,1,0:T(8,128)(2,1)S(1)} %constant_dynamic-update-slice_fusion.r0), channel_id=1, source_target_pairs={{0,192},{4,196},{8,200},{12,204},{16,208},{20,212},{24,216},{28,22... | collective-permute-start | bytes 98312 | tf_op jit(solution)/shard_map/ppermute | solution.py:407
  76.3 1.9 %collective-permute-start.11 = (bf16[2,32,256]{2,1,0:T(8,128)(2,1)S(1)}, bf16[2,32,256]{2,1,0:T(8,128)(2,1)S(1)}, u32[]{:S(2)}, u32[]{:S(2)}) collective-permute-start(bf16[2,32,256]{2,1,0:T(8,128)(2,1)S(1)} %constant_dynamic-update-slice_fusion.r0), channel_id=1, source_target_pairs={{0,128},{4,132},{8,136},{12,140},{16,144},{20,148},{24,152},{28,15... | collective-permute-start | bytes 98312 | tf_op jit(solution)/shard_map/ppermute | solution.py:407
  78.1 2.2 %collective-permute-start.10 = (bf16[2,32,256]{2,1,0:T(8,128)(2,1)S(1)}, bf16[2,32,256]{2,1,0:T(8,128)(2,1)S(1)}, u32[]{:S(2)}, u32[]{:S(2)}) collective-permute-start(bf16[2,32,256]{2,1,0:T(8,128)(2,1)S(1)} %constant_dynamic-update-slice_fusion.r0), channel_id=1, source_target_pairs={{0,64},{4,68},{8,72},{12,76},{16,80},{20,84},{24,88},{28,92},{32,9... | collective-permute-start | bytes 98312 | tf_op jit(solution)/shard_map/ppermute | solution.py:407
  81.4 3.7 %collective-permute-done.11.r2 = bf16[2,32,256]{2,1,0:T(8,128)(2,1)S(1)} collective-permute-done((bf16[2,32,256]{2,1,0:T(8,128)(2,1)S(1)}, bf16[2,32,256]{2,1,0:T(8,128)(2,1)S(1)}, u32[]{:S(2)}, u32[]{:S(2)}) %collective-permute-start.11) | collective-permute-done | bytes 32800 | tf_op jit(solution)/shard_map/ppermute | solution.py:407
  85.2 2.9 %collective-permute-start.18 = (bf16[8,32,256]{2,1,0:T(8,128)(2,1)S(1)}, bf16[8,32,256]{2,1,0:T(8,128)(2,1)S(1)}, u32[]{:S(2)}, u32[]{:S(2)}) collective-permute-start(bf16[8,32,256]{2,1,0:T(8,128)(2,1)S(1)} %shard_map.200.b0), channel_id=1, source_target_pairs={{0,24},{4,28},{8,0},{12,4},{16,8},{20,12},{24,16},{28,20},{32,56},... | collective-permute-start | bytes 393224 | tf_op jit(solution)/shard_map/ppermute | solution.py:407
  88.9 2.3 %collective-permute-start.13 = (bf16[8,32,256]{2,1,0:T(8,128)(2,1)S(1)}, bf16[8,32,256]{2,1,0:T(8,128)(2,1)S(1)}, u32[]{:S(2)}, u32[]{:S(2)}) collective-permute-start(bf16[8,32,256]{2,1,0:T(8,128)(2,1)S(1)} %shard_map.200.b0), channel_id=1, source_target_pairs={{0,4},{4,0},{8,12},{12,8},{16,20},{20,16},{24,28},{28,24},{32,36},... | collective-permute-start | bytes 393224 | tf_op jit(solution)/shard_map/ppermute | solution.py:407
  91.3 3.4 %collective-permute-start.19 = (bf16[8,32,256]{2,1,0:T(8,128)(2,1)S(1)}, bf16[8,32,256]{2,1,0:T(8,128)(2,1)S(1)}, u32[]{:S(2)}, u32[]{:S(2)}) collective-permute-start(bf16[8,32,256]{2,1,0:T(8,128)(2,1)S(1)} %collective-permute-done.18.b6), channel_id=1, source_target_pairs={{0,4},{4,0},{8,12},{12,8},{16,20},{20,16},{24,28},{28,24},{32,36},... | collective-permute-start | bytes 393224 | tf_op jit(solution)/shard_map/ppermute | solution.py:407
  94.7 2.3 %collective-permute-start.17 = (bf16[8,32,256]{2,1,0:T(8,128)(2,1)S(1)}, bf16[8,32,256]{2,1,0:T(8,128)(2,1)S(1)}, u32[]{:S(2)}, u32[]{:S(2)}) collective-permute-start(bf16[8,32,256]{2,1,0:T(8,128)(2,1)S(1)} %collective-permute-done.16.b4), channel_id=1, source_target_pairs={{0,4},{4,0},{8,12},{12,8},{16,20},{20,16},{24,28},{28,24},{32,36},... | collective-permute-start | bytes 393224 | tf_op jit(solution)/shard_map/ppermute | solution.py:407
  98.3 2.2 %shard_map.199 = (bf16[96,512]{1,0:T(8,128)(2,1)S(1)}, bf16[16,128]{1,0:T(8,128)(2,1)}, f32[16,128]{1,0:T(8,128)S(1)}) custom-call(s32[6,16]{1,0:T(8,128)} %bitcast.23, f32[6,16]{1,0:T(8,128)} %bitcast.24, bf16[16,2048]{1,0:T(8,128)(2,1)} %tok_hbm.2, f32[1,2048]{1,0:T(1,128)} %bitcast.21, bf16[64,2048]{1,0:T(8,128)(2,1)} %bitcast.18, ...), custom_call_target="tpu_custom_call" | custom-call | tf_op jit(solution)/shard_map/pallas_call | solution.py:47
  100.6 1.7 %shard_map.201 = (f32[16,512]{1,0:T(8,128)S(1)}, bf16[16,512]{1,0:T(8,128)(2,1)S(1)}, bf16[16,512]{1,0:T(8,128)(2,1)S(1)}, bf16[16,512]{1,0:T(8,128)(2,1)S(1)}) custom-call(s32[2]{0:T(128)S(1)} %pad_add_fusion.at_ref, bf16[16,2048]{1,0:T(8,128)(2,1)S(1)} %copy-done.4, bf16[128,2048]{1,0:T(8,128)(2,1)S(1)} %copy-done.3, ...), custom_call_target="tpu_custom_call" | custom-call | tf_op jit(solution)/shard_map/pallas_call | solution.py:47
  103.6 2.7 %collective-permute-start.22 = (bf16[16,512]{1,0:T(8,128)(2,1)S(1)}, bf16[16,512]{1,0:T(8,128)(2,1)S(1)}, u32[]{:S(2)}, u32[]{:S(2)}) collective-permute-start(bf16[16,512]{1,0:T(8,128)(2,1)S(1)} %get-tuple-element.50), channel_id=1, source_target_pairs={{0,3},{1,0},{2,1},{3,2},{4,7},{5,4},{6,5},{7,6},{8,11},{9,8},{10,9... | collective-permute-start | bytes 49160 | tf_op jit(solution)/shard_map/ppermute | solution.py:469
  (54 shorter events, 15.4 us)
Async XLA Ops:
  6.6 5.1 %collective-permute-start.2 = (bf16[16,2048]{1,0:T(8,128)(2,1)S(1)}, bf16[16,2048]{1,0:T(8,128)(2,1)S(1)}, u32[]{:S(2)}, u32[]{:S(2)}) collective-permute-start(bf16[16,2048]{1,0:T(8,128)(2,1)S(1)} %get-tuple-element.27.p0), channel_id=1, source_target_pairs={{0,3},{1,0},{2,1},{3,2},{4,7},{5,4},{6,5},{7,6},{8,11},{9,8},{10,9... | collective-permute-start | bytes 196616 | tf_op jit(solution)/shard_map/ppermute | solution.py:413
  10.0 4.9 %collective-permute-start.1 = (bf16[16,2048]{1,0:T(8,128)(2,1)S(1)}, bf16[16,2048]{1,0:T(8,128)(2,1)S(1)}, u32[]{:S(2)}, u32[]{:S(2)}) collective-permute-start(bf16[16,2048]{1,0:T(8,128)(2,1)S(1)} %get-tuple-element.27.p0), channel_id=1, source_target_pairs={{0,1},{1,2},{2,3},{3,0},{4,5},{5,6},{6,7},{7,4},{8,9},{9,10},{10,1... | collective-permute-start | bytes 196616 | tf_op jit(solution)/shard_map/ppermute | solution.py:413
  10.0 5.1 %collective-permute-start = (bf16[16,2048]{1,0:T(8,128)(2,1)S(1)}, bf16[16,2048]{1,0:T(8,128)(2,1)S(1)}, u32[]{:S(2)}, u32[]{:S(2)}) collective-permute-start(bf16[16,2048]{1,0:T(8,128)(2,1)S(1)} %get-tuple-element.27.p0), channel_id=1, source_target_pairs={{0,2},{1,3},{2,0},{3,1},{4,6},{5,7},{6,4},{7,5},{8,10},{9,11},{10,... | collective-permute-start | bytes 196616 | tf_op jit(solution)/shard_map/ppermute | solution.py:412
  16.5 36.7 %all-to-all-start = ((bf16[64,8,768]{2,1,0:T(8,128)(2,1)}), bf16[64,8,768]{2,1,0:T(8,128)(2,1)S(1)}, u32[]{:S(2)}, u32[]{:S(2)}) async-start(bf16[64,8,768]{2,1,0:T(8,128)(2,1)} %bitcast.17), calls=%async_computation | async-start | bytes 1572864 | tf_op jit(solution)/shard_map/all_to_all | solution.py:422
  32.6 8.9 %collective-permute-start.3 = (bf16[256,512]{1,0:T(8,128)(2,1)}, bf16[256,512]{1,0:T(8,128)(2,1)S(1)}, u32[]{:S(2)}, u32[]{:S(2)}) collective-permute-start(bf16[256,512]{1,0:T(8,128)(2,1)} %get-tuple-element.32), channel_id=1, source_target_pairs={{0,1},{1,2},{2,3},{3,0},{4,5},{5,6},{6,7},{7,4},{8,9},{9,10},{10,1... | collective-permute-start | bytes 786440 | tf_op jit(solution)/shard_map/ppermute | solution.py:432
  32.6 15.4 %collective-permute-start.4 = (bf16[256,512]{1,0:T(8,128)(2,1)}, bf16[256,512]{1,0:T(8,128)(2,1)S(1)}, u32[]{:S(2)}, u32[]{:S(2)}) collective-permute-start(bf16[256,512]{1,0:T(8,128)(2,1)} %get-tuple-element.33), channel_id=1, source_target_pairs={{0,2},{1,3},{2,0},{3,1},{4,6},{5,7},{6,4},{7,5},{8,10},{9,11},{10,... | collective-permute-start | bytes 786440 | tf_op jit(solution)/shard_map/ppermute | solution.py:432
  36.3 12.5 %collective-permute-start.5 = (bf16[256,512]{1,0:T(8,128)(2,1)}, bf16[256,512]{1,0:T(8,128)(2,1)}, u32[]{:S(2)}, u32[]{:S(2)}) collective-permute-start(bf16[256,512]{1,0:T(8,128)(2,1)} %get-tuple-element.34), channel_id=1, source_target_pairs={{0,3},{1,0},{2,1},{3,2},{4,7},{5,4},{6,5},{7,6},{8,11},{9,8},{10,9... | collective-permute-start | bytes 786440 | tf_op jit(solution)/shard_map/ppermute | solution.py:432
  54.5 7.0 %collective-permute-start.8 = (bf16[192,256]{1,0:T(8,128)(2,1)S(1)}, bf16[192,256]{1,0:T(8,128)(2,1)S(1)}, u32[]{:S(2)}, u32[]{:S(2)}) collective-permute-start(bf16[192,256]{1,0:T(8,128)(2,1)S(1)} %get-tuple-element.35.h0), channel_id=1, source_target_pairs={{0,3},{1,0},{2,1},{3,2},{4,7},{5,4},{6,5},{7,6},{8,11},{9,8},{10,9... | collective-permute-start | bytes 294920 | tf_op jit(solution)/shard_map/ppermute | solution.py:449
  57.0 5.1 %collective-permute-start.7 = (bf16[192,256]{1,0:T(8,128)(2,1)S(1)}, bf16[192,256]{1,0:T(8,128)(2,1)S(1)}, u32[]{:S(2)}, u32[]{:S(2)}) collective-permute-start(bf16[192,256]{1,0:T(8,128)(2,1)S(1)} %get-tuple-element.35.h0), channel_id=1, source_target_pairs={{0,2},{1,3},{2,0},{3,1},{4,6},{5,7},{6,4},{7,5},{8,10},{9,11},{10,... | collective-permute-start | bytes 294920 | tf_op jit(solution)/shard_map/ppermute | solution.py:449
  57.0 7.7 %collective-permute-start.6 = (bf16[192,256]{1,0:T(8,128)(2,1)S(1)}, bf16[192,256]{1,0:T(8,128)(2,1)S(1)}, u32[]{:S(2)}, u32[]{:S(2)}) collective-permute-start(bf16[192,256]{1,0:T(8,128)(2,1)S(1)} %get-tuple-element.35.h0), channel_id=1, source_target_pairs={{0,1},{1,2},{2,3},{3,0},{4,5},{5,6},{6,7},{7,4},{8,9},{9,10},{10,1... | collective-permute-start | bytes 294920 | tf_op jit(solution)/shard_map/ppermute | solution.py:449
  57.7 3.8 %collective-permute-start.9 = (bf16[1,32,256]{2,1,0:T(8,128)(2,1)S(1)}, bf16[1,32,256]{2,1,0:T(8,128)(2,1)S(1)}, u32[]{:S(2)}, u32[]{:S(2)}) collective-permute-start(bf16[1,32,256]{2,1,0:T(8,128)(2,1)S(1)} %get-tuple-element.44), channel_id=1, source_target_pairs={{0,32},{4,36},{8,40},{12,44},{16,48},{20,52},{24,56},{28,60},{32,6... | collective-permute-start | bytes 49160 | tf_op jit(solution)/shard_map/ppermute | solution.py:407
  66.2 41.2 %all-to-all-start.1 = ((bf16[64,8,256]{2,1,0:T(8,128)(2,1)}), bf16[64,8,256]{2,1,0:T(8,128)(2,1)S(1)}, u32[]{:S(2)}, u32[]{:S(2)}) async-start(bf16[64,8,256]{2,1,0:T(8,128)(2,1)} %bitcast.16), calls=%async_computation.1 | async-start | bytes 524288 | tf_op jit(solution)/shard_map/all_to_all | solution.py:457
  72.5 8.9 %collective-permute-start.12 = (bf16[2,32,256]{2,1,0:T(8,128)(2,1)S(1)}, bf16[2,32,256]{2,1,0:T(8,128)(2,1)S(1)}, u32[]{:S(2)}, u32[]{:S(2)}) collective-permute-start(bf16[2,32,256]{2,1,0:T(8,128)(2,1)S(1)} %constant_dynamic-update-slice_fusion.r0), channel_id=1, source_target_pairs={{0,192},{4,196},{8,200},{12,204},{16,208},{20,212},{24,216},{28,22... | collective-permute-start | bytes 98312 | tf_op jit(solution)/shard_map/ppermute | solution.py:407
  76.3 8.9 %collective-permute-start.11 = (bf16[2,32,256]{2,1,0:T(8,128)(2,1)S(1)}, bf16[2,32,256]{2,1,0:T(8,128)(2,1)S(1)}, u32[]{:S(2)}, u32[]{:S(2)}) collective-permute-start(bf16[2,32,256]{2,1,0:T(8,128)(2,1)S(1)} %constant_dynamic-update-slice_fusion.r0), channel_id=1, source_target_pairs={{0,128},{4,132},{8,136},{12,140},{16,144},{20,148},{24,152},{28,15... | collective-permute-start | bytes 98312 | tf_op jit(solution)/shard_map/ppermute | solution.py:407
  78.1 7.0 %collective-permute-start.10 = (bf16[2,32,256]{2,1,0:T(8,128)(2,1)S(1)}, bf16[2,32,256]{2,1,0:T(8,128)(2,1)S(1)}, u32[]{:S(2)}, u32[]{:S(2)}) collective-permute-start(bf16[2,32,256]{2,1,0:T(8,128)(2,1)S(1)} %constant_dynamic-update-slice_fusion.r0), channel_id=1, source_target_pairs={{0,64},{4,68},{8,72},{12,76},{16,80},{20,84},{24,88},{28,92},{32,9... | collective-permute-start | bytes 98312 | tf_op jit(solution)/shard_map/ppermute | solution.py:407
  85.2 6.1 %collective-permute-start.18 = (bf16[8,32,256]{2,1,0:T(8,128)(2,1)S(1)}, bf16[8,32,256]{2,1,0:T(8,128)(2,1)S(1)}, u32[]{:S(2)}, u32[]{:S(2)}) collective-permute-start(bf16[8,32,256]{2,1,0:T(8,128)(2,1)S(1)} %shard_map.200.b0), channel_id=1, source_target_pairs={{0,24},{4,28},{8,0},{12,4},{16,8},{20,12},{24,16},{28,20},{32,56},... | collective-permute-start | bytes 393224 | tf_op jit(solution)/shard_map/ppermute | solution.py:407
  88.1 6.6 %collective-permute-start.16 = (bf16[8,32,256]{2,1,0:T(8,128)(2,1)S(1)}, bf16[8,32,256]{2,1,0:T(8,128)(2,1)S(1)}, u32[]{:S(2)}, u32[]{:S(2)}) collective-permute-start(bf16[8,32,256]{2,1,0:T(8,128)(2,1)S(1)} %shard_map.200.b0), channel_id=1, source_target_pairs={{0,16},{4,20},{8,24},{12,28},{16,0},{20,4},{24,8},{28,12},{32,48},... | collective-permute-start | bytes 393224 | tf_op jit(solution)/shard_map/ppermute | solution.py:407
  88.3 8.7 %collective-permute-start.14 = (bf16[8,32,256]{2,1,0:T(8,128)(2,1)S(1)}, bf16[8,32,256]{2,1,0:T(8,128)(2,1)S(1)}, u32[]{:S(2)}, u32[]{:S(2)}) collective-permute-start(bf16[8,32,256]{2,1,0:T(8,128)(2,1)S(1)} %shard_map.200.b0), channel_id=1, source_target_pairs={{0,8},{4,12},{8,16},{12,20},{16,24},{20,28},{24,0},{28,4},{32,40},... | collective-permute-start | bytes 393224 | tf_op jit(solution)/shard_map/ppermute | solution.py:407
  88.9 11.6 %collective-permute-start.13 = (bf16[8,32,256]{2,1,0:T(8,128)(2,1)S(1)}, bf16[8,32,256]{2,1,0:T(8,128)(2,1)S(1)}, u32[]{:S(2)}, u32[]{:S(2)}) collective-permute-start(bf16[8,32,256]{2,1,0:T(8,128)(2,1)S(1)} %shard_map.200.b0), channel_id=1, source_target_pairs={{0,4},{4,0},{8,12},{12,8},{16,20},{20,16},{24,28},{28,24},{32,36},... | collective-permute-start | bytes 393224 | tf_op jit(solution)/shard_map/ppermute | solution.py:407
  91.3 9.3 %collective-permute-start.19 = (bf16[8,32,256]{2,1,0:T(8,128)(2,1)S(1)}, bf16[8,32,256]{2,1,0:T(8,128)(2,1)S(1)}, u32[]{:S(2)}, u32[]{:S(2)}) collective-permute-start(bf16[8,32,256]{2,1,0:T(8,128)(2,1)S(1)} %collective-permute-done.18.b6), channel_id=1, source_target_pairs={{0,4},{4,0},{8,12},{12,8},{16,20},{20,16},{24,28},{28,24},{32,36},... | collective-permute-start | bytes 393224 | tf_op jit(solution)/shard_map/ppermute | solution.py:407
  94.7 5.9 %collective-permute-start.17 = (bf16[8,32,256]{2,1,0:T(8,128)(2,1)S(1)}, bf16[8,32,256]{2,1,0:T(8,128)(2,1)S(1)}, u32[]{:S(2)}, u32[]{:S(2)}) collective-permute-start(bf16[8,32,256]{2,1,0:T(8,128)(2,1)S(1)} %collective-permute-done.16.b4), channel_id=1, source_target_pairs={{0,4},{4,0},{8,12},{12,8},{16,20},{20,16},{24,28},{28,24},{32,36},... | collective-permute-start | bytes 393224 | tf_op jit(solution)/shard_map/ppermute | solution.py:407
  102.3 4.2 %collective-permute-start.20 = (bf16[16,512]{1,0:T(8,128)(2,1)S(1)}, bf16[16,512]{1,0:T(8,128)(2,1)S(1)}, u32[]{:S(2)}, u32[]{:S(2)}) collective-permute-start(bf16[16,512]{1,0:T(8,128)(2,1)S(1)} %get-tuple-element.48), channel_id=1, source_target_pairs={{0,2},{1,3},{2,0},{3,1},{4,6},{5,7},{6,4},{7,5},{8,10},{9,11},{10,... | collective-permute-start | bytes 49160 | tf_op jit(solution)/shard_map/ppermute | solution.py:468
  103.6 3.8 %collective-permute-start.21 = (bf16[16,512]{1,0:T(8,128)(2,1)S(1)}, bf16[16,512]{1,0:T(8,128)(2,1)S(1)}, u32[]{:S(2)}, u32[]{:S(2)}) collective-permute-start(bf16[16,512]{1,0:T(8,128)(2,1)S(1)} %get-tuple-element.49), channel_id=1, source_target_pairs={{0,1},{1,2},{2,3},{3,0},{4,5},{5,6},{6,7},{7,4},{8,9},{9,10},{10,1... | collective-permute-start | bytes 49160 | tf_op jit(solution)/shard_map/ppermute | solution.py:469
  103.6 3.8 %collective-permute-start.22 = (bf16[16,512]{1,0:T(8,128)(2,1)S(1)}, bf16[16,512]{1,0:T(8,128)(2,1)S(1)}, u32[]{:S(2)}, u32[]{:S(2)}) collective-permute-start(bf16[16,512]{1,0:T(8,128)(2,1)S(1)} %get-tuple-element.50), channel_id=1, source_target_pairs={{0,3},{1,0},{2,1},{3,2},{4,7},{5,4},{6,5},{7,6},{8,11},{9,8},{10,9... | collective-permute-start | bytes 49160 | tf_op jit(solution)/shard_map/ppermute | solution.py:469
  (9 other events, 285.7 us)
